TPU v7x, 256 devices: a whole 4x4x8 slice. The times are simulated.
256 devices in a mesh: sp: 32 (over z, x), fs: 4 (over y), tp: 2 (over core).
Axes of the slice: x: 4, y: 4, z: 8, core: 2. Of those that a mesh axis runs over, the one named last changes fastest.
Arguments:
- inputs: bfloat16 [4, 4096, 2048], P('fs', 'sp', 'tp'), may hold values from -1000 to 1000
- input_norm_gain: float32 [2048], replicated, may hold values from 0.1 to 1.9
- receptance_weight: bfloat16 [2048, 1024], P(('sp', 'fs'), 'tp'), may hold values from -0.125 to 0.125
- linear_key_weight: bfloat16 [2048, 1024], P(('sp', 'fs'), 'tp'), may hold values from -0.125 to 0.125
- linear_value_weight: bfloat16 [2048, 1024], P(('sp', 'fs'), 'tp'), may hold values from -0.125 to 0.125
- window_query_weight: bfloat16 [2048, 1024], P(('sp', 'fs'), 'tp'), may hold values from -1 to 1
- window_key_weight: bfloat16 [2048, 256], P(('sp', 'fs'), 'tp'), may hold values from -1 to 1
- window_value_weight: bfloat16 [2048, 256], P(('sp', 'fs'), 'tp'), may hold values from -0.125 to 0.125
- decay_down_weight: bfloat16 [2048, 96], replicated, may hold values from -0.125 to 0.125
- decay_up_weight: bfloat16 [2, 96, 1024], replicated, may hold values from -1 to 1
- decay_offset: float32 [2, 1024], replicated, may hold values from -13 to -3
- decay_log_extra: float32 [4, 16, 4096], P('fs', 'tp', 'sp'), may hold values from -1.4 to 0
- erasure_down_weight: bfloat16 [2048, 96], replicated, may hold values from -0.125 to 0.125
- erasure_up_weight: bfloat16 [2, 96, 1024], replicated, may hold values from -0.625 to 0.625
- erasure_offset: float32 [2, 1024], replicated, may hold values from -9.5 to 1
- initial_state: float32 [2, 16, 64, 64], replicated, may hold values from -384 to 384
- head_norm_gain: float32 [1024], replicated, may hold values from 0.1 to 1.9
- query_sink_logit: float32 [16], replicated, may hold values from 2 to 7
- linear_output_weight: bfloat16 [1024, 2048], P('tp', ('sp', 'fs')), may hold values from -0.1875 to 0.1875
- window_output_weight: bfloat16 [1024, 2048], P('tp', ('sp', 'fs')), may hold values from -1.5 to 1.5
Outputs:
- layer_out: bfloat16 [4, 4096, 2048], P('fs', ('sp', 'tp'))
All inputs are finite; a program needn't handle non-finite values.
Results may differ from a plain program's by a relative error of at most 0.006.
The roundings to bfloat16 on the way count: a program that leaves them out, or rounds other values in their place, can miss the bound.
Values may be sent and summed in bfloat16 or wider, within the bound.
A program may use at most 128 MiB of HBM per device.

v0:
```python
import jax
import jax.numpy as jnp
from jax import lax
from jax.sharding import Mesh
from jax.sharding import PartitionSpec as P

HD = 64
WINDOW = 128
GRID_W = 64
ATT_BLOCK = 128
SPAN = 8
SP = ("sp_0", "sp_1")
SP_FS = ("sp_0", "sp_1", "fs")
SP_TP = ("sp_0", "sp_1", "tp")


NORM_EPS = 1e-06
GROUP_EPS = 0.00064
ROPE_BASE = 10000.0
HIGHEST = lax.Precision.HIGHEST


def laid_out(parts, dim):
    parts = jnp.moveaxis(parts, 0, dim)
    dims = parts.shape
    return parts.reshape(*dims[:dim], dims[dim] * dims[dim + 1], *dims[dim + 2 :])


def from_everyone(value, axis):
    copies = jnp.broadcast_to(value, (lax.axis_size(axis), *value.shape))
    return lax.all_to_all(copies, axis, split_axis=0, concat_axis=0, tiled=True)


def gather_directly(value, axis, dim):
    return laid_out(from_everyone(value, axis), dim)


def whole_of(value, axes, dim):
    out = value
    for number in range(len(axes) - 1, -1, -1):
        out = lax.all_gather(out, axes[number], axis=dim, tiled=True)
    return out


def neutral_like(value, identity):
    return jax.tree.map(
        lambda a, e: jnp.broadcast_to(jnp.asarray(e, a.dtype), a.shape), value, identity
    )


def prefix_by_axis(value, axes, combine, identity, reverse):
    before = start = neutral_like(value, identity)
    subtotal = value
    for axis in reversed(axes):
        size, place = (lax.axis_size(axis), lax.axis_index(axis))
        pieces = jax.tree.map(lambda part: lax.all_gather(part, axis), subtotal)
        inside, subtotal = (start, start)
        for k in reversed(range(size)) if reverse else range(size):
            passed = k > place if reverse else k < place
            subtotal = combine(subtotal, jax.tree.map(lambda part: part[k], pieces))
            inside = jax.tree.map(lambda new, old: jnp.where(passed, new, old), subtotal, inside)
        before = combine(inside, before)
    return before


def padded(block, sides, width):
    for axis, dim in sides:
        count = lax.axis_size(axis)
        forward = [(i, i + 1) for i in range(count - 1)]
        backward = [(target, source) for source, target in forward]
        low = lax.ppermute(
            lax.slice_in_dim(block, block.shape[dim] - width, None, axis=dim), axis, forward
        )
        high = lax.ppermute(lax.slice_in_dim(block, 0, width, axis=dim), axis, backward)
        block = jnp.concatenate([low, block, high], axis=dim)
    return block


def turned_gather(arrays, axis, dims):
    turned = [jnp.moveaxis(a, dim, 0) for a, dim in zip(arrays, dims)]
    both = jnp.concatenate([t.reshape(len(t), -1) for t in turned], axis=1)
    out, at, gathered = (lax.all_gather(both, axis, axis=0, tiled=True), 0, [])
    for t, dim in zip(turned, dims):
        share = out[:, at : at + t[0].size].reshape(-1, *t.shape[1:])
        gathered.append(jnp.moveaxis(share, 0, dim))
        at += t[0].size
    return tuple(gathered)


def cut_along(value, dim, size):
    dims = value.shape
    parts = value.reshape(*dims[:dim], size, dims[dim] // size, *dims[dim + 1 :])
    return jnp.moveaxis(parts, dim, 0)


def sum_at_owner(value, axis, dim):
    parts = cut_along(value, dim, lax.axis_size(axis))
    arrived = lax.all_to_all(parts, axis, split_axis=0, concat_axis=0, tiled=True)
    return arrived.sum(axis=0)


def to_bf16(array):
    return lax.optimization_barrier(array.astype(jnp.bfloat16))


def rope_axial(values, positions):
    quarter = values.shape[-1] // 4
    inverse = ROPE_BASE ** (-jnp.arange(quarter, dtype=jnp.float32) / quarter)
    grid_rows = (positions // GRID_W).astype(jnp.float32)
    grid_cols = (positions % GRID_W).astype(jnp.float32)
    pieces = []
    for which_half, coordinate in ((0, grid_rows), (1, grid_cols)):
        angles = coordinate[:, None] * inverse[None, :]
        cosine = jnp.cos(angles)[:, None, :]
        sine_part = jnp.sin(angles)[:, None, :]
        front_part = values[..., 2 * which_half * quarter : (2 * which_half + 1) * quarter]
        back_part = values[..., (2 * which_half + 1) * quarter : (2 * which_half + 2) * quarter]
        pieces.append(front_part * cosine - back_part * sine_part)
        pieces.append(front_part * sine_part + back_part * cosine)
    return jnp.concatenate(pieces, axis=-1)


def compose(earlier, later):
    return (
        jnp.einsum("...ij,...jk->...ik", earlier[0], later[0], precision=HIGHEST),
        jnp.einsum("...ij,...jk->...ik", earlier[1], later[0], precision=HIGHEST) + later[1],
    )


def to_steps(stacked):
    directions, tokens, head_count, head_size = stacked.shape
    blocked = stacked.reshape(directions, tokens // SPAN, SPAN, head_count, head_size)
    return jnp.transpose(blocked, (2, 4, 0, 1, 3)).reshape(SPAN, head_size, -1)


def segment_pass(read_steps, decay_steps, key_steps, unit_steps, erase_steps):
    batch = read_steps.shape[2]

    def advance(step_idx, carry):
        diagonal, left_side, right_side, carried, read_outs, key_outs = carry
        read_now = lax.dynamic_index_in_dim(read_steps, step_idx, 0, keepdims=False)
        decay_now = lax.dynamic_index_in_dim(decay_steps, step_idx, 0, keepdims=False)
        key_now = lax.dynamic_index_in_dim(key_steps, step_idx, 0, keepdims=False)
        unit_now = lax.dynamic_index_in_dim(unit_steps, step_idx, 0, keepdims=False)
        erase_now = lax.dynamic_index_in_dim(erase_steps, step_idx, 0, keepdims=False)
        marker = (jnp.arange(SPAN) == step_idx).astype(jnp.float32)[None, :, None]
        intersection = jnp.einsum("icg,ig->cg", right_side, unit_now, precision=HIGHEST)
        column = diagonal * unit_now - jnp.einsum(
            "icg,cg->ig", left_side, intersection, precision=HIGHEST
        )
        left_side = left_side + column[:, None, :] * marker
        right_side = right_side * decay_now[:, None, :] + erase_now[:, None, :] * marker
        diagonal = diagonal * decay_now
        along = jnp.einsum("ig,icg->cg", unit_now, carried, precision=HIGHEST)
        carried = (
            carried * decay_now[:, None, :]
            - erase_now[:, None, :] * along[None, :, :]
            + key_now[:, None, :] * marker
        )
        read_weights = jnp.einsum("icg,ig->cg", right_side, read_now, precision=HIGHEST)
        read_vec = diagonal * read_now - jnp.einsum(
            "icg,cg->ig", left_side, read_weights, precision=HIGHEST
        )
        key_vec = jnp.einsum("icg,ig->cg", carried, read_now, precision=HIGHEST)
        read_outs = lax.dynamic_update_index_in_dim(read_outs, read_vec, step_idx, 0)
        key_outs = lax.dynamic_update_index_in_dim(key_outs, key_vec, step_idx, 0)
        return (diagonal, left_side, right_side, carried, read_outs, key_outs)

    zero_cols = jnp.zeros((HD, SPAN, batch), jnp.float32)
    carry_init = (
        jnp.ones((HD, batch), jnp.float32),
        zero_cols,
        zero_cols,
        zero_cols,
        jnp.zeros((SPAN, HD, batch), jnp.float32),
        jnp.zeros((SPAN, SPAN, batch), jnp.float32),
    )
    return lax.fori_loop(0, SPAN, advance, carry_init)


def local(
    inputs,
    input_norm_gain,
    receptance_weight,
    linear_key_weight,
    linear_value_weight,
    window_query_weight,
    window_key_weight,
    window_value_weight,
    decay_down_weight,
    decay_up_weight,
    decay_offset,
    decay_log_extra,
    erasure_down_weight,
    erasure_up_weight,
    erasure_offset,
    initial_state,
    head_norm_gain,
    query_sink_logit,
    linear_output_weight,
    window_output_weight,
):
    tokens = inputs.shape[1]
    tp_index = lax.axis_index("tp")
    length = tokens * lax.axis_size(SP)
    offset = lax.axis_index(SP) * tokens
    gathered = gather_directly(inputs, "tp", 2)[0]
    widened = gathered.astype(jnp.float32)
    hidden = to_bf16(
        widened
        * lax.rsqrt(jnp.mean(widened * widened, axis=-1, keepdims=True) + NORM_EPS)
        * input_norm_gain
    )
    weights = (
        receptance_weight,
        linear_key_weight,
        linear_value_weight,
        window_query_weight,
        window_key_weight,
        window_value_weight,
    )
    widths = [weight.shape[1] for weight in weights]
    joined = jnp.concatenate(weights, axis=1)
    regrouped = lax.all_to_all(joined, "fs", split_axis=1, concat_axis=0, tiled=True)
    every_seq = gather_directly(hidden, "fs", 0)
    whole_cols = whole_of(regrouped, SP, 0)
    partial_cols = jnp.dot(every_seq, whole_cols, preferred_element_type=jnp.float32)
    returned = lax.all_to_all(to_bf16(partial_cols), "fs", split_axis=0, concat_axis=1, tiled=True)
    bounds = [0]
    for col_width in widths:
        bounds.append(bounds[-1] + col_width)
    projected = [returned[:, bounds[role_idx] : bounds[role_idx + 1]] for role_idx in range(6)]
    recept, lin_keys, lin_values, queries, att_keys, att_values = projected
    head_width = recept.shape[1]
    head_count = head_width // HD
    first_col = tp_index * head_width
    up_decay = lax.dynamic_slice_in_dim(decay_up_weight, first_col, head_width, 2)
    up_learn = lax.dynamic_slice_in_dim(erasure_up_weight, first_col, head_width, 2)
    base_decay = lax.dynamic_slice_in_dim(decay_offset, first_col, head_width, 1)
    base_learn = lax.dynamic_slice_in_dim(erasure_offset, first_col, head_width, 1)
    gain_local = lax.dynamic_slice_in_dim(head_norm_gain, first_col, head_width, 0)
    state_local = lax.dynamic_slice_in_dim(initial_state, tp_index * head_count, head_count, 1)
    decay_spikes = jnp.transpose(decay_log_extra[0])[:, :, None]

    def lin_heads(array):
        return array.astype(jnp.float32).reshape(tokens, head_count, HD)

    read_in = lin_heads(recept)
    key_in = lin_heads(lin_keys)
    value_in = lin_heads(lin_values)
    unit_in = key_in * lax.rsqrt(jnp.sum(key_in * key_in, axis=-1, keepdims=True) + NORM_EPS)
    decay_low = to_bf16(jnp.dot(hidden, decay_down_weight, preferred_element_type=jnp.float32))
    decay_act = to_bf16(jnp.tanh(decay_low.astype(jnp.float32)))
    learn_low = to_bf16(jnp.dot(hidden, erasure_down_weight, preferred_element_type=jnp.float32))
    decay_factors = []
    erases = []
    for direction in range(2):
        pre_decay = base_decay[direction] + jnp.dot(
            decay_act, up_decay[direction], preferred_element_type=jnp.float32
        )
        erasure_rate = lin_heads(jnp.exp(-jax.nn.softplus(-pre_decay) - 0.5))
        decay_factors.append(jnp.exp(decay_spikes - erasure_rate))
        learn = lin_heads(
            jax.nn.sigmoid(
                base_learn[direction]
                + jnp.dot(learn_low, up_learn[direction], preferred_element_type=jnp.float32)
            )
        )
        erases.append(unit_in * learn)

    def both_ways(forward_part, backward_part):
        return to_steps(jnp.stack([forward_part, jnp.flip(backward_part, 0)]))

    read_steps = both_ways(read_in, read_in)
    value_steps = both_ways(value_in, value_in)
    diagonal, left_side, right_side, carried, read_outs, key_outs = segment_pass(
        read_steps,
        both_ways(decay_factors[0], decay_factors[1]),
        both_ways(key_in, key_in),
        both_ways(unit_in, unit_in),
        both_ways(erases[0], erases[1]),
    )
    identity = jnp.eye(HD, dtype=jnp.float32)
    segments = tokens // SPAN
    state_shape = (2, segments, head_count, HD, HD)
    block_prod = (
        jnp.einsum("ig,ij->gij", diagonal, identity)
        - jnp.einsum("icg,jcg->gij", left_side, right_side, precision=HIGHEST)
    ).reshape(state_shape)
    block_add = jnp.einsum("cvg,kcg->gvk", value_steps, carried, precision=HIGHEST).reshape(
        state_shape
    )
    seg_prod = jnp.moveaxis(block_prod, 1, 0)
    seg_add = jnp.moveaxis(block_add, 1, 0)

    def fold_maps(totals, pair):
        return (compose(totals, pair), None)

    total_init = (
        jnp.broadcast_to(identity, (2, head_count, HD, HD)),
        jnp.zeros((2, head_count, HD, HD), jnp.float32),
    )
    (total_prod, total_add), _ = lax.scan(fold_maps, total_init, (seg_prod, seg_add))
    eye_heads = jnp.broadcast_to(identity, (head_count, HD, HD))
    zero_heads = jnp.zeros((head_count, HD, HD), jnp.float32)
    fwd_prod, fwd_add = prefix_by_axis(
        (total_prod[0], total_add[0]), SP, compose, (eye_heads, zero_heads), False
    )
    bwd_prod, bwd_add = prefix_by_axis(
        (total_prod[1], total_add[1]), SP, compose, (eye_heads, zero_heads), True
    )
    entry = jnp.stack(
        [
            jnp.einsum("hvk,hkj->hvj", state_local[0], fwd_prod, precision=HIGHEST) + fwd_add,
            jnp.einsum("hvk,hkj->hvj", state_local[1], bwd_prod, precision=HIGHEST) + bwd_add,
        ]
    )

    def walk_state(state_now, pair):
        later = jnp.einsum("dhvk,dhkj->dhvj", state_now, pair[0], precision=HIGHEST) + pair[1]
        return (later, state_now)

    _, starts = lax.scan(walk_state, entry, (seg_prod, seg_add))
    block_start = jnp.moveaxis(starts, 0, 1)
    read_five = read_outs.reshape(SPAN, HD, 2, segments, head_count)
    key_five = key_outs.reshape(SPAN, SPAN, 2, segments, head_count)
    value_five = value_steps.reshape(SPAN, HD, 2, segments, head_count)
    lin_out = (
        jnp.einsum("dnhvk,ckdnh->dnchv", block_start, read_five, precision=HIGHEST)
        + jnp.einsum("cednh,evdnh->dnchv", key_five, value_five, precision=HIGHEST)
    ).reshape(2, tokens, head_count, HD)
    lin_sum = lin_out[0] + jnp.flip(lin_out[1], 0)
    centred = lin_sum - jnp.mean(lin_sum, axis=-1, keepdims=True)
    normed = centred * lax.rsqrt(jnp.mean(centred * centred, axis=-1, keepdims=True) + GROUP_EPS)
    lin_mix = (normed.reshape(tokens, head_width) * gain_local).astype(jnp.bfloat16)
    positions = offset + jnp.arange(tokens, dtype=jnp.int32)
    query_count = queries.shape[1] // HD
    group_count = att_keys.shape[1] // HD
    group_size = query_count // group_count
    roped_q = rope_axial(
        queries.astype(jnp.float32).reshape(tokens, query_count, HD), positions
    ).astype(jnp.bfloat16)
    roped_k = rope_axial(
        att_keys.astype(jnp.float32).reshape(tokens, group_count, HD), positions
    ).astype(jnp.bfloat16)
    kv_width = group_count * HD
    packed = jnp.concatenate([roped_k.reshape(tokens, kv_width), att_values], axis=1)
    bordered = padded(packed, ((SP, 0),), WINDOW)
    sink_local = lax.dynamic_slice_in_dim(
        query_sink_logit, tp_index * query_count, query_count, 0
    ).reshape(group_count, group_size)[:, :, None, None]
    reach = ATT_BLOCK + 2 * WINDOW
    query_rows = roped_q.reshape(ATT_BLOCK, group_count, group_size, HD)
    key_rows = bordered[:, :kv_width].reshape(reach, group_count, HD)
    value_rows = bordered[:, kv_width:].reshape(reach, group_count, HD)
    scores = jnp.einsum(
        "qgrd,kgd->grqk", query_rows, key_rows, preferred_element_type=jnp.float32
    ) * HD ** (-0.5)
    query_pos = offset + 0 + jnp.arange(ATT_BLOCK, dtype=jnp.int32)
    key_pos = offset + 0 - WINDOW + jnp.arange(reach, dtype=jnp.int32)
    allowed = (
        (jnp.abs(query_pos[:, None] - key_pos[None, :]) <= WINDOW)
        & (key_pos[None, :] >= 0)
        & (key_pos[None, :] < length)
    )
    scores = jnp.where(allowed, scores, -jnp.inf)
    top_score = jnp.maximum(jnp.max(scores, axis=-1, keepdims=True), sink_local)
    raised = jnp.exp(scores - top_score)
    denominator = jnp.exp(sink_local - top_score) + jnp.sum(raised, axis=-1, keepdims=True)
    weights_bf = (raised / denominator).astype(jnp.bfloat16)
    mixed = jnp.einsum("grqk,kgd->qgrd", weights_bf, value_rows, preferred_element_type=jnp.float32)
    outputs = mixed.astype(jnp.bfloat16).reshape(ATT_BLOCK, query_count * HD)
    lin_weight, att_weight = turned_gather(
        (linear_output_weight, window_output_weight), SP_FS, (1, 1)
    )
    layer_out = sum_at_owner(
        jnp.dot(lin_mix, lin_weight, preferred_element_type=jnp.float32)
        + jnp.dot(outputs, att_weight, preferred_element_type=jnp.float32),
        "tp",
        0,
    )
    return layer_out.astype(jnp.bfloat16)[None]


def solution(mesh):
    finer = Mesh(
        mesh.devices.reshape(8, 4, mesh.shape["fs"], mesh.shape["tp"]), ("sp_0", "sp_1", "fs", "tp")
    )
    placed = (
        P("fs", SP, "tp"),
        P(),
        P(SP_FS, "tp"),
        P(SP_FS, "tp"),
        P(SP_FS, "tp"),
        P(SP_FS, "tp"),
        P(SP_FS, "tp"),
        P(SP_FS, "tp"),
        P(),
        P(),
        P(),
        P("fs", "tp", SP),
        P(),
        P(),
        P(),
        P(),
        P(),
        P(),
        P("tp", SP_FS),
        P("tp", SP_FS),
    )
    return jax.shard_map(
        local, mesh=finer, in_specs=placed, out_specs=P("fs", SP_TP, None), check_vma=False
    )
```

profile of v0, /device:TPU:1, one launch (start us, length us, event | category | flops | bytes accessed | tf_op | source)
XLA Modules:
  0.0 655.1 jit_solution(14134650834117106408)
XLA Ops:
  11.1 9.4 %all_to_all.53 = bf16[16,4,576]{2,0,1:T(8,128)(2,1)S(1)} all-to-all(bf16[16,4,576]{2,0,1:T(8,128)(2,1)S(1)} %copy.161), channel_id=1, replica_groups=mesh['sp_0'=8,'sp_1'=4,'fs'=4,'tp'=2] {'fs'}, dimensions={1} | all-to-all | bytes 147456 | tf_op jit(solution)/shard_map/all_to_all | solution.py:224
  20.4 10.6 %all_gather.45 = bf16[256,576]{1,0:T(8,128)(2,1)} all-gather(bf16[64,576]{1,0:T(8,128)(2,1)S(1)} %bitcast.439), channel_id=1, replica_groups=mesh['sp_0'=8,'sp_1'=4,'fs'=4,'tp'=2] {'sp_1'}, dimensions={0}, use_global_device_ids=true | all-gather | bytes 368640 | tf_op jit(solution)/shard_map/all_gather | solution.py:41
  32.2 9.1 %all_to_all.54 = bf16[2,1,128,1024]{2,3,1,0:T(8,128)(2,1)S(1)} all-to-all(bf16[2,1,128,1024]{2,3,1,0:T(8,128)(2,1)S(1)} %broadcast_in_dim.137), channel_id=1, replica_groups=mesh['sp_0'=8,'sp_1'=4,'fs'=4,'tp'=2] {'tp'}, dimensions={0} | all-to-all | bytes 1048576 | tf_op jit(solution)/shard_map/all_to_all | solution.py:31
  43.9 4.6 all-to-all-start.1
  64.6 10.1 %all-to-all-done.1 = bf16[4,128,2048]{2,1,0:T(8,128)(2,1)} async-done(((bf16[4,128,2048]{2,1,0:T(8,128)(2,1)}), bf16[4,128,2048]{2,1,0:T(8,128)(2,1)}, u32[]{:S(2)}, u32[]{:S(2)}) %all-to-all-start.1) | async-done | bytes 2097184 | tf_op jit(solution)/shard_map/all_to_all | solution.py:31
  74.9 3.8 convolution_convert_fusion
  79.6 4.2 all-to-all-start.3
  87.3 2.3 copy.175
  107.5 2.3 copy.177
  116.0 2.3 copy.176
  124.4 2.3 copy.178
  136.7 2.3 copy.179
  139.0 53.3 %while.50 = (s32[]{:T(128)}, f32[64,256]{1,0:T(8,128)S(1)}, f32[64,8,256]{2,1,0:T(8,128)S(1)}, f32[64,8,256]{2,1,0:T(8,128)S(1)}, f32[64,8,256]{2,1,0:T(8,128)S(...) while((s32[]{:T(128)}, f32[64,256]{1,0:T(8,128)S(1)}, ...), condition=%wide.region_3.4_spmd.clone, body=%wide.region_2.3_spmd.clone.sunk | while | flops 3743763 | bytes 6628616 | solution.py:178
  199.5 16.6 %fusion.192 = f32[256,64,64]{2,1,0:T(8,128)} fusion(f32[8,64,256]{1,0,2:T(8,128)} %bitcast.416, f32[64,8,256]{0,1,2:T(8,128)} %copy.190), kind=kOutput, calls=%fused_computation.348 | convolution fusion | flops 100663296 | bytes 5242880 | tf_op jit(solution)/shard_map/cvg,kcg->gvk/dot_general | solution.py:290
  216.1 9.3 %copy.191 = f32[2,16,8,64,64]{3,4,2,0,1:T(8,128)} copy(f32[2,16,8,64,64]{4,3,2,1,0:T(8,128)} %bitcast.412) | data formatting | bytes 8388608 | tf_op jit(solution)/shard_map/reshape | solution.py:290
  228.3 18.7 %bitcast_subtract_fusion.2 = f32[256,64,64]{2,1,0:T(8,128)} fusion(f32[64,256]{0,1:T(8,128)S(1)} %copy.182, f32[64,64]{1,0:T(8,128)S(1)} %fusion.164, f32[64,8,256]{0,1,2:T(8,128)S(1)} %copy-done.6, f32[64,8,256]{0,1,2:T(8,128)} %copy.184), kind=kOutput, calls=%fused_computation.43 | convolution fusion | flops 102760448 | bytes 5324800 | tf_op jit(solution)/shard_map/icg,jcg->gij/dot_general | solution.py:288
  246.9 9.3 %copy.185 = f32[2,16,8,64,64]{3,4,2,0,1:T(8,128)} copy(f32[2,16,8,64,64]{4,3,2,1,0:T(8,128)} %bitcast.413) | data formatting | bytes 8388608 | tf_op jit(solution)/shard_map/reshape | solution.py:289
  256.2 59.0 %while.51 = (s32[]{:T(128)}, f32[2,8,64,64]{2,3,1,0:T(8,128)S(1)}, f32[2,8,64,64]{2,3,1,0:T(8,128)S(1)}, f32[16,2,8,64,64]{3,4,2,1,0:T(8,128)}, f32[16,2,8,64,64]{3,4,2,1,0:T(8,128)}, /*index=5*/s32[]{:T(128)}, s32[]{:T(128)}) while((s32[]{:T(128)}, f32[2,8,64,64]{2,3,1,0:T(8,128)S(1)}, f32[2,8,64,64]{2,3,1,0:T(8,128)S(1)}, ...), condition=%wide.region_5.6_spmd.clone, body=%wide.region_4.5_spmd.clone.sunk | while | flops 100794368 | bytes 3671639 | solution.py:303
  316.2 12.4 %all_gather.47 = f32[4,8,64,64]{3,2,1,0:T(8,128)S(1)} all-gather(f32[1,8,64,64]{3,2,1,0:T(8,128)S(1)} %get-tuple-element.458), channel_id=1, replica_groups=mesh['sp_0'=8,'sp_1'=4,'fs'=4,'tp'=2] {'sp_1'}, dimensions={0}, use_global_device_ids=true | all-gather | bytes 655360 | tf_op jit(solution)/shard_map/all_gather | solution.py:56
  329.6 12.4 %all_gather.50 = f32[4,8,64,64]{3,2,1,0:T(8,128)S(1)} all-gather(f32[1,8,64,64]{3,2,1,0:T(8,128)S(1)} %get-tuple-element.456), channel_id=1, replica_groups=mesh['sp_0'=8,'sp_1'=4,'fs'=4,'tp'=2] {'sp_1'}, dimensions={0}, use_global_device_ids=true | all-gather | bytes 655360 | tf_op jit(solution)/shard_map/all_gather | solution.py:56
  349.4 11.0 %all_gather.53 = f32[4,8,64,64]{3,2,1,0:T(8,128)S(1)} all-gather(f32[1,8,64,64]{3,2,1,0:T(8,128)S(1)} %copy-done.29), channel_id=1, replica_groups=mesh['sp_0'=8,'sp_1'=4,'fs'=4,'tp'=2] {'sp_1'}, dimensions={0}, use_global_device_ids=true | all-gather | bytes 655360 | tf_op jit(solution)/shard_map/all_gather | solution.py:56
  360.4 14.0 %all_gather.56 = f32[4,8,64,64]{3,2,1,0:T(8,128)S(1)} all-gather(f32[1,8,64,64]{3,2,1,0:T(8,128)} %get-tuple-element.457), channel_id=1, replica_groups=mesh['sp_0'=8,'sp_1'=4,'fs'=4,'tp'=2] {'sp_1'}, dimensions={0}, use_global_device_ids=true | all-gather | bytes 655360 | tf_op jit(solution)/shard_map/all_gather | solution.py:56
  385.8 3.4 collective-permute-start
  398.3 33.6 %all-gather.15.cloned.1.call-done = f32[64,64,64]{2,1,0:T(8,128)} async-done(((f32[8,64,64]{2,1,0:T(8,128)}), f32[64,64,64]{2,1,0:T(8,128)}) %all-gather.15.cloned.1.call-update) | async-done | bytes 1048592 | tf_op jit(solution)/shard_map/all_gather | solution.py:56
  447.7 25.4 %all-gather.21.cloned.1.call-done = f32[64,64,64]{2,1,0:T(8,128)} async-done(((f32[8,64,64]{2,1,0:T(8,128)}), f32[64,64,64]{2,1,0:T(8,128)}) %all-gather.21.cloned.1.call-update) | async-done | bytes 1048592 | tf_op jit(solution)/shard_map/all_gather | solution.py:56
  473.1 41.2 %all-gather.19.cloned.1.call-done = f32[64,64,64]{2,1,0:T(8,128)} async-done(((f32[8,64,64]{2,1,0:T(8,128)}), f32[64,64,64]{2,1,0:T(8,128)}) %all-gather.19.cloned.1.call-update) | async-done | bytes 1048592 | tf_op jit(solution)/shard_map/all_gather | solution.py:56
  531.6 44.3 %while.49 = (s32[]{:T(128)}, f32[2,8,64,64]{2,3,1,0:T(8,128)S(1)}, f32[16,2,8,64,64]{3,4,2,1,0:T(8,128)}, f32[16,2,8,64,64]{3,4,2,1,0:T(8,128)}, f32[16,2,8,64,64]{3,4,2,1,0:T(8,128)}, /*index=5*/s32[]{:T(128)}) while((s32[]{:T(128)}, f32[2,8,64,64]{2,3,1,0:T(8,128)S(1)}, f32[16,2,8,64,64]{3,4,2,1,0:T(8,128)}, ...), condition=%wide.region_7.8_spmd, body=%wide.region_6.7_spmd.sunk | while | flops 50397184 | bytes 2885189 | solution.py:323
  575.9 9.6 %fusion.21 = f32[2,16,8,8,64]{4,2,3,1,0:T(8,128)S(1)} fusion(f32[8,64,2,16,8]{1,0,4,3,2:T(8,128)S(1)} %bitcast.417, f32[16,2,8,64,64]{3,4,2,1,0:T(8,128)} %get-tuple-element.271), kind=kOutput, calls=%fused_computation.52 | convolution fusion | flops 100663296 | bytes 5242880 | tf_op jit(solution)/shard_map/dnhvk,ckdnh->dnchv/dot_general | solution.py:329
  589.1 44.5 %all-gather.13.cloned.1.call-done = bf16[2048,1024]{1,0:T(8,128)(2,1)} async-done(((bf16[16,1024]{1,0:T(8,128)(2,1)}), bf16[2048,1024]{1,0:T(8,128)(2,1)}) %all-gather.13.cloned.1.call-update) | async-done | bytes 4194320 | tf_op jit(solution)/shard_map/all_gather | solution.py:82
  633.6 2.4 fusion.18
  636.0 2.4 convolution_add_fusion
  638.4 8.8 %all_to_all.55 = f32[2,64,2048]{2,1,0:T(8,128)S(1)} all-to-all(f32[2,64,2048]{2,1,0:T(8,128)S(1)} %bitcast.424), channel_id=1, replica_groups=mesh['sp_0'=8,'sp_1'=4,'fs'=4,'tp'=2] {'tp'}, dimensions={0} | all-to-all | bytes 2097152 | tf_op jit(solution)/shard_map/all_to_all | solution.py:98
  (491 shorter events, 299.8 us)
Async XLA Ops:
  6.5 523.1 %copy-start = (f32[2,16,64,64]{3,2,1,0:T(8,128)S(1)}, f32[2,16,64,64]{3,2,1,0:T(8,128)}, u32[]{:S(2)}) copy-start(f32[2,16,64,64]{3,2,1,0:T(8,128)} %param.41) | copy-start | bytes 1572868
  6.5 68.3 %all-gather.11.cloned.1.call-start = ((), (), s32[]{:S(2)}) async-start(), calls=%async_computation.5 | async-start | bytes 2949120 | tf_op jit(solution)/shard_map/all_gather | solution.py:41
  32.1 9.6 %copy-start.36 = (f32[2048]{0:T(1024)S(1)}, f32[2048]{0:T(1024)}, u32[]{:S(2)}) copy-start(f32[2048]{0:T(1024)} %param.27) | copy-start | bytes 24580
  43.9 6.1 copy-start.39
  43.9 6.1 copy-start.40
  43.9 30.7 %all-to-all-start.1 = ((bf16[4,128,2048]{2,1,0:T(8,128)(2,1)}), bf16[4,128,2048]{2,1,0:T(8,128)(2,1)}, u32[]{:S(2)}, u32[]{:S(2)}) async-start(bf16[4,128,2048]{2,1,0:T(8,128)(2,1)} %broadcast_in_dim.138), calls=%async_computation.1 | async-start | bytes 4194304 | tf_op jit(solution)/shard_map/all_to_all | solution.py:31
  52.1 7.2 %copy-start.33 = (f32[1,8,128]{2,1,0:T(8,128)S(1)}, f32[1,8,128]{2,1,0:T(8,128)}, u32[]{:S(2)}) copy-start(f32[1,8,128]{2,1,0:T(8,128)} %param.37) | copy-start | bytes 12292
  79.6 11.6 %all-to-all-start.3 = ((bf16[4,128,576]{1,2,0:T(8,128)(2,1)}), bf16[4,128,576]{1,2,0:T(8,128)(2,1)}, u32[]{:S(2)}, u32[]{:S(2)}) async-start(bf16[4,128,576]{1,2,0:T(8,128)(2,1)} %copy_bitcast_fusion), calls=%async_computation.3 | async-start | bytes 1179648 | tf_op jit(solution)/shard_map/all_to_all | solution.py:228
  83.8 314.5 %all-gather.17.cloned.1.call-start = ((), (), s32[]{:S(2)}) async-start(), calls=%async_computation.8 | async-start | bytes 2359296 | tf_op jit(solution)/shard_map/all_gather | solution.py:56
  104.0 2.3 copy-start.27
  346.3 3.1 copy-start.29
  346.3 85.7 %all-gather.15.cloned.1.call-start = ((), (), s32[]{:S(2)}) async-start(), calls=%async_computation.7 | async-start | bytes 2359296 | tf_op jit(solution)/shard_map/all_gather | solution.py:56
  348.2 12.1 %copy-start.7 = (f32[8,64,64]{2,1,0:T(8,128)}, f32[8,64,64]{2,1,0:T(8,128)S(1)}, u32[]{:S(2)}) copy-start(f32[8,64,64]{2,1,0:T(8,128)S(1)} %fusion.73) | copy-start | bytes 393220
  349.4 123.7 %all-gather.21.cloned.1.call-start = ((), (), s32[]{:S(2)}) async-start(), calls=%async_computation.10 | async-start | bytes 2359296 | tf_op jit(solution)/shard_map/all_gather | solution.py:56
  377.6 4.2 copy-start.34
  377.6 4.2 copy-start.35
  377.6 5.0 copy-start.42
  377.6 5.7 copy-start.41
  378.7 13.0 %copy-start.8 = (f32[8,64,64]{2,1,0:T(8,128)S(1)}, f32[8,64,64]{2,1,0:T(8,128)}, u32[]{:S(2)}) copy-start(f32[8,64,64]{2,1,0:T(8,128)} %copy-done.7) | copy-start | bytes 393220
  378.7 135.6 %all-gather.19.cloned.1.call-start = ((), (), s32[]{:S(2)}) async-start(), calls=%async_computation.9 | async-start | bytes 2359296 | tf_op jit(solution)/shard_map/all_gather | solution.py:56
  381.7 10.5 %copy-start.9 = (f32[8,64,64]{2,1,0:T(8,128)S(1)}, f32[8,64,64]{2,1,0:T(8,128)}, u32[]{:S(2)}) copy-start(f32[8,64,64]{2,1,0:T(8,128)} %fusion.78) | copy-start | bytes 393220
  381.7 10.5 %copy-start.12 = (f32[8,64,64]{2,1,0:T(8,128)S(1)}, f32[8,64,64]{2,1,0:T(8,128)}, u32[]{:S(2)}) copy-start(f32[8,64,64]{2,1,0:T(8,128)} %copy-done.11) | copy-start | bytes 393220
  381.7 251.9 %all-gather.13.cloned.1.call-start = ((), (), s32[]{:S(2)}) async-start(), calls=%async_computation.6 | async-start | bytes 4227072 | tf_op jit(solution)/shard_map/all_gather | solution.py:82
  385.8 9.7 %collective-permute-start = (bf16[128,256]{0,1:T(8,128)(2,1)}, bf16[128,256]{0,1:T(8,128)(2,1)}, u32[]{:S(2)}, u32[]{:S(2)}) collective-permute-start(bf16[128,256]{0,1:T(8,128)(2,1)} %pad_maximum_fusion.2), channel_id=1, source_target_pairs={{0,8},{8,16},{16,24},{24,32},{32,40},{40,48},{48,56},{56,64},{64,7... | collective-permute-start | bytes 196616 | tf_op jit(solution)/shard_map/ppermute | solution.py:71
  389.1 6.4 collective-permute-start.1
  392.2 2.0 copy-start.31
  394.1 2.7 copy-start.38
  432.0 4.4 copy-start.2
  514.3 4.4 copy-start.1
  575.9 9.6 %copy-start.4 = (f32[2,16,8,8,64]{4,2,3,1,0:T(8,128)S(1)}, f32[2,16,8,8,64]{4,2,3,1,0:T(8,128)}, u32[]{:S(2)}) copy-start(f32[2,16,8,8,64]{4,2,3,1,0:T(8,128)} %copy_dynamic-update-slice_fusion) | copy-start | bytes 1572868
  575.9 9.6 %copy-start.5 = (f32[8,8,256]{1,0,2:T(8,128)S(1)}, f32[8,8,256]{1,0,2:T(8,128)}, u32[]{:S(2)}) copy-start(f32[8,8,256]{1,0,2:T(8,128)} %copy.255) | copy-start | bytes 196612
  588.7 47.3 %copy-start.30 = (bf16[2,64,4,128]{3,1,2,0:T(8,128)(2,1)S(1)}, bf16[2,64,4,128]{3,1,2,0:T(8,128)(2,1)}, u32[]{:S(2)}) copy-start(bf16[2,64,4,128]{3,1,2,0:T(8,128)(2,1)} %convolution_convert_fusion.1) | copy-start | bytes 393220
  (21 other events, 25.6 us)
Sparse Core Ops, SparseCore 0:
  31.1 43.6 all-gather.10
  346.4 44.2 all-gather.16
  392.5 39.4 all-gather.14
  433.6 39.4 all-gather.20
  474.7 39.5 all-gather.18
  517.8 115.7 all-gather.12
where the time goes:
time: 668 us; the launch traced here: 655 us
  matrix products  194 us (29%)
  waiting for transfers between devices  157 us (24%)
  local copies, waits for them, and re-layouts  139 us (21%)
  blocking collectives  87.7 us (13%)
  other arithmetic  47.6 us (7%)
  between operations  15.2 us (2%)
  starting transfers between devices  14 us (2%)
    all_gather x4, waiting for transfers between devices, prefix_by_axis(): pieces = jax.tree.map(lambda part: lax.all_gather(part, axis), subtotal)  100 us
    dot_general x44, matrix products, compose(): jnp.einsum('...ij,...jk->...ik', earlier[1], later[0], precision=HIGHEST)  57.9 us
    all_gather x4, blocking collectives, prefix_by_axis(): pieces = jax.tree.map(lambda part: lax.all_gather(part, axis), subtotal)  49.8 us
    all_gather x1, waiting for transfers between devices, turned_gather(): out, at, gathered = (lax.all_gather(both, axis, axis=0, tiled=True), 0, [])  44.5 us
    dot_general x44, matrix products, compose(): jnp.einsum('...ij,...jk->...ik', earlier[0], later[0], precision=HIGHEST)  40.2 us
    dot_general x16, matrix products, walk_state(): jnp.einsum('dhvk,dhkj->dhvj', state_now, pair[0], precision=HIGHEST)  29.4 us
    unnamed x97, local copies, waits for them, and re-layouts  22.5 us
    dot_general x1, matrix products, local(): jnp.einsum('icg,jcg->gij', left_side, right_side, precision=HIGHEST)  18.7 us
  transfers between devices with their start and end apart: 10, of which 7 were waited for; matrix products, arithmetic and copies ran while one was open for 20% of the time, Pallas kernels for 0%

commit v1 on v0

v1 whole, which is shorter than its diff:
```python
import functools
import jax
import jax.numpy as jnp
from jax import lax
from jax.experimental import pallas as pl
from jax.experimental.pallas import tpu as pltpu

from jax.sharding import Mesh
from jax.sharding import PartitionSpec as P

HD = 64
CH = 64
PAIR = 128
WINDOW = 128
GRID_W = 64
ATT_BLOCK = 128
SP = ("sp_0", "sp_1")
SP_FS = ("sp_0", "sp_1", "fs")
SP_TP = ("sp_0", "sp_1", "tp")
NORM_EPS = 1e-06
GROUP_EPS = 0.00064
ROPE_BASE = 10000.0
F32 = jnp.float32
BF = jnp.bfloat16
MESSAGE = jnp.float32
NN = (((1,), (0,)), ((), ()))
NT = (((1,), (1,)), ((), ()))
TN = (((0,), (0,)), ((), ()))


def dot(a, b, dims=NN):
    return lax.dot_general(a, b, dims, preferred_element_type=F32)


def split2(a):
    high = a.astype(BF)
    return high, (a - high.astype(F32)).astype(BF)


def split3(a):
    high, rest = a.astype(BF), None
    rest = a - high.astype(F32)
    mid = rest.astype(BF)
    return high, mid, (rest - mid.astype(F32)).astype(BF)


def mm3(a, b, dims=NN):
    (ka,), (kb,) = dims[0]
    a_hi, a_lo = split2(a)
    b_hi, b_lo = split2(b)
    main = dot(
        jnp.concatenate([a_hi, a_lo], axis=ka), jnp.concatenate([b_hi, b_hi], axis=kb), dims
    )
    return main + dot(a_hi, b_lo, dims)


def mm2(a, b_exact, dims=NN):
    (ka,), (kb,) = dims[0]
    a_hi, a_lo = split2(a)
    return dot(
        jnp.concatenate([a_hi, a_lo], axis=ka), jnp.concatenate([b_exact, b_exact], axis=kb), dims
    )


def iota(shape, dim):
    return lax.broadcasted_iota(jnp.int32, shape, dim)


def ones_where(cond):
    return jnp.where(cond, 1.0, 0.0).astype(BF)


def rates_kernel(
    hidden_ref, down_d_ref, down_e_ref, up_d_ref, up_e_ref, off_d_ref, off_e_ref, extra_ref,
    logd_ref, learn_ref,
):
    width = logd_ref.shape[2]
    start = pl.multiple_of(lax.axis_index("tp") * width, width)
    cols = pl.ds(start, width)
    hidden = hidden_ref[...]
    decay_low = dot(hidden, down_d_ref[...]).astype(BF)
    learn_low = dot(hidden, down_e_ref[...]).astype(BF)
    decay_act = jnp.tanh(decay_low.astype(F32)).astype(BF)
    heads = width // HD
    spread = ones_where(iota((heads, width), 1) // HD == iota((heads, width), 0)).astype(F32)
    spikes = lax.dot_general(
        extra_ref[0], spread, TN, precision=lax.Precision.HIGHEST, preferred_element_type=F32
    )
    for d in range(2):
        x = off_d_ref[d : d + 1, cols] + dot(decay_act, up_d_ref[d, :, cols])
        softplus = jnp.maximum(-x, 0.0) + jnp.log1p(jnp.exp(-jnp.abs(x)))
        logd_ref[d] = spikes - jnp.exp(-softplus - 0.5)
        y = off_e_ref[d : d + 1, cols] + dot(learn_low, up_e_ref[d, :, cols])
        learn_ref[d] = jax.nn.sigmoid(y)


def stacked(x):
    low = iota(x.shape, 1) < HD
    return jnp.concatenate([jnp.where(low, x, 0.0), jnp.where(low, 0.0, x)], axis=0)


def unstacked(x):
    return x[:CH] + x[CH:]


def local_kernel(proj_ref, logd_ref, learn_ref, q_ref, o_ref, msg_ref):
    width = o_ref.shape[1]
    row = iota((2 * CH, 2 * CH), 0)
    col = iota((2 * CH, 2 * CH), 1)
    t, s = row % CH, col % CH
    eye = row == col
    same_head = ones_where(row // HD == col // HD)
    tri = [ones_where((iota((CH, CH), 0) >= iota((CH, CH), 1))), ones_where((iota((CH, CH), 0) <= iota((CH, CH), 1)))]
    strict = [t > s, t < s]
    within = [t >= s, t <= s]

    def one_pair(p, carry):
        lanes = pl.ds(pl.multiple_of(p * PAIR, PAIR), PAIR)
        recept = proj_ref[:, pl.ds(pl.multiple_of(p * PAIR, PAIR), PAIR)].astype(F32)
        keys = proj_ref[:, pl.ds(pl.multiple_of(width + p * PAIR, PAIR), PAIR)].astype(F32)
        values = proj_ref[:, pl.ds(pl.multiple_of(2 * width + p * PAIR, PAIR), PAIR)].astype(F32)
        squares = mm2(keys * keys, same_head)
        unit = keys * lax.rsqrt(squares + NORM_EPS)
        jobs = [(d, c) for d in range(2) for c in range(2)]
        stage = {}
        for d, c in jobs:
            rows = slice(c * CH, (c + 1) * CH)
            logd = logd_ref[d, rows, lanes]
            parts = jnp.concatenate(split3(logd), axis=0)
            total = dot(jnp.concatenate([tri[d]] * 3, axis=1), parts)
            middle = total[CH // 2 - 1 : CH // 2] if d == 0 else total[CH // 2 : CH // 2 + 1]
            last = total[CH - 1 : CH] if d == 0 else total[0:1]
            grow = jnp.exp(total - middle)
            shrink = jnp.exp(middle - total)
            read = recept[rows] * grow
            mark = unit[rows] * jnp.exp(total - logd - middle)
            erase = unit[rows] * learn_ref[d, rows, lanes] * shrink
            key = keys[rows] * shrink
            read_s, mark_s, erase_s, key_s = map(stacked, (read, mark, erase, key))
            scores = mm3(
                jnp.concatenate([mark_s, read_s], axis=0),
                jnp.concatenate([erase_s, key_s], axis=0),
                NT,
            )
            stage[d, c] = (read, mark_s, erase_s, key_s, scores, jnp.exp(middle), jnp.exp(last - middle), jnp.exp(last))
        inverse = {}
        grams = {}
        for d, c in jobs:
            gram = jnp.where(strict[d], stage[d, c][4][: 2 * CH, : 2 * CH], 0.0)
            grams[d, c] = gram
            inverse[d, c] = jnp.where(eye, 1.0, 0.0) - jnp.where(t // 2 == s // 2, gram, 0.0)
        block = 2
        while block < CH:
            joins = (t // (2 * block) == s // (2 * block)) & (t // block != s // block)
            for job in jobs:
                x = inverse[job]
                inverse[job] = x - mm3(x, mm3(jnp.where(joins, grams[job], 0.0), x))
            block *= 2
        maps, reads, outs = {}, {}, {}
        for d, c in jobs:
            rows = slice(c * CH, (c + 1) * CH)
            read, mark_s, erase_s, key_s, scores, to_start, to_end, whole = stage[d, c]
            val_s = stacked(values[rows]).astype(BF)
            cross = jnp.where(strict[d], scores[: 2 * CH, 2 * CH :], 0.0)
            read_e = jnp.where(within[d], scores[2 * CH :, : 2 * CH], 0.0)
            read_k = jnp.where(within[d], scores[2 * CH :, 2 * CH :], 0.0)
            solved = mm3(inverse[d, c], jnp.concatenate([mark_s, mm2(cross, val_s)], axis=1))
            solved = jnp.concatenate([solved[:, :PAIR] * to_start, solved[:, PAIR:]], axis=1)
            taken = mm3(read_e, solved)
            reads[d, c] = read * to_start - unstacked(taken[:, :PAIR])
            outs[d, c] = unstacked(mm2(read_k, val_s) - taken[:, PAIR:])
            ended = mm3(solved, erase_s * to_end, TN)
            k_hi, k_lo = split2(key_s * to_end)
            added = dot(jnp.concatenate([val_s, val_s], axis=0), jnp.concatenate([k_hi, k_lo], axis=0), TN)
            prod = jnp.where(eye, whole - 1.0, 0.0) - ended[:PAIR]
            maps[d, c] = (prod, added - ended[PAIR:])
        out_rows = [outs[0, 0] + outs[1, 0], outs[0, 1] + outs[1, 1]]
        for d in range(2):
            first, second = (0, 1) if d == 0 else (1, 0)
            (prod1, add1), (prod2, add2) = maps[d, first], maps[d, second]
            both = jnp.concatenate([prod1, add1], axis=0)
            through = mm3(reads[d, second], both, NT)
            q_ref[d, first * CH : (first + 1) * CH, lanes] = reads[d, first]
            q_ref[d, second * CH : (second + 1) * CH, lanes] = reads[d, second] + through[:, :PAIR]
            out_rows[second] = out_rows[second] + through[:, PAIR:]
            joined = mm3(both, prod2)
            prod = prod1 + prod2 + joined[:PAIR]
            add = add1 + joined[PAIR:] + add2
            for hh in range(2):
                for half in range(2):
                    message = jnp.concatenate(
                        [
                            folded(prod, hh, hh * HD, HD // 2),
                            folded(add, hh, hh * HD + half * (HD // 2), HD // 4),
                        ],
                        axis=0,
                    )
                    msg_ref[d * 16 + p * 4 + hh * 2 + half] = message.astype(msg_ref.dtype)
        for c in range(2):
            o_ref[c * CH : (c + 1) * CH, lanes] = out_rows[c]
        return carry

    lax.fori_loop(0, width // PAIR, one_pair, 0)


def folded(x, hh, first, count):
    upper, lower = x[first : first + count], x[first + count : first + 2 * count]
    if hh == 0:
        return upper + pltpu.roll(lower, HD, 1)
    return pltpu.roll(upper, HD, 1) + lower


def chain_kernel(recv_ref, init_ref, sent_ref):
    place = lax.axis_index("sp_0") * lax.axis_size("sp_1") + lax.axis_index("sp_1")
    count = recv_ref.shape[0]
    unit_idx = place // 2
    direction, head, half = unit_idx // 8, unit_idx % 8, place % 2
    rows = HD // 2
    start = pl.multiple_of(half * rows, rows)
    state = init_ref[direction, lax.axis_index("tp") * 8 + head, pl.ds(start, rows), :]

    def unfolded(x):
        return jnp.concatenate([x[:, :HD], x[:, HD:]], axis=0)

    for step in range(count):
        idx = direction * (count - 1) + step * (1 - 2 * direction)
        quarter = rows // 2
        sent_ref[idx] = jnp.concatenate([state[:quarter], state[quarter:]], axis=1).astype(sent_ref.dtype)
        if step == count - 1:
            break
        message = recv_ref[idx].astype(F32)
        prod = unfolded(message[:rows])
        state = state + mm3(state, prod) + unfolded(message[rows:])


def finish_kernel(q_ref, o_ref, enter_ref, gain_ref, mix_ref):
    width = o_ref.shape[1]
    row = iota((PAIR, PAIR), 0)
    col = iota((PAIR, PAIR), 1)
    same_head = ones_where(row // HD == col // HD)
    low = iota((HD // 4, PAIR), 1) < HD
    start = lax.axis_index("tp") * width

    def one_pair(p, carry):
        lanes = pl.ds(pl.multiple_of(p * PAIR, PAIR), PAIR)
        out = o_ref[:, lanes]
        for d in range(2):
            pieces = []
            for hh in range(2):
                for half in range(2):
                    m = enter_ref[d * 16 + p * 4 + hh * 2 + half].astype(F32)
                    turned = pltpu.roll(m, HD, 1)
                    if hh == 0:
                        pieces += [jnp.where(low, m, 0.0), jnp.where(low, turned, 0.0)]
                    else:
                        pieces += [jnp.where(low, 0.0, turned), jnp.where(low, 0.0, m)]
            out = out + mm3(q_ref[d, :, lanes], jnp.concatenate(pieces, axis=0), NT)
        centred = out - mm2(out, same_head) * (1.0 / HD)
        spread = mm2(centred * centred, same_head) * (1.0 / HD)
        gain = gain_ref[:, pl.ds(pl.multiple_of(start + p * PAIR, PAIR), PAIR)]
        mix_ref[:, lanes] = (centred * lax.rsqrt(spread + GROUP_EPS) * gain).astype(BF)
        return carry

    lax.fori_loop(0, width // PAIR, one_pair, 0)


def laid_out(parts, dim):
    parts = jnp.moveaxis(parts, 0, dim)
    dims = parts.shape
    return parts.reshape(*dims[:dim], dims[dim] * dims[dim + 1], *dims[dim + 2 :])


def from_everyone(value, axis):
    copies = jnp.broadcast_to(value, (lax.axis_size(axis), *value.shape))
    return lax.all_to_all(copies, axis, split_axis=0, concat_axis=0, tiled=True)


def gather_directly(value, axis, dim):
    return laid_out(from_everyone(value, axis), dim)


def whole_of(value, axes, dim):
    out = value
    for number in range(len(axes) - 1, -1, -1):
        out = lax.all_gather(out, axes[number], axis=dim, tiled=True)
    return out


def padded(block, sides, width):
    for axis, dim in sides:
        count = lax.axis_size(axis)
        forward = [(i, i + 1) for i in range(count - 1)]
        backward = [(target, source) for source, target in forward]
        low = lax.ppermute(
            lax.slice_in_dim(block, block.shape[dim] - width, None, axis=dim), axis, forward
        )
        high = lax.ppermute(lax.slice_in_dim(block, 0, width, axis=dim), axis, backward)
        block = jnp.concatenate([low, block, high], axis=dim)
    return block


def turned_gather(arrays, axis, dims):
    turned = [jnp.moveaxis(a, dim, 0) for a, dim in zip(arrays, dims)]
    both = jnp.concatenate([t.reshape(len(t), -1) for t in turned], axis=1)
    out, at, gathered = (lax.all_gather(both, axis, axis=0, tiled=True), 0, [])
    for t, dim in zip(turned, dims):
        share = out[:, at : at + t[0].size].reshape(-1, *t.shape[1:])
        gathered.append(jnp.moveaxis(share, 0, dim))
        at += t[0].size
    return tuple(gathered)


def cut_along(value, dim, size):
    dims = value.shape
    parts = value.reshape(*dims[:dim], size, dims[dim] // size, *dims[dim + 1 :])
    return jnp.moveaxis(parts, dim, 0)


def sum_at_owner(value, axis, dim):
    parts = cut_along(value, dim, lax.axis_size(axis))
    arrived = lax.all_to_all(parts, axis, split_axis=0, concat_axis=0, tiled=True)
    return arrived.sum(axis=0)


def to_bf16(array):
    return lax.optimization_barrier(array.astype(jnp.bfloat16))


def rope_axial(values, positions):
    quarter = values.shape[-1] // 4
    inverse = ROPE_BASE ** (-jnp.arange(quarter, dtype=jnp.float32) / quarter)
    grid_rows = (positions // GRID_W).astype(jnp.float32)
    grid_cols = (positions % GRID_W).astype(jnp.float32)
    pieces = []
    for which_half, coordinate in ((0, grid_rows), (1, grid_cols)):
        angles = coordinate[:, None] * inverse[None, :]
        cosine = jnp.cos(angles)[:, None, :]
        sine_part = jnp.sin(angles)[:, None, :]
        front_part = values[..., 2 * which_half * quarter : (2 * which_half + 1) * quarter]
        back_part = values[..., (2 * which_half + 1) * quarter : (2 * which_half + 2) * quarter]
        pieces.append(front_part * cosine - back_part * sine_part)
        pieces.append(front_part * sine_part + back_part * cosine)
    return jnp.concatenate(pieces, axis=-1)


def local(
    inputs,
    input_norm_gain,
    receptance_weight,
    linear_key_weight,
    linear_value_weight,
    window_query_weight,
    window_key_weight,
    window_value_weight,
    decay_down_weight,
    decay_up_weight,
    decay_offset,
    decay_log_extra,
    erasure_down_weight,
    erasure_up_weight,
    erasure_offset,
    initial_state,
    head_norm_gain,
    query_sink_logit,
    linear_output_weight,
    window_output_weight,
):
    tokens = inputs.shape[1]
    tp_index = lax.axis_index("tp")
    length = tokens * lax.axis_size(SP)
    offset = lax.axis_index(SP) * tokens
    gathered = gather_directly(inputs, "tp", 2)[0]
    widened = gathered.astype(jnp.float32)
    hidden = to_bf16(
        widened
        * lax.rsqrt(jnp.mean(widened * widened, axis=-1, keepdims=True) + NORM_EPS)
        * input_norm_gain
    )
    weights = (
        receptance_weight,
        linear_key_weight,
        linear_value_weight,
        window_query_weight,
        window_key_weight,
        window_value_weight,
    )
    widths = [weight.shape[1] for weight in weights]
    joined = jnp.concatenate(weights, axis=1)
    regrouped = lax.all_to_all(joined, "fs", split_axis=1, concat_axis=0, tiled=True)
    every_seq = gather_directly(hidden, "fs", 0)
    whole_cols = whole_of(regrouped, SP, 0)
    partial_cols = jnp.dot(every_seq, whole_cols, preferred_element_type=jnp.float32)
    returned = lax.all_to_all(to_bf16(partial_cols), "fs", split_axis=0, concat_axis=1, tiled=True)
    bounds = [0]
    for col_width in widths:
        bounds.append(bounds[-1] + col_width)
    projected = [returned[:, bounds[role_idx] : bounds[role_idx + 1]] for role_idx in range(6)]
    recept, lin_keys, lin_values, queries, att_keys, att_values = projected
    head_width = recept.shape[1]
    logd, learn = pl.pallas_call(
        rates_kernel,
        out_shape=[jax.ShapeDtypeStruct((2, tokens, head_width), F32)] * 2,
        name="rates",
        cost_estimate=pl.CostEstimate(flops=2 * tokens * 2048 * 96 * 4, bytes_accessed=2**21, transcendentals=0),
    )(
        hidden, decay_down_weight, erasure_down_weight, decay_up_weight, erasure_up_weight,
        decay_offset, erasure_offset, decay_log_extra,
    )
    reads, local_out, messages = pl.pallas_call(
        local_kernel,
        out_shape=[
            jax.ShapeDtypeStruct((2, tokens, head_width), F32),
            jax.ShapeDtypeStruct((tokens, head_width), F32),
            jax.ShapeDtypeStruct((32, 48, PAIR), MESSAGE),
        ],
        name="local_maps",
        cost_estimate=pl.CostEstimate(flops=10**9, bytes_accessed=2**21, transcendentals=0),
    )(returned, logd, learn)
    arrived = lax.all_to_all(messages, SP, split_axis=0, concat_axis=0, tiled=True)
    entries = pl.pallas_call(
        chain_kernel,
        out_shape=jax.ShapeDtypeStruct((32, 16, PAIR), MESSAGE),
        name="chain",
    )(arrived, initial_state)
    entered = lax.all_to_all(entries, SP, split_axis=0, concat_axis=0, tiled=True)
    lin_mix = pl.pallas_call(
        finish_kernel,
        out_shape=jax.ShapeDtypeStruct((tokens, head_width), BF),
        name="finish",
    )(reads, local_out, entered, head_norm_gain[None])
    positions = offset + jnp.arange(tokens, dtype=jnp.int32)
    query_count = queries.shape[1] // HD
    group_count = att_keys.shape[1] // HD
    group_size = query_count // group_count
    roped_q = rope_axial(
        queries.astype(jnp.float32).reshape(tokens, query_count, HD), positions
    ).astype(jnp.bfloat16)
    roped_k = rope_axial(
        att_keys.astype(jnp.float32).reshape(tokens, group_count, HD), positions
    ).astype(jnp.bfloat16)
    kv_width = group_count * HD
    packed = jnp.concatenate([roped_k.reshape(tokens, kv_width), att_values], axis=1)
    bordered = padded(packed, ((SP, 0),), WINDOW)
    sink_local = lax.dynamic_slice_in_dim(
        query_sink_logit, tp_index * query_count, query_count, 0
    ).reshape(group_count, group_size)[:, :, None, None]
    reach = ATT_BLOCK + 2 * WINDOW
    query_rows = roped_q.reshape(ATT_BLOCK, group_count, group_size, HD)
    key_rows = bordered[:, :kv_width].reshape(reach, group_count, HD)
    value_rows = bordered[:, kv_width:].reshape(reach, group_count, HD)
    scores = jnp.einsum(
        "qgrd,kgd->grqk", query_rows, key_rows, preferred_element_type=jnp.float32
    ) * HD ** (-0.5)
    query_pos = offset + 0 + jnp.arange(ATT_BLOCK, dtype=jnp.int32)
    key_pos = offset + 0 - WINDOW + jnp.arange(reach, dtype=jnp.int32)
    allowed = (
        (jnp.abs(query_pos[:, None] - key_pos[None, :]) <= WINDOW)
        & (key_pos[None, :] >= 0)
        & (key_pos[None, :] < length)
    )
    scores = jnp.where(allowed, scores, -jnp.inf)
    top_score = jnp.maximum(jnp.max(scores, axis=-1, keepdims=True), sink_local)
    raised = jnp.exp(scores - top_score)
    denominator = jnp.exp(sink_local - top_score) + jnp.sum(raised, axis=-1, keepdims=True)
    weights_bf = (raised / denominator).astype(jnp.bfloat16)
    mixed = jnp.einsum("grqk,kgd->qgrd", weights_bf, value_rows, preferred_element_type=jnp.float32)
    outputs = mixed.astype(jnp.bfloat16).reshape(ATT_BLOCK, query_count * HD)
    lin_weight, att_weight = turned_gather(
        (linear_output_weight, window_output_weight), SP_FS, (1, 1)
    )
    layer_out = sum_at_owner(
        jnp.dot(lin_mix, lin_weight, preferred_element_type=jnp.float32)
        + jnp.dot(outputs, att_weight, preferred_element_type=jnp.float32),
        "tp",
        0,
    )
    return layer_out.astype(jnp.bfloat16)[None]


def solution(mesh):
    finer = Mesh(
        mesh.devices.reshape(8, 4, mesh.shape["fs"], mesh.shape["tp"]), ("sp_0", "sp_1", "fs", "tp")
    )
    placed = (
        P("fs", SP, "tp"),
        P(),
        P(SP_FS, "tp"),
        P(SP_FS, "tp"),
        P(SP_FS, "tp"),
        P(SP_FS, "tp"),
        P(SP_FS, "tp"),
        P(SP_FS, "tp"),
        P(),
        P(),
        P(),
        P("fs", "tp", SP),
        P(),
        P(),
        P(),
        P(),
        P(),
        P(),
        P("tp", SP_FS),
        P("tp", SP_FS),
    )
    return jax.shard_map(
        local, mesh=finer, in_specs=placed, out_specs=P("fs", SP_TP, None), check_vma=False
    )
```

time: 668 us -> 218 us (0.33); the launches traced: 655 us -> 216 us
  matrix products: 194 us -> 8.94 us
  local copies, waits for them, and re-layouts: 139 us -> 14.1 us
  waiting for transfers between devices: 157 us -> 69.2 us
  blocking collectives: 87.7 us -> 38 us
  other arithmetic: 47.6 us -> 3.55 us
  Pallas kernels: 0 us -> 37.7 us
  starting transfers between devices: 14 us -> 31.3 us
    dot_general x116 -> x0, matrix products: 183 us -> none  [the longest x44 57.9 us: compose(): jnp.einsum('...ij,...jk->...ik', earlier[1], later[0], precision=HIGHEST)]
    all_gather x4 -> x0, waiting for transfers between devices: 100 us -> none  [prefix_by_axis(): pieces = jax.tree.map(lambda part: lax.all_gather(part, axis), subtotal)]
    all_gather x4 -> x0, blocking collectives: 49.8 us -> none  [prefix_by_axis(): pieces = jax.tree.map(lambda part: lax.all_gather(part, axis), subtotal)]
    pallas_call x0 -> x4, Pallas kernels: none -> 37.7 us  [the longest x1 21.9 us: local(): pl.pallas_call(local_kernel, out_shape=[jax.ShapeDtypeStruct((2, tokens,...]
    all_gather x1, waiting for transfers between devices: 44.5 us -> 16.2 us  [turned_gather(): out, at, gathered = (lax.all_gather(both, axis, axis=0, tiled=True), 0, [])]
    reshape x8 -> x0, local copies, waits for them, and re-layouts: 26.2 us -> none  [the longest x1 9.28 us: local(): block_prod = (jnp.einsum('ig,ij->gij', diagonal, identity) - jnp.einsum('...]
    all_to_all x0 -> x2, waiting for transfers between devices: none -> 21.4 us  [the longest x1 11.5 us: local(): lax.all_to_all(messages, SP, split_axis=0, concat_axis=0, tiled=True)]
    all_to_all x0 -> x2, starting transfers between devices: none -> 19.4 us  [the longest x1 11.5 us: local(): lax.all_to_all(messages, SP, split_axis=0, concat_axis=0, tiled=True)]
  transfers between devices with their start and end apart: 10 -> 8, of which waited for: 7 -> 7; matrix products, arithmetic and copies ran while one was open for 20% -> 7% of each run, Pallas kernels for 0% -> 17%
where the time goes in v1:
time: 218 us; the launch traced here: 216 us
  waiting for transfers between devices  69.2 us (32%)
  blocking collectives  38 us (17%)
  Pallas kernels  37.7 us (17%)
  starting transfers between devices  31.3 us (14%)
  local copies, waits for them, and re-layouts  14.1 us (6%)
  between operations  13.7 us (6%)
  matrix products  8.94 us (4%)
  other arithmetic  3.55 us (2%)
    pallas_call x1, Pallas kernels, local(): pl.pallas_call(local_kernel, out_shape=[jax.ShapeDtypeStruct((2, tokens,...  21.9 us
    all_to_all x1, waiting for transfers between devices, from_everyone(): return lax.all_to_all(copies, axis, split_axis=0, concat_axis=0, tiled=True)  20.1 us
    all_gather x1, waiting for transfers between devices, turned_gather(): out, at, gathered = (lax.all_gather(both, axis, axis=0, tiled=True), 0, [])  16.2 us
    all_to_all x1, starting transfers between devices, local(): lax.all_to_all(messages, SP, split_axis=0, concat_axis=0, tiled=True)  11.5 us
    all_to_all x1, waiting for transfers between devices, local(): lax.all_to_all(messages, SP, split_axis=0, concat_axis=0, tiled=True)  11.5 us
    all_gather x1, blocking collectives, whole_of(): out = lax.all_gather(out, axes[number], axis=dim, tiled=True)  10.6 us
    all_to_all x1, waiting for transfers between devices, local(): lax.all_to_all(entries, SP, split_axis=0, concat_axis=0, tiled=True)  9.91 us
    all_to_all x1, blocking collectives, local(): lax.all_to_all(joined, 'fs', split_axis=1, concat_axis=0, tiled=True)  9.37 us
  transfers between devices with their start and end apart: 8, of which 7 were waited for; matrix products, arithmetic and copies ran while one was open for 7% of the time, Pallas kernels for 17%

profile of v1, /device:TPU:1, one launch (start us, length us, event | category | flops | bytes accessed | tf_op | source)
XLA Modules:
  0.0 216.4 jit_solution(9994427405104434451)
XLA Ops:
  11.0 9.4 %all_to_all.63 = bf16[16,4,576]{2,0,1:T(8,128)(2,1)S(1)} all-to-all(bf16[16,4,576]{2,0,1:T(8,128)(2,1)S(1)} %copy.43), channel_id=1, replica_groups=mesh['sp_0'=8,'sp_1'=4,'fs'=4,'tp'=2] {'fs'}, dimensions={1} | all-to-all | bytes 147456 | tf_op jit(solution)/shard_map/all_to_all | solution.py:389
  20.3 10.6 %all_gather.9 = bf16[256,576]{1,0:T(8,128)(2,1)} all-gather(bf16[64,576]{1,0:T(8,128)(2,1)S(1)} %bitcast.63), channel_id=1, replica_groups=mesh['sp_0'=8,'sp_1'=4,'fs'=4,'tp'=2] {'sp_1'}, dimensions={0}, use_global_device_ids=true | all-gather | bytes 368640 | tf_op jit(solution)/shard_map/all_gather | solution.py:285
  31.0 1.3 pad_maximum_fusion.2
  32.4 1.0 broadcast_in_dim.12
  33.4 9.1 %all_to_all.64 = bf16[2,1,128,1024]{3,2,1,0:T(8,128)(2,1)S(1)} all-to-all(bf16[2,1,128,1024]{3,2,1,0:T(8,128)(2,1)S(1)} %broadcast_in_dim.12), channel_id=1, replica_groups=mesh['sp_0'=8,'sp_1'=4,'fs'=4,'tp'=2] {'tp'}, dimensions={0} | all-to-all | bytes 1048576 | tf_op jit(solution)/shard_map/all_to_all | solution.py:275
  44.2 1.7 broadcast_in_dim.13
  45.8 3.8 %all-to-all-start.1 = ((bf16[4,128,2048]{2,1,0:T(8,128)(2,1)}), bf16[4,128,2048]{2,1,0:T(8,128)(2,1)S(1)}, u32[]{:S(2)}, u32[]{:S(2)}) async-start(bf16[4,128,2048]{2,1,0:T(8,128)(2,1)} %broadcast_in_dim.13), calls=%async_computation.1 | async-start | bytes 4194304 | tf_op jit(solution)/shard_map/all_to_all | solution.py:275
  49.8 1.0 copy.45.down_d_ref
  50.8 1.0 copy.46.down_e_ref
  51.8 3.6 %rates.1 = (f32[2,128,512]{2,1,0:T(8,128)}, f32[2,128,512]{2,1,0:T(8,128)}) custom-call(bf16[128,2048]{1,0:T(8,128)(2,1)} %copy-done, bf16[2048,96]{1,0:T(8,128)(2,1)} %copy.45.down_d_ref, bf16[2048,96]{1,0:T(8,128)(2,1)} %copy.46.down_e_ref, bf16[2,96,1024]{2,1,0:T(8,128)(2,1)} %up_d_ref.1, bf16[2,96,1024]{2,1,0:T(8,128)(2,1)} %up_e_ref.1, ...), custom_call_target="tpu_custom_call" | custom-call | flops 201326592 | bytes 2097152 | tf_op jit(solution)/shard_map/rates/pallas_call | solution.py:400
  55.5 20.1 %all-to-all-done.1 = bf16[4,128,2048]{2,1,0:T(8,128)(2,1)S(1)} async-done(((bf16[4,128,2048]{2,1,0:T(8,128)(2,1)}), bf16[4,128,2048]{2,1,0:T(8,128)(2,1)S(1)}, u32[]{:S(2)}, u32[]{:S(2)}) %all-to-all-start.1) | async-done | bytes 2097184 | tf_op jit(solution)/shard_map/all_to_all | solution.py:275
  75.6 3.2 %convolution_convert_fusion = bf16[512,576]{0,1:T(8,128)(2,1)S(1)} fusion(bf16[512,2048]{1,0:T(8,128)(2,1)S(1)} %bitcast.61, bf16[2048,576]{1,0:T(8,128)(2,1)} %all-gather.3.cloned.1.call-done), kind=kOutput, calls=%fused_computation.8 | convolution fusion | flops 1208254464 | bytes 5046272 | tf_op jit(solution)/shard_map/dot_general | solution.py:392
  78.8 0.9 copy_bitcast_fusion
  79.7 3.5 %all-to-all-start.3 = ((bf16[4,128,576]{1,2,0:T(8,128)(2,1)}), bf16[4,128,576]{1,2,0:T(8,128)(2,1)S(1)}, u32[]{:S(2)}, u32[]{:S(2)}) async-start(bf16[4,128,576]{1,2,0:T(8,128)(2,1)} %copy_bitcast_fusion), calls=%async_computation.3 | async-start | bytes 1179648 | tf_op jit(solution)/shard_map/all_to_all | solution.py:393
  83.6 6.9 %all-to-all-done.3 = bf16[4,128,576]{1,2,0:T(8,128)(2,1)S(1)} async-done(((bf16[4,128,576]{1,2,0:T(8,128)(2,1)}), bf16[4,128,576]{1,2,0:T(8,128)(2,1)S(1)}, u32[]{:S(2)}, u32[]{:S(2)}) %all-to-all-start.3) | async-done | bytes 589856 | tf_op jit(solution)/shard_map/all_to_all | solution.py:393
  90.5 1.1 copy.47.proj_ref
  91.6 21.9 %local_maps.1 = (f32[2,128,512]{2,1,0:T(8,128)}, f32[128,512]{1,0:T(8,128)}, f32[32,48,128]{2,1,0:T(8,128)}) custom-call(bf16[128,2304]{1,0:T(8,128)(2,1)} %copy.47.proj_ref, f32[2,128,512]{2,1,0:T(8,128)} %get-tuple-element.10.logd_ref, f32[2,128,512]{2,1,0:T(8,128)} %get-tuple-element.11.learn_ref), custom_call_target="tpu_custom_call" | custom-call | flops 1000000000 | bytes 2097152 | tf_op jit(solution)/shard_map/local_maps/pallas_call | solution.py:409
  113.4 11.5 %all-to-all-start.4 = ((f32[32,48,128]{2,1,0:T(8,128)}), f32[32,48,128]{2,1,0:T(8,128)S(1)}, u32[]{:S(2)}, u32[]{:S(2)}) async-start(f32[32,48,128]{2,1,0:T(8,128)} %get-tuple-element.14), calls=%async_computation.4 | async-start | bytes 1572864 | tf_op jit(solution)/shard_map/all_to_all | solution.py:419
  125.0 3.1 %collective-permute-start = (bf16[128,256]{0,1:T(8,128)(2,1)S(1)}, bf16[128,256]{0,1:T(8,128)(2,1)S(1)}, u32[]{:S(2)}, u32[]{:S(2)}) collective-permute-start(bf16[128,256]{0,1:T(8,128)(2,1)S(1)} %pad_maximum_fusion.1), channel_id=1, source_target_pairs={{0,8},{8,16},{16,24},{24,32},{32,40},{40,48},{48,56},{56,64},{64,7... | collective-permute-start | bytes 196616 | tf_op jit(solution)/shard_map/ppermute | solution.py:294
  128.2 1.5 collective-permute-start.1
  130.1 4.2 %collective-permute-done.1 = bf16[128,256]{0,1:T(8,128)(2,1)S(1)} collective-permute-done((bf16[128,256]{0,1:T(8,128)(2,1)S(1)}, bf16[128,256]{0,1:T(8,128)(2,1)S(1)}, u32[]{:S(2)}, u32[]{:S(2)}) %collective-permute-start.1) | collective-permute-done | bytes 65568 | tf_op jit(solution)/shard_map/ppermute | solution.py:297
  135.1 11.5 %all-to-all-done.4.recv_ref = f32[32,48,128]{2,1,0:T(8,128)S(1)} async-done(((f32[32,48,128]{2,1,0:T(8,128)}), f32[32,48,128]{2,1,0:T(8,128)S(1)}, u32[]{:S(2)}, u32[]{:S(2)}) %all-to-all-start.4) | async-done | bytes 786464 | tf_op jit(solution)/shard_map/all_to_all | solution.py:419
  146.6 0.9 copy-done.1
  147.5 8.1 %chain.1 = f32[32,16,128]{2,1,0:T(8,128)} custom-call(f32[32,48,128]{2,1,0:T(8,128)} %copy-done.1, f32[2,16,64,64]{3,2,1,0:T(8,128)} %init_ref.1), custom_call_target="tpu_custom_call" | custom-call | tf_op jit(solution)/shard_map/chain/pallas_call | solution.py:420
  155.6 7.9 %all-to-all-start.5 = ((f32[32,16,128]{2,1,0:T(8,128)}), f32[32,16,128]{2,1,0:T(8,128)S(1)}, u32[]{:S(2)}, u32[]{:S(2)}) async-start(f32[32,16,128]{2,1,0:T(8,128)} %chain.1), calls=%async_computation.5 | async-start | bytes 524288 | tf_op jit(solution)/shard_map/all_to_all | solution.py:425
  163.9 9.9 %all-to-all-done.5.enter_ref = f32[32,16,128]{2,1,0:T(8,128)S(1)} async-done(((f32[32,16,128]{2,1,0:T(8,128)}), f32[32,16,128]{2,1,0:T(8,128)S(1)}, u32[]{:S(2)}, u32[]{:S(2)}) %all-to-all-start.5) | async-done | bytes 262176 | tf_op jit(solution)/shard_map/all_to_all | solution.py:425
  174.6 4.1 %finish.1 = bf16[128,512]{1,0:T(8,128)(2,1)} custom-call(f32[2,128,512]{2,1,0:T(8,128)} %get-tuple-element.12.q_ref, f32[128,512]{1,0:T(8,128)} %get-tuple-element.13.o_ref, f32[32,16,128]{2,1,0:T(8,128)} %copy-done.2, f32[1,1024]{1,0:T(1,128)} %bitcast.77), custom_call_target="tpu_custom_call" | custom-call | tf_op jit(solution)/shard_map/finish/pallas_call | solution.py:426
  178.7 16.2 %all-gather.5.cloned.1.call-done = bf16[2048,1024]{1,0:T(8,128)(2,1)} async-done(((bf16[16,1024]{1,0:T(8,128)(2,1)}), bf16[2048,1024]{1,0:T(8,128)(2,1)}) %all-gather.5.cloned.1.call-update) | async-done | bytes 4194320 | tf_op jit(solution)/shard_map/all_gather | solution.py:305
  194.9 2.5 %fusion.1 = f32[128,2048]{1,0:T(8,128)S(1)} fusion(bf16[128,512]{1,0:T(8,128)(2,1)} %finish.1, bf16[2048,1024]{1,0:T(8,128)(2,1)} %all-gather.5.cloned.1.call-done), kind=kOutput, calls=%fused_computation.2 | convolution fusion | flops 268435456 | bytes 3276800 | tf_op jit(solution)/shard_map/dot_general | solution.py:472
  197.4 2.4 %convolution_add_fusion = f32[128,2048]{1,0:T(8,128)S(1)} fusion(f32[128,2048]{1,0:T(8,128)S(1)} %fusion.1, bf16[128,512]{0,1:T(8,128)(2,1)S(1)} %bitcast.67, bf16[2048,1024]{1,0:T(8,128)(2,1)} %all-gather.5.cloned.1.call-done), kind=kOutput, calls=%fused_computation | convolution fusion | flops 268697600 | bytes 4325376 | tf_op jit(solution)/shard_map/dot_general | solution.py:473
  199.9 8.9 %all_to_all.65 = f32[2,64,2048]{2,1,0:T(8,128)S(1)} all-to-all(f32[2,64,2048]{2,1,0:T(8,128)S(1)} %bitcast.57), channel_id=1, replica_groups=mesh['sp_0'=8,'sp_1'=4,'fs'=4,'tp'=2] {'tp'}, dimensions={0} | all-to-all | bytes 2097152 | tf_op jit(solution)/shard_map/all_to_all | solution.py:321
  208.7 0.8 reduce_sum.29
  (57 shorter events, 9.2 us)
Async XLA Ops:
  6.5 69.1 %all-gather.3.cloned.1.call-start = ((), (), s32[]{:S(2)}) async-start(), calls=%async_computation.7 | async-start | bytes 2949120 | tf_op jit(solution)/shard_map/all_gather | solution.py:285
  30.9 164.0 %all-gather.5.cloned.1.call-start = ((), (), s32[]{:S(2)}) async-start(), calls=%async_computation.8 | async-start | bytes 4227072 | tf_op jit(solution)/shard_map/all_gather | solution.py:305
  42.6 1.4 copy-start.5
  44.2 1.7 copy-start
  45.8 3.8 %copy-start.6 = (f32[16]{0:T(128)S(1)}, f32[16]{0:T(128)}, u32[]{:S(2)}) copy-start(f32[16]{0:T(128)} %param.37) | copy-start | bytes 196
  45.8 3.9 %copy-start.3 = (bf16[2048,96]{0,1:T(8,128)(2,1)S(1)}, bf16[2048,96]{0,1:T(8,128)(2,1)}, u32[]{:S(2)}) copy-start(bf16[2048,96]{0,1:T(8,128)(2,1)} %param.28) | copy-start | bytes 1179652
  45.8 5.0 %copy-start.4 = (bf16[2048,96]{0,1:T(8,128)(2,1)S(1)}, bf16[2048,96]{0,1:T(8,128)(2,1)}, u32[]{:S(2)}) copy-start(bf16[2048,96]{0,1:T(8,128)(2,1)} %param.32) | copy-start | bytes 1179652
  45.8 29.8 %all-to-all-start.1 = ((bf16[4,128,2048]{2,1,0:T(8,128)(2,1)}), bf16[4,128,2048]{2,1,0:T(8,128)(2,1)S(1)}, u32[]{:S(2)}, u32[]{:S(2)}) async-start(bf16[4,128,2048]{2,1,0:T(8,128)(2,1)} %broadcast_in_dim.13), calls=%async_computation.1 | async-start | bytes 4194304 | tf_op jit(solution)/shard_map/all_to_all | solution.py:275
  79.7 10.7 %all-to-all-start.3 = ((bf16[4,128,576]{1,2,0:T(8,128)(2,1)}), bf16[4,128,576]{1,2,0:T(8,128)(2,1)S(1)}, u32[]{:S(2)}, u32[]{:S(2)}) async-start(bf16[4,128,576]{1,2,0:T(8,128)(2,1)} %copy_bitcast_fusion), calls=%async_computation.3 | async-start | bytes 1179648 | tf_op jit(solution)/shard_map/all_to_all | solution.py:393
  113.4 33.1 %all-to-all-start.4 = ((f32[32,48,128]{2,1,0:T(8,128)}), f32[32,48,128]{2,1,0:T(8,128)S(1)}, u32[]{:S(2)}, u32[]{:S(2)}) async-start(f32[32,48,128]{2,1,0:T(8,128)} %get-tuple-element.14), calls=%async_computation.4 | async-start | bytes 1572864 | tf_op jit(solution)/shard_map/all_to_all | solution.py:419
  125.0 5.1 %collective-permute-start = (bf16[128,256]{0,1:T(8,128)(2,1)S(1)}, bf16[128,256]{0,1:T(8,128)(2,1)S(1)}, u32[]{:S(2)}, u32[]{:S(2)}) collective-permute-start(bf16[128,256]{0,1:T(8,128)(2,1)S(1)} %pad_maximum_fusion.1), channel_id=1, source_target_pairs={{0,8},{8,16},{16,24},{24,32},{32,40},{40,48},{48,56},{56,64},{64,7... | collective-permute-start | bytes 196616 | tf_op jit(solution)/shard_map/ppermute | solution.py:294
  128.2 6.1 %collective-permute-start.1 = (bf16[128,256]{0,1:T(8,128)(2,1)S(1)}, bf16[128,256]{0,1:T(8,128)(2,1)S(1)}, u32[]{:S(2)}, u32[]{:S(2)}) collective-permute-start(bf16[128,256]{0,1:T(8,128)(2,1)S(1)} %pad_maximum_fusion.1), channel_id=1, source_target_pairs={{8,0},{16,8},{24,16},{32,24},{40,32},{48,40},{56,48},{64,56},{72,6... | collective-permute-start | bytes 196616 | tf_op jit(solution)/shard_map/ppermute | solution.py:297
  146.6 0.9 copy-start.1
  155.6 18.3 %all-to-all-start.5 = ((f32[32,16,128]{2,1,0:T(8,128)}), f32[32,16,128]{2,1,0:T(8,128)S(1)}, u32[]{:S(2)}, u32[]{:S(2)}) async-start(f32[32,16,128]{2,1,0:T(8,128)} %chain.1), calls=%async_computation.5 | async-start | bytes 524288 | tf_op jit(solution)/shard_map/all_to_all | solution.py:425
  173.9 0.7 copy-start.2
Sparse Core Ops, SparseCore 0:
  31.1 43.6 all-gather.2
  78.3 116.5 all-gather.4

commit v2 on v1

--- a/solution.py
+++ b/solution.py
@@ -22,7 +22,8 @@
 ROPE_BASE = 10000.0
 F32 = jnp.float32
 BF = jnp.bfloat16
-MESSAGE = jnp.float32
+MESSAGE = jnp.bfloat16
+MESH = pl.DeviceIdType.MESH
 NN = (((1,), (0,)), ((), ()))
 NT = (((1,), (1,)), ((), ()))
 TN = (((0,), (0,)), ((), ()))
@@ -210,39 +211,188 @@
     return pltpu.roll(upper, HD, 1) + lower
 
 
-def chain_kernel(recv_ref, init_ref, sent_ref):
+def peer_id(index):
+    inner = lax.axis_size("sp_1")
+    return {"sp_0": index // inner, "sp_1": index % inner}
+
+
+def exchange_kernel(
+    msg_ref, init_ref, reads_ref, local_ref, gain_ref, proj_ref, cos_ref, sin_ref, sink_ref,
+    mix_ref, att_ref,
+    recv_ref, sent_ref, enter_ref, halo_ref,
+    out_sem, in_sem, back_out_sem, back_in_sem, halo_out_sem, halo_in_sem,
+):
+    count = recv_ref.shape[0]
     place = lax.axis_index("sp_0") * lax.axis_size("sp_1") + lax.axis_index("sp_1")
-    count = recv_ref.shape[0]
+    width = local_ref.shape[1]
+    kv_first = 4 * width
+    barrier = pltpu.get_barrier_semaphore()
+
+    def greet(k, carry):
+        pl.semaphore_signal(barrier, inc=1, device_id=peer_id((place + k) % count), device_id_type=MESH)
+        return carry
+
+    lax.fori_loop(1, count, greet, 0)
+    pl.semaphore_wait(barrier, count - 1)
+
+    def halo_copy(side):
+        target = (place + count - 1 + 2 * side) % count
+        return pltpu.make_async_remote_copy(
+            src_ref=proj_ref.at[:, kv_first : kv_first + 2 * PAIR],
+            dst_ref=halo_ref.at[1 - side],
+            send_sem=halo_out_sem.at[side],
+            recv_sem=halo_in_sem.at[1 - side],
+            device_id=peer_id(target),
+            device_id_type=MESH,
+        )
+
+    def map_copy(target):
+        return pltpu.make_async_remote_copy(
+            src_ref=msg_ref.at[target],
+            dst_ref=recv_ref.at[place],
+            send_sem=out_sem.at[target],
+            recv_sem=in_sem.at[place],
+            device_id=peer_id(target),
+            device_id_type=MESH,
+        )
+
+    def map_arrival(source):
+        return pltpu.make_async_remote_copy(
+            src_ref=msg_ref.at[source],
+            dst_ref=recv_ref.at[source],
+            send_sem=out_sem.at[source],
+            recv_sem=in_sem.at[source],
+            device_id=peer_id(source),
+            device_id_type=MESH,
+        )
+
+    def entry_copy(target):
+        return pltpu.make_async_remote_copy(
+            src_ref=sent_ref.at[target],
+            dst_ref=enter_ref.at[place],
+            send_sem=back_out_sem.at[target],
+            recv_sem=back_in_sem.at[place],
+            device_id=peer_id(target),
+            device_id_type=MESH,
+        )
+
+    def entry_arrival(source):
+        return pltpu.make_async_remote_copy(
+            src_ref=sent_ref.at[source],
+            dst_ref=enter_ref.at[source],
+            send_sem=back_out_sem.at[source],
+            recv_sem=back_in_sem.at[source],
+            device_id=peer_id(source),
+            device_id_type=MESH,
+        )
+
+    halo_copy(0).start()
+    halo_copy(1).start()
+
+    def send_map(k, carry):
+        map_copy((place + k) % count).start()
+        return carry
+
+    lax.fori_loop(1, count, send_map, 0)
+    recv_ref[place] = msg_ref[place]
+
+    tokens = local_ref.shape[0]
+    for side in range(2):
+        halo_copy(side).wait()
+    kv = jnp.concatenate(
+        [halo_ref[0], proj_ref[:, kv_first : kv_first + 2 * PAIR], halo_ref[1]], axis=0
+    )
+    lane = iota((1, PAIR), 1)
+    low = lane < HD
+    front = lane % 32 < 16
+
+    def turned(x, rows):
+        other = jnp.where(front, -pltpu.roll(x, PAIR - 16, 1), pltpu.roll(x, 16, 1))
+        return x * cos_ref[rows, :] + other * sin_ref[rows, :]
+
+    reach = 3 * tokens
+    roped_k = turned(kv[:, :PAIR].astype(F32), slice(0, reach))
+    values = kv[:, PAIR:].astype(F32)
+    q_pos = place * tokens + iota((2 * tokens, reach), 0) % tokens
+    k_pos = (place - 1) * tokens + iota((2 * tokens, reach), 1)
+    allowed = (jnp.abs(q_pos - k_pos) <= WINDOW) & (k_pos >= 0) & (k_pos < count * tokens)
+    upper = iota((2 * tokens, 1), 0) < tokens
+    head_first = lax.axis_index("tp") * (width // HD)
+    for group in range(2):
+        doubled = []
+        for x in (roped_k, values):
+            other = pltpu.roll(x, HD, 1)
+            doubled.append((jnp.where(low, x, other) if group == 0 else jnp.where(low, other, x)).astype(BF))
+        for p in (2 * group, 2 * group + 1):
+            lanes = slice(p * PAIR, (p + 1) * PAIR)
+            query = turned(proj_ref[:, 3 * width + p * PAIR : 3 * width + (p + 1) * PAIR].astype(F32), slice(tokens, 2 * tokens))
+            query = jnp.concatenate([jnp.where(low, query, 0.0), jnp.where(low, 0.0, query)], axis=0)
+            scores = dot(query.astype(BF), doubled[0], NT) * HD**-0.5
+            scores = jnp.where(allowed, scores, -jnp.inf)
+            head = head_first + 2 * p
+            sink = jnp.where(upper, sink_ref[head], sink_ref[head + 1])
+            top = jnp.maximum(jnp.max(scores, axis=-1, keepdims=True), sink)
+            raised = jnp.exp(scores - top)
+            total = jnp.exp(sink - top) + jnp.sum(raised, axis=-1, keepdims=True)
+            mixed = dot((raised / total).astype(BF), doubled[1])
+            att_ref[:, lanes] = jnp.where(low, mixed[:tokens], mixed[tokens:]).astype(BF)
+
+    def await_map(k, carry):
+        map_arrival((place + k) % count).wait()
+        return carry
+
+    lax.fori_loop(1, count, await_map, 0)
+
     unit_idx = place // 2
     direction, head, half = unit_idx // 8, unit_idx % 8, place % 2
     rows = HD // 2
+    quarter = rows // 2
     start = pl.multiple_of(half * rows, rows)
-    state = init_ref[direction, lax.axis_index("tp") * 8 + head, pl.ds(start, rows), :]
 
     def unfolded(x):
         return jnp.concatenate([x[:, :HD], x[:, HD:]], axis=0)
 
-    for step in range(count):
-        idx = direction * (count - 1) + step * (1 - 2 * direction)
-        quarter = rows // 2
-        sent_ref[idx] = jnp.concatenate([state[:quarter], state[quarter:]], axis=1).astype(sent_ref.dtype)
-        if step == count - 1:
-            break
+    def nth(step):
+        return direction * (count - 1) + step * (1 - 2 * direction)
+
+    def advance(step, state):
+        idx = nth(step)
+        sent_ref[idx] = jnp.concatenate([state[:quarter], state[quarter:]], axis=1).astype(BF)
+        before = nth(step - 1)
+
+        @pl.when((step > 0) & (before != place))
+        def _():
+            entry_copy(before).start()
+
         message = recv_ref[idx].astype(F32)
-        prod = unfolded(message[:rows])
-        state = state + mm3(state, prod) + unfolded(message[rows:])
-
-
-def finish_kernel(q_ref, o_ref, enter_ref, gain_ref, mix_ref):
+        return state + mm3(state, unfolded(message[:rows])) + unfolded(message[rows:])
+
+    state = init_ref[direction, lax.axis_index("tp") * 8 + head, pl.ds(start, rows), :]
+    lax.fori_loop(0, count, advance, state)
+    final = nth(count - 1)
+    enter_ref[place] = sent_ref[place]
+
+    @pl.when(final != place)
+    def _():
+        entry_copy(final).start()
+
+    def await_entry(k, carry):
+        entry_arrival((place + k) % count).wait()
+        return carry
+
+    lax.fori_loop(1, count, await_entry, 0)
+    finish(reads_ref, local_ref, enter_ref, gain_ref, mix_ref)
+
+
+def finish(q_ref, o_ref, enter_ref, gain_ref, mix_ref):
     width = o_ref.shape[1]
     row = iota((PAIR, PAIR), 0)
     col = iota((PAIR, PAIR), 1)
     same_head = ones_where(row // HD == col // HD)
     low = iota((HD // 4, PAIR), 1) < HD
     start = lax.axis_index("tp") * width
-
-    def one_pair(p, carry):
-        lanes = pl.ds(pl.multiple_of(p * PAIR, PAIR), PAIR)
+    for p in range(width // PAIR):
+        lanes = slice(p * PAIR, (p + 1) * PAIR)
         out = o_ref[:, lanes]
         for d in range(2):
             pieces = []
@@ -254,14 +404,11 @@
                         pieces += [jnp.where(low, m, 0.0), jnp.where(low, turned, 0.0)]
                     else:
                         pieces += [jnp.where(low, 0.0, turned), jnp.where(low, 0.0, m)]
-            out = out + mm3(q_ref[d, :, lanes], jnp.concatenate(pieces, axis=0), NT)
+            out = out + mm2(q_ref[d, :, lanes], jnp.concatenate(pieces, axis=0).astype(BF), NT)
         centred = out - mm2(out, same_head) * (1.0 / HD)
         spread = mm2(centred * centred, same_head) * (1.0 / HD)
         gain = gain_ref[:, pl.ds(pl.multiple_of(start + p * PAIR, PAIR), PAIR)]
         mix_ref[:, lanes] = (centred * lax.rsqrt(spread + GROUP_EPS) * gain).astype(BF)
-        return carry
-
-    lax.fori_loop(0, width // PAIR, one_pair, 0)
 
 
 def laid_out(parts, dim):
@@ -284,19 +431,6 @@
     for number in range(len(axes) - 1, -1, -1):
         out = lax.all_gather(out, axes[number], axis=dim, tiled=True)
     return out
-
-
-def padded(block, sides, width):
-    for axis, dim in sides:
-        count = lax.axis_size(axis)
-        forward = [(i, i + 1) for i in range(count - 1)]
-        backward = [(target, source) for source, target in forward]
-        low = lax.ppermute(
-            lax.slice_in_dim(block, block.shape[dim] - width, None, axis=dim), axis, forward
-        )
-        high = lax.ppermute(lax.slice_in_dim(block, 0, width, axis=dim), axis, backward)
-        block = jnp.concatenate([low, block, high], axis=dim)
-    return block
 
 
 def turned_gather(arrays, axis, dims):
@@ -416,55 +550,37 @@
         name="local_maps",
         cost_estimate=pl.CostEstimate(flops=10**9, bytes_accessed=2**21, transcendentals=0),
     )(returned, logd, learn)
-    arrived = lax.all_to_all(messages, SP, split_axis=0, concat_axis=0, tiled=True)
-    entries = pl.pallas_call(
-        chain_kernel,
-        out_shape=jax.ShapeDtypeStruct((32, 16, PAIR), MESSAGE),
-        name="chain",
-    )(arrived, initial_state)
-    entered = lax.all_to_all(entries, SP, split_axis=0, concat_axis=0, tiled=True)
-    lin_mix = pl.pallas_call(
-        finish_kernel,
-        out_shape=jax.ShapeDtypeStruct((tokens, head_width), BF),
-        name="finish",
-    )(reads, local_out, entered, head_norm_gain[None])
-    positions = offset + jnp.arange(tokens, dtype=jnp.int32)
-    query_count = queries.shape[1] // HD
-    group_count = att_keys.shape[1] // HD
-    group_size = query_count // group_count
-    roped_q = rope_axial(
-        queries.astype(jnp.float32).reshape(tokens, query_count, HD), positions
-    ).astype(jnp.bfloat16)
-    roped_k = rope_axial(
-        att_keys.astype(jnp.float32).reshape(tokens, group_count, HD), positions
-    ).astype(jnp.bfloat16)
-    kv_width = group_count * HD
-    packed = jnp.concatenate([roped_k.reshape(tokens, kv_width), att_values], axis=1)
-    bordered = padded(packed, ((SP, 0),), WINDOW)
-    sink_local = lax.dynamic_slice_in_dim(
-        query_sink_logit, tp_index * query_count, query_count, 0
-    ).reshape(group_count, group_size)[:, :, None, None]
-    reach = ATT_BLOCK + 2 * WINDOW
-    query_rows = roped_q.reshape(ATT_BLOCK, group_count, group_size, HD)
-    key_rows = bordered[:, :kv_width].reshape(reach, group_count, HD)
-    value_rows = bordered[:, kv_width:].reshape(reach, group_count, HD)
-    scores = jnp.einsum(
-        "qgrd,kgd->grqk", query_rows, key_rows, preferred_element_type=jnp.float32
-    ) * HD ** (-0.5)
-    query_pos = offset + 0 + jnp.arange(ATT_BLOCK, dtype=jnp.int32)
-    key_pos = offset + 0 - WINDOW + jnp.arange(reach, dtype=jnp.int32)
-    allowed = (
-        (jnp.abs(query_pos[:, None] - key_pos[None, :]) <= WINDOW)
-        & (key_pos[None, :] >= 0)
-        & (key_pos[None, :] < length)
-    )
-    scores = jnp.where(allowed, scores, -jnp.inf)
-    top_score = jnp.maximum(jnp.max(scores, axis=-1, keepdims=True), sink_local)
-    raised = jnp.exp(scores - top_score)
-    denominator = jnp.exp(sink_local - top_score) + jnp.sum(raised, axis=-1, keepdims=True)
-    weights_bf = (raised / denominator).astype(jnp.bfloat16)
-    mixed = jnp.einsum("grqk,kgd->qgrd", weights_bf, value_rows, preferred_element_type=jnp.float32)
-    outputs = mixed.astype(jnp.bfloat16).reshape(ATT_BLOCK, query_count * HD)
+    angle_pos = offset - WINDOW + jnp.arange(tokens + 2 * WINDOW, dtype=jnp.int32)
+    inverse = ROPE_BASE ** (-jnp.arange(HD // 4, dtype=jnp.float32) / (HD // 4))
+    row_angles = (angle_pos // GRID_W).astype(F32)[:, None] * inverse[None, :]
+    col_angles = (angle_pos % GRID_W).astype(F32)[:, None] * inverse[None, :]
+    angles = jnp.concatenate([row_angles, row_angles, col_angles, col_angles] * 2, axis=1)
+    whole = [pl.BlockSpec(memory_space=pltpu.VMEM)] * 8 + [pl.BlockSpec(memory_space=pltpu.SMEM)]
+    places = lax.axis_size(SP)
+    lin_mix, outputs = pl.pallas_call(
+        exchange_kernel,
+        out_shape=[jax.ShapeDtypeStruct((tokens, head_width), BF)] * 2,
+        in_specs=whole,
+        out_specs=[pl.BlockSpec(memory_space=pltpu.VMEM)] * 2,
+        scratch_shapes=[
+            pltpu.VMEM((places, 48, PAIR), BF),
+            pltpu.VMEM((places, 16, PAIR), BF),
+            pltpu.VMEM((places, 16, PAIR), BF),
+            pltpu.VMEM((2, tokens, 2 * PAIR), BF),
+            pltpu.SemaphoreType.DMA((places,)),
+            pltpu.SemaphoreType.DMA((places,)),
+            pltpu.SemaphoreType.DMA((places,)),
+            pltpu.SemaphoreType.DMA((places,)),
+            pltpu.SemaphoreType.DMA((2,)),
+            pltpu.SemaphoreType.DMA((2,)),
+        ],
+        compiler_params=pltpu.CompilerParams(collective_id=0, has_side_effects=True),
+        name="exchange",
+        cost_estimate=pl.CostEstimate(flops=10**9, bytes_accessed=2**21, transcendentals=0),
+    )(
+        messages, initial_state, reads, local_out, head_norm_gain[None], returned,
+        jnp.cos(angles), jnp.sin(angles), query_sink_logit,
+    )
     lin_weight, att_weight = turned_gather(
         (linear_output_weight, window_output_weight), SP_FS, (1, 1)
     )

time: 218 us -> 216 us (level)
  Pallas kernels: 37.7 us -> 65.5 us
  starting transfers between devices: 31.3 us -> 7.44 us
  waiting for transfers between devices: 69.2 us -> 65.2 us
    pallas_call x2 -> x1, Pallas kernels: 12.2 us -> 40.2 us  [local(): pl.pallas_call(exchange_kernel, out_shape=[jax.ShapeDtypeStruct((tokens,...]
    all_gather x1, waiting for transfers between devices: 16.2 us -> 39.9 us  [turned_gather(): out, at, gathered = (lax.all_gather(both, axis, axis=0, tiled=True), 0, [])]
    all_to_all x2 -> x0, waiting for transfers between devices: 21.4 us -> none  [the longest x1 11.5 us: local(): lax.all_to_all(messages, SP, split_axis=0, concat_axis=0, tiled=True)]
    all_to_all x2 -> x0, starting transfers between devices: 19.4 us -> none  [the longest x1 11.5 us: local(): lax.all_to_all(messages, SP, split_axis=0, concat_axis=0, tiled=True)]
    all_to_all x1, waiting for transfers between devices: 6.88 us -> 1.32 us  [local(): lax.all_to_all(to_bf16(partial_cols), 'fs', split_axis=0, concat_axis=1,...]
    ppermute x2 -> x0, starting transfers between devices: 4.61 us -> none  [the longest x1 3.14 us: padded(): lax.ppermute(lax.slice_in_dim(block, block.shape[dim] - width, None, axis...]
    ppermute x2 -> x0, waiting for transfers between devices: 4.52 us -> none  [the longest x1 4.18 us: padded(): lax.ppermute(lax.slice_in_dim(block, 0, width, axis=dim), axis, backward)]
    all_to_all x1, waiting for transfers between devices: 20.1 us -> 23.9 us  [from_everyone(): return lax.all_to_all(copies, axis, split_axis=0, concat_axis=0, tiled=True)]
  transfers between devices with their start and end apart: 8 -> 4, of which waited for: 7 -> 3; matrix products, arithmetic and copies ran while one was open for 7% -> 7% of each run, Pallas kernels for 17% -> 31%
where the time goes in v2:
time: 216 us; the launch traced here: 215 us
  Pallas kernels  65.5 us (30%)
  waiting for transfers between devices  65.2 us (30%)
  blocking collectives  37.9 us (18%)
  local copies, waits for them, and re-layouts  14.2 us (7%)
  between operations  13.6 us (6%)
  matrix products  8.05 us (4%)
  starting transfers between devices  7.44 us (3%)
  other arithmetic  2.8 us (1%)
    pallas_call x1, Pallas kernels, local(): pl.pallas_call(exchange_kernel, out_shape=[jax.ShapeDtypeStruct((tokens,...  40.2 us
    all_gather x1, waiting for transfers between devices, turned_gather(): out, at, gathered = (lax.all_gather(both, axis, axis=0, tiled=True), 0, [])  39.9 us
    all_to_all x1, waiting for transfers between devices, from_everyone(): return lax.all_to_all(copies, axis, split_axis=0, concat_axis=0, tiled=True)  23.9 us
    pallas_call x1, Pallas kernels, local(): pl.pallas_call(local_kernel, out_shape=[jax.ShapeDtypeStruct((2, tokens,...  21.7 us
    all_gather x1, blocking collectives, whole_of(): out = lax.all_gather(out, axes[number], axis=dim, tiled=True)  10.6 us
    all_to_all x1, blocking collectives, local(): lax.all_to_all(joined, 'fs', split_axis=1, concat_axis=0, tiled=True)  9.37 us
    all_to_all x1, blocking collectives, from_everyone(): return lax.all_to_all(copies, axis, split_axis=0, concat_axis=0, tiled=True)  9.14 us
    all_to_all x1, blocking collectives, sum_at_owner(): lax.all_to_all(parts, axis, split_axis=0, concat_axis=0, tiled=True)  8.83 us
  transfers between devices with their start and end apart: 4, of which 3 were waited for; matrix products, arithmetic and copies ran while one was open for 7% of the time, Pallas kernels for 31%

profile of v2, /device:TPU:1, one launch (start us, length us, event | category | flops | bytes accessed | tf_op | source)
XLA Modules:
  0.0 214.7 jit_solution(10028410023785017645)
XLA Ops:
  6.5 0.7 constant_dynamic-update-slice_fusion.5
  7.3 0.7 constant_dynamic-update-slice_fusion.4
  8.0 0.7 constant_dynamic-update-slice_fusion.3
  8.7 0.7 constant_dynamic-update-slice_fusion.2
  9.4 0.7 constant_dynamic-update-slice_fusion.1
  10.1 0.7 constant_dynamic-update-slice_fusion
  11.0 9.4 %all_to_all.53 = bf16[16,4,576]{2,0,1:T(8,128)(2,1)S(1)} all-to-all(bf16[16,4,576]{2,0,1:T(8,128)(2,1)S(1)} %copy.36), channel_id=1, replica_groups=mesh['sp_0'=8,'sp_1'=4,'fs'=4,'tp'=2] {'fs'}, dimensions={1} | all-to-all | bytes 147456 | tf_op jit(solution)/shard_map/all_to_all | solution.py:523
  20.3 10.6 %all_gather.9 = bf16[256,576]{1,0:T(8,128)(2,1)} all-gather(bf16[64,576]{1,0:T(8,128)(2,1)S(1)} %bitcast.34), channel_id=1, replica_groups=mesh['sp_0'=8,'sp_1'=4,'fs'=4,'tp'=2] {'sp_1'}, dimensions={0}, use_global_device_ids=true | all-gather | bytes 368640 | tf_op jit(solution)/shard_map/all_gather | solution.py:432
  31.0 1.3 pad_maximum_fusion
  32.3 1.0 broadcast_in_dim.6
  33.4 9.1 %all_to_all.54 = bf16[2,1,128,1024]{3,2,1,0:T(8,128)(2,1)S(1)} all-to-all(bf16[2,1,128,1024]{3,2,1,0:T(8,128)(2,1)S(1)} %broadcast_in_dim.6), channel_id=1, replica_groups=mesh['sp_0'=8,'sp_1'=4,'fs'=4,'tp'=2] {'tp'}, dimensions={0} | all-to-all | bytes 1048576 | tf_op jit(solution)/shard_map/all_to_all | solution.py:422
  42.6 0.8 copy.35
  44.2 1.7 broadcast_in_dim.7
  45.9 3.7 %all-to-all-start.1 = ((bf16[4,128,2048]{2,1,0:T(8,128)(2,1)}), bf16[4,128,2048]{2,1,0:T(8,128)(2,1)S(1)}, u32[]{:S(2)}, u32[]{:S(2)}) async-start(bf16[4,128,2048]{2,1,0:T(8,128)(2,1)} %broadcast_in_dim.7), calls=%async_computation.1 | async-start | bytes 4194304 | tf_op jit(solution)/shard_map/all_to_all | solution.py:422
  49.6 1.0 copy.38.down_d_ref
  50.6 1.0 copy.39.down_e_ref
  51.7 23.9 %all-to-all-done.1 = bf16[4,128,2048]{2,1,0:T(8,128)(2,1)S(1)} async-done(((bf16[4,128,2048]{2,1,0:T(8,128)(2,1)}), bf16[4,128,2048]{2,1,0:T(8,128)(2,1)S(1)}, u32[]{:S(2)}, u32[]{:S(2)}) %all-to-all-start.1) | async-done | bytes 2097184 | tf_op jit(solution)/shard_map/all_to_all | solution.py:422
  75.6 3.2 %convolution_convert_fusion = bf16[512,576]{0,1:T(8,128)(2,1)S(1)} fusion(bf16[512,2048]{1,0:T(8,128)(2,1)S(1)} %bitcast.33, bf16[2048,576]{1,0:T(8,128)(2,1)} %all-gather.3.cloned.1.call-done), kind=kOutput, calls=%fused_computation.4 | convolution fusion | flops 1208254464 | bytes 5046272 | tf_op jit(solution)/shard_map/dot_general | solution.py:526
  78.8 0.9 copy_bitcast_fusion
  79.7 3.7 %all-to-all-start.3 = ((bf16[4,128,576]{1,2,0:T(8,128)(2,1)}), bf16[4,128,576]{1,2,0:T(8,128)(2,1)S(1)}, u32[]{:S(2)}, u32[]{:S(2)}) async-start(bf16[4,128,576]{1,2,0:T(8,128)(2,1)} %copy_bitcast_fusion), calls=%async_computation.3 | async-start | bytes 1179648 | tf_op jit(solution)/shard_map/all_to_all | solution.py:527
  83.5 0.4 concatenate.10
  84.0 3.7 %rates.1 = (f32[2,128,512]{2,1,0:T(8,128)}, f32[2,128,512]{2,1,0:T(8,128)}) custom-call(bf16[128,2048]{1,0:T(8,128)(2,1)} %copy-done, bf16[2048,96]{1,0:T(8,128)(2,1)} %copy.38.down_d_ref, bf16[2048,96]{1,0:T(8,128)(2,1)} %copy.39.down_e_ref, bf16[2,96,1024]{2,1,0:T(8,128)(2,1)} %up_d_ref.1, bf16[2,96,1024]{2,1,0:T(8,128)(2,1)} %up_e_ref.1, ...), custom_call_target="tpu_custom_call" | custom-call | flops 201326592 | bytes 2097152 | tf_op jit(solution)/shard_map/rates/pallas_call | solution.py:534
  87.7 1.5 fusion.9
  89.1 1.3 all-to-all-done.3
  90.4 1.1 copy.40.proj_ref
  91.5 21.7 %local_maps.1 = (f32[2,128,512]{2,1,0:T(8,128)}, f32[128,512]{1,0:T(8,128)}, bf16[32,48,128]{2,1,0:T(8,128)(2,1)}) custom-call(bf16[128,2304]{1,0:T(8,128)(2,1)} %copy.40.proj_ref, f32[2,128,512]{2,1,0:T(8,128)} %get-tuple-element.12.logd_ref, f32[2,128,512]{2,1,0:T(8,128)} %get-tuple-element.13.learn_ref), custom_call_target="tpu_custom_call" | custom-call | flops 1000000000 | bytes 2097152 | tf_op jit(solution)/shard_map/local_maps/pallas_call | solution.py:543
  113.2 40.2 %exchange.1 = (bf16[128,512]{1,0:T(8,128)(2,1)}, bf16[128,512]{1,0:T(8,128)(2,1)}) custom-call(bf16[32,48,128]{2,1,0:T(8,128)(2,1)} %get-tuple-element.14.msg_ref, f32[2,16,64,64]{3,2,1,0:T(8,128)} %init_ref.1, f32[2,128,512]{2,1,0:T(8,128)} %get-tuple-element.15.reads_ref, f32[128,512]{1,0:T(8,128)} %get-tuple-element.16.local_ref, f32[1,1024]{1,0:T(1,128)} %bitcast.38, ...), custom_call_target="tpu_custom_call" | custom-call | flops 1000000000 | bytes 2097152 | tf_op jit(solution)/shard_map/exchange/pallas_call | solution.py:560
  153.4 39.9 %all-gather.5.cloned.1.call-done = bf16[2048,1024]{1,0:T(8,128)(2,1)} async-done(((bf16[16,1024]{1,0:T(8,128)(2,1)}), bf16[2048,1024]{1,0:T(8,128)(2,1)}) %all-gather.5.cloned.1.call-update) | async-done | bytes 4194320 | tf_op jit(solution)/shard_map/all_gather | solution.py:439
  193.3 2.5 %fusion.1 = f32[128,2048]{1,0:T(8,128)S(1)} fusion(bf16[128,512]{1,0:T(8,128)(2,1)} %get-tuple-element.17, bf16[2048,1024]{1,0:T(8,128)(2,1)} %all-gather.5.cloned.1.call-done), kind=kOutput, calls=%fused_computation.2 | convolution fusion | flops 268435456 | bytes 3276800 | tf_op jit(solution)/shard_map/dot_general | solution.py:588
  195.8 2.4 %convolution_add_fusion = f32[128,2048]{1,0:T(8,128)S(1)} fusion(f32[128,2048]{1,0:T(8,128)S(1)} %fusion.1, bf16[128,512]{1,0:T(8,128)(2,1)S(1)} %copy-done.3, bf16[2048,1024]{1,0:T(8,128)(2,1)} %all-gather.5.cloned.1.call-done), kind=kOutput, calls=%fused_computation | convolution fusion | flops 268697600 | bytes 4325376 | tf_op jit(solution)/shard_map/dot_general | solution.py:589
  198.3 8.8 %all_to_all.55 = f32[2,64,2048]{2,1,0:T(8,128)S(1)} all-to-all(f32[2,64,2048]{2,1,0:T(8,128)S(1)} %bitcast.31), channel_id=1, replica_groups=mesh['sp_0'=8,'sp_1'=4,'fs'=4,'tp'=2] {'tp'}, dimensions={0} | all-to-all | bytes 2097152 | tf_op jit(solution)/shard_map/all_to_all | solution.py:455
  207.1 0.8 reduce_sum.19
  (25 shorter events, 1.2 us)
Async XLA Ops:
  6.5 69.1 %all-gather.3.cloned.1.call-start = ((), (), s32[]{:S(2)}) async-start(), calls=%async_computation.5 | async-start | bytes 2949120 | tf_op jit(solution)/shard_map/all_gather | solution.py:432
  30.9 162.4 %all-gather.5.cloned.1.call-start = ((), (), s32[]{:S(2)}) async-start(), calls=%async_computation.6 | async-start | bytes 4227072 | tf_op jit(solution)/shard_map/all_gather | solution.py:439
  42.6 1.4 copy-start.4
  44.2 1.7 copy-start
  45.9 3.8 %copy-start.1 = (bf16[2048,96]{0,1:T(8,128)(2,1)S(1)}, bf16[2048,96]{0,1:T(8,128)(2,1)}, u32[]{:S(2)}) copy-start(bf16[2048,96]{0,1:T(8,128)(2,1)} %param.28) | copy-start | bytes 1179652
  45.9 4.8 %copy-start.2 = (bf16[2048,96]{0,1:T(8,128)(2,1)S(1)}, bf16[2048,96]{0,1:T(8,128)(2,1)}, u32[]{:S(2)}) copy-start(bf16[2048,96]{0,1:T(8,128)(2,1)} %param.32) | copy-start | bytes 1179652
  45.9 29.8 %all-to-all-start.1 = ((bf16[4,128,2048]{2,1,0:T(8,128)(2,1)}), bf16[4,128,2048]{2,1,0:T(8,128)(2,1)S(1)}, u32[]{:S(2)}, u32[]{:S(2)}) async-start(bf16[4,128,2048]{2,1,0:T(8,128)(2,1)} %broadcast_in_dim.7), calls=%async_computation.1 | async-start | bytes 4194304 | tf_op jit(solution)/shard_map/all_to_all | solution.py:422
  79.7 10.7 %all-to-all-start.3 = ((bf16[4,128,576]{1,2,0:T(8,128)(2,1)}), bf16[4,128,576]{1,2,0:T(8,128)(2,1)S(1)}, u32[]{:S(2)}, u32[]{:S(2)}) async-start(bf16[4,128,576]{1,2,0:T(8,128)(2,1)} %copy_bitcast_fusion), calls=%async_computation.3 | async-start | bytes 1179648 | tf_op jit(solution)/shard_map/all_to_all | solution.py:527
  153.4 42.4 %copy-start.3 = (bf16[128,512]{1,0:T(8,128)(2,1)S(1)}, bf16[128,512]{1,0:T(8,128)(2,1)}, u32[]{:S(2)}) copy-start(bf16[128,512]{1,0:T(8,128)(2,1)} %get-tuple-element.18) | copy-start | bytes 393220
Sparse Core Ops, SparseCore 0:
  31.1 43.5 all-gather.2
  78.3 115.0 all-gather.4

commit v3 on v2

v3 whole, which is shorter than its diff:
```python
import functools
import jax
import jax.numpy as jnp
from jax import lax
from jax.experimental import pallas as pl
from jax.experimental.pallas import tpu as pltpu

from jax.sharding import Mesh
from jax.sharding import PartitionSpec as P

HD = 64
CH = 64
PAIR = 128
WINDOW = 128
GRID_W = 64
ATT_BLOCK = 128
SP = ("sp_0", "sp_1")
FOUR = 4
SP_FS = ("sp_0", "sp_1", "fs")
SP_TP = ("sp_0", "sp_1", "tp")
NORM_EPS = 1e-06
GROUP_EPS = 0.00064
ROPE_BASE = 10000.0
F32 = jnp.float32
BF = jnp.bfloat16
MESSAGE = jnp.bfloat16
MESH = pl.DeviceIdType.MESH
NN = (((1,), (0,)), ((), ()))
NT = (((1,), (1,)), ((), ()))
TN = (((0,), (0,)), ((), ()))


def dot(a, b, dims=NN):
    return lax.dot_general(a, b, dims, preferred_element_type=F32)


def split2(a):
    high = a.astype(BF)
    return high, (a - high.astype(F32)).astype(BF)


def split3(a):
    high, rest = a.astype(BF), None
    rest = a - high.astype(F32)
    mid = rest.astype(BF)
    return high, mid, (rest - mid.astype(F32)).astype(BF)


def mm3(a, b, dims=NN):
    (ka,), (kb,) = dims[0]
    a_hi, a_lo = split2(a)
    b_hi, b_lo = split2(b)
    main = dot(
        jnp.concatenate([a_hi, a_lo], axis=ka), jnp.concatenate([b_hi, b_hi], axis=kb), dims
    )
    return main + dot(a_hi, b_lo, dims)


def mm2(a, b_exact, dims=NN):
    (ka,), (kb,) = dims[0]
    a_hi, a_lo = split2(a)
    return dot(
        jnp.concatenate([a_hi, a_lo], axis=ka), jnp.concatenate([b_exact, b_exact], axis=kb), dims
    )


def iota(shape, dim):
    return lax.broadcasted_iota(jnp.int32, shape, dim)


def ones_where(cond):
    return jnp.where(cond, 1.0, 0.0).astype(BF)


def ring_of_four(buf, out_sem, in_sem):
    me = lax.axis_index("fs")
    right, left, far = (me + 1) % FOUR, (me + 3) % FOUR, (me + 2) % FOUR
    half = buf.shape[1] // 2

    def piece(block, part, target, number):
        where = buf.at[block, part * half : (part + 1) * half]
        return pltpu.make_async_remote_copy(
            src_ref=where, dst_ref=where, send_sem=out_sem.at[number], recv_sem=in_sem.at[number],
            device_id={"fs": target}, device_id_type=MESH,
        )

    def start():
        piece(me, 0, right, 0).start()
        piece(me, 1, left, 1).start()
        piece(me, 1, right, 2).start()
        piece(me, 0, left, 3).start()

    def relay():
        piece(left, 0, right, 0).wait_recv()
        piece(left, 0, right, 4).start()
        piece(right, 1, left, 1).wait_recv()
        piece(right, 1, left, 5).start()

    def arrive_near():
        piece(left, 1, right, 2).wait_recv()
        piece(right, 0, left, 3).wait_recv()

    def arrive_far():
        piece(far, 0, right, 4).wait_recv()
        piece(far, 1, left, 5).wait_recv()

    def finish_sends():
        piece(me, 0, right, 0).wait_send()
        piece(me, 1, left, 1).wait_send()
        piece(me, 1, right, 2).wait_send()
        piece(me, 0, left, 3).wait_send()
        piece(left, 0, right, 4).wait_send()
        piece(right, 1, left, 5).wait_send()

    return start, relay, arrive_near, arrive_far, finish_sends


def front_kernel(
    x_ref, gain_ref, wr_ref, wk_ref, wv_ref, wq_ref, wak_ref, wav_ref,
    down_d_ref, down_e_ref, up_d_ref, up_e_ref, off_d_ref, off_e_ref, extra_ref,
    proj_ref, logd_ref, learn_ref,
    both_ref, hid_ref, stage_ref, cols_ref, ext_ref,
    x_out, x_in, hid_out, hid_in, stage_out, stage_in, ext_out, ext_in,
    z_out, z_in, near_out, near_in, far_out, far_in,
):
    z, x, f, c = (lax.axis_index(a) for a in ("sp_0", "sp_1", "fs", "tp"))
    nz, nx = lax.axis_size("sp_0"), lax.axis_size("sp_1")
    mine = z * nx + x
    rows = wr_ref.shape[0]
    barrier = pltpu.get_barrier_semaphore()
    peers = [{"fs": (f + k) % FOUR} for k in range(1, FOUR)] + [{"tp": 1 - c}]
    peers += [{"sp_0": (z + k) % nz} for k in (1, nz - 1)] + [{"sp_1": (x + k) % nx} for k in (1, nx - 1)]
    for peer in peers:
        pl.semaphore_signal(barrier, inc=1, device_id=peer, device_id_type=MESH)
    low = iota((rows, PAIR), 1) < HD
    keys, values = wak_ref[...].astype(F32), wav_ref[...].astype(F32)
    shared = [
        jnp.where(low, keys, pltpu.roll(values, HD, 1)).astype(BF),
        jnp.where(low, pltpu.roll(keys, HD, 1), values).astype(BF),
    ]
    for g in range(FOUR):
        lanes = slice(g * PAIR, (g + 1) * PAIR)
        for k, ref in enumerate((wr_ref, wk_ref, wv_ref, wq_ref)):
            stage_ref[g, :, k * PAIR : (k + 1) * PAIR] = ref[:, lanes]
        stage_ref[g, :, 4 * PAIR :] = shared[g // 2]
    both_ref[c] = x_ref[...]
    ext_ref[f] = extra_ref[0]
    my_rows = pl.ds(pl.multiple_of(f * rows, rows), rows)
    cols_ref[mine, my_rows, :] = stage_ref[f]
    pl.semaphore_wait(barrier, len(peers))

    half_copy = pltpu.make_async_remote_copy(
        src_ref=x_ref, dst_ref=both_ref.at[c], send_sem=x_out, recv_sem=x_in,
        device_id={"tp": 1 - c}, device_id_type=MESH,
    )
    half_copy.start()

    def stage_copy(k):
        g = (f + k) % FOUR
        return pltpu.make_async_remote_copy(
            src_ref=stage_ref.at[g], dst_ref=cols_ref.at[mine, my_rows, :],
            send_sem=stage_out.at[k], recv_sem=stage_in.at[k], device_id={"fs": g}, device_id_type=MESH,
        )

    def stage_arrival(k):
        g = (f + FOUR - k) % FOUR
        return pltpu.make_async_remote_copy(
            src_ref=stage_ref.at[g], dst_ref=cols_ref.at[mine, pl.ds(pl.multiple_of(g * rows, rows), rows), :],
            send_sem=stage_out.at[k], recv_sem=stage_in.at[k], device_id={"fs": g}, device_id_type=MESH,
        )

    def ext_copy(k, source):
        return pltpu.make_async_remote_copy(
            src_ref=extra_ref.at[0], dst_ref=ext_ref.at[source],
            send_sem=ext_out.at[k], recv_sem=ext_in.at[k], device_id={"fs": (f + k) % FOUR}, device_id_type=MESH,
        )

    for k in range(1, FOUR):
        stage_copy(k).start()

    def z_block(k):
        if k == 0:
            return z
        step = (k - 1) // 2
        return (z + nz - 1 - step) % nz if k % 2 else (z + 1 + step) % nz

    def z_copy(k_from, side, step):
        where = cols_ref.at[z_block(k_from) * nx + x]
        return pltpu.make_async_remote_copy(
            src_ref=where, dst_ref=where, send_sem=z_out.at[side, step], recv_sem=z_in.at[side, step],
            device_id={"sp_0": (z + (1 if side == 0 else nz - 1)) % nz}, device_id_type=MESH,
        )

    def near_copy(k, side, column):
        where = cols_ref.at[z_block(k) * nx + column]
        return pltpu.make_async_remote_copy(
            src_ref=where, dst_ref=where, send_sem=near_out.at[k, side], recv_sem=near_in.at[k, side],
            device_id={"sp_1": (x + (1 if side == 0 else nx - 1)) % nx}, device_id_type=MESH,
        )

    def far_copy(k, column):
        where = cols_ref.at[z_block(k) * nx + column]
        return pltpu.make_async_remote_copy(
            src_ref=where, dst_ref=where, send_sem=far_out.at[k], recv_sem=far_in.at[k],
            device_id={"sp_1": (x + (1 if k % 2 == 0 else nx - 1)) % nx}, device_id_type=MESH,
        )

    left, right, across = (x + nx - 1) % nx, (x + 1) % nx, (x + 2) % nx

    def spread(k):
        near_copy(k, 0, x).start()
        near_copy(k, 1, x).start()

    def pass_on(k):
        near_copy(k, 0, left).wait_recv()
        near_copy(k, 1, right).wait_recv()
        far_copy(k, left if k % 2 == 0 else right).start()

    for k in range(1, FOUR):
        stage_arrival(k).wait_recv()
    z_copy(0, 0, 0).start()
    z_copy(0, 1, 0).start()
    spread(0)

    half_copy.wait_recv()
    full = jnp.concatenate([both_ref[0], both_ref[1]], axis=1).astype(F32)
    scale = lax.rsqrt(jnp.mean(full * full, axis=-1, keepdims=True) + NORM_EPS)
    hid_ref[f] = (full * scale * gain_ref[...]).astype(BF)
    start, relay, arrive_near, arrive_far, finish_sends = ring_of_four(hid_ref, hid_out, hid_in)
    for k in range(1, FOUR):
        ext_copy(k, f).start()
    start()

    steps = nz // 2
    for step in range(steps):
        k = 2 * step + 1
        z_copy(k, 0, step).wait_recv()
        if step < steps - 1:
            z_copy(k, 0, step + 1).start()
        spread(k)
        if step < steps - 1:
            z_copy(k + 1, 1, step).wait_recv()
            if step < steps - 2:
                z_copy(k + 1, 1, step + 1).start()
            spread(k + 1)
        if step == 0:
            pass_on(0)
        else:
            pass_on(k - 2)
            pass_on(k - 1)
        if step == 1:
            relay()
    pass_on(nz - 1)
    arrive_near()
    arrive_far()
    for k in range(1, FOUR):
        ext_copy(k, (f + FOUR - k) % FOUR).wait_recv()

    tokens = hid_ref.shape[1]
    hidden = hid_ref[...].reshape(FOUR * tokens, hid_ref.shape[2])
    decay_low = dot(hidden, down_d_ref[...]).astype(BF)
    learn_low = dot(hidden, down_e_ref[...]).astype(BF)
    decay_act = jnp.tanh(decay_low.astype(F32)).astype(BF)
    heads = extra_ref.shape[1]
    first = c * heads * HD + f * PAIR
    chosen = pl.ds(pl.multiple_of(first, PAIR), PAIR)
    select = ones_where(iota((heads, PAIR), 0) == 2 * f + iota((heads, PAIR), 1) // HD).astype(F32)
    spikes = [
        lax.dot_general(
            ext_ref[p], select, TN, precision=lax.Precision.HIGHEST, preferred_element_type=F32
        )
        for p in range(FOUR)
    ]
    for d in range(2):
        pre = off_d_ref[d : d + 1, chosen] + dot(decay_act, up_d_ref[d, :, chosen])
        softplus = jnp.maximum(-pre, 0.0) + jnp.log1p(jnp.exp(-jnp.abs(pre)))
        rate = jnp.exp(-softplus - 0.5)
        learn = jax.nn.sigmoid(off_e_ref[d : d + 1, chosen] + dot(learn_low, up_e_ref[d, :, chosen]))
        for p in range(FOUR):
            part = slice(p * tokens, (p + 1) * tokens)
            logd_ref[d, p] = spikes[p] - rate[part]
            learn_ref[d, p] = learn[part]

    for k in range(nz):
        far_copy(k, across).wait_recv()
    depth = cols_ref.shape[0] * cols_ref.shape[1]
    for first_col, last_col in ((0, 256), (256, 512), (512, 640)):
        weight = cols_ref[:, :, first_col:last_col].reshape(depth, last_col - first_col)
        result = dot(hidden, weight).astype(BF)
        for p in range(FOUR):
            proj_ref[p, :, first_col:last_col] = result[p * tokens : (p + 1) * tokens]

    half_copy.wait_send()
    finish_sends()
    for k in range(1, FOUR):
        stage_copy(k).wait_send()
        ext_copy(k, f).wait_send()
    for step in range(steps):
        z_copy(0, 0, step).wait_send()
        if step < steps - 1:
            z_copy(0, 1, step).wait_send()
    for k in range(nz):
        near_copy(k, 0, x).wait_send()
        near_copy(k, 1, x).wait_send()
        far_copy(k, left).wait_send()


def stacked(x):
    low = iota(x.shape, 1) < HD
    return jnp.concatenate([jnp.where(low, x, 0.0), jnp.where(low, 0.0, x)], axis=0)


def unstacked(x):
    return x[:CH] + x[CH:]


def local_kernel(
    proj_ref, logd_ref, learn_ref, wout_ref, q_ref, o_ref, msg_ref, rows_ref,
    z_out, z_in, x_out, x_in,
):
    z, x = lax.axis_index("sp_0"), lax.axis_index("sp_1")
    nz, nx = lax.axis_size("sp_0"), lax.axis_size("sp_1")
    barrier = pltpu.get_barrier_semaphore()
    peers = [{"sp_0": (z + k) % nz} for k in range(1, nz)] + [{"sp_1": (x + k) % nx} for k in range(1, nx)]
    for peer in peers:
        pl.semaphore_signal(barrier, inc=1, device_id=peer, device_id_type=MESH)
    rows_ref[z, x] = wout_ref[...]
    pl.semaphore_wait(barrier, len(peers))

    def z_copy(k, source):
        return pltpu.make_async_remote_copy(
            src_ref=wout_ref, dst_ref=rows_ref.at[source, x], send_sem=z_out.at[k], recv_sem=z_in.at[k],
            device_id={"sp_0": (z + k) % nz}, device_id_type=MESH,
        )

    def x_copy(k, column):
        where = rows_ref.at[:, column]
        return pltpu.make_async_remote_copy(
            src_ref=where, dst_ref=where, send_sem=x_out.at[k], recv_sem=x_in.at[k],
            device_id={"sp_1": (x + k) % nx}, device_id_type=MESH,
        )

    for k in range(1, nz):
        z_copy(k, z).start()
    row = iota((2 * CH, 2 * CH), 0)
    col = iota((2 * CH, 2 * CH), 1)
    t, s = row % CH, col % CH
    eye = row == col
    same_head = ones_where(row // HD == col // HD)
    tri = [ones_where((iota((CH, CH), 0) >= iota((CH, CH), 1))), ones_where((iota((CH, CH), 0) <= iota((CH, CH), 1)))]
    strict = [t > s, t < s]
    within = [t >= s, t <= s]

    def one_pair(p, carry):
        @pl.when(p == FOUR // 2)
        def _():
            for k in range(1, nz):
                z_copy(k, (z + nz - k) % nz).wait_recv()
            for k in range(1, nx):
                x_copy(k, x).start()

        recept = proj_ref[p, :, :PAIR].astype(F32)
        keys = proj_ref[p, :, PAIR : 2 * PAIR].astype(F32)
        values = proj_ref[p, :, 2 * PAIR : 3 * PAIR].astype(F32)
        squares = mm2(keys * keys, same_head)
        unit = keys * lax.rsqrt(squares + NORM_EPS)
        jobs = [(d, c) for d in range(2) for c in range(2)]
        stage = {}
        for d, c in jobs:
            rows = slice(c * CH, (c + 1) * CH)
            logd = logd_ref[d, p, rows, :]
            parts = jnp.concatenate(split3(logd), axis=0)
            total = dot(jnp.concatenate([tri[d]] * 3, axis=1), parts)
            middle = total[CH // 2 - 1 : CH // 2] if d == 0 else total[CH // 2 : CH // 2 + 1]
            last = total[CH - 1 : CH] if d == 0 else total[0:1]
            grow = jnp.exp(total - middle)
            shrink = jnp.exp(middle - total)
            read = recept[rows] * grow
            mark = unit[rows] * jnp.exp(total - logd - middle)
            erase = unit[rows] * learn_ref[d, p, rows, :] * shrink
            key = keys[rows] * shrink
            read_s, mark_s, erase_s, key_s = map(stacked, (read, mark, erase, key))
            scores = mm3(
                jnp.concatenate([mark_s, read_s], axis=0),
                jnp.concatenate([erase_s, key_s], axis=0),
                NT,
            )
            stage[d, c] = (read, mark_s, erase_s, key_s, scores, jnp.exp(middle), jnp.exp(last - middle), jnp.exp(last))
        inverse = {}
        grams = {}
        for d, c in jobs:
            gram = jnp.where(strict[d], stage[d, c][4][: 2 * CH, : 2 * CH], 0.0)
            grams[d, c] = gram
            inverse[d, c] = jnp.where(eye, 1.0, 0.0) - jnp.where(t // 2 == s // 2, gram, 0.0)
        block = 2
        while block < CH:
            joins = (t // (2 * block) == s // (2 * block)) & (t // block != s // block)
            for job in jobs:
                found = inverse[job]
                inverse[job] = found - mm3(found, mm3(jnp.where(joins, grams[job], 0.0), found))
            block *= 2
        maps, reads, outs = {}, {}, {}
        for d, c in jobs:
            rows = slice(c * CH, (c + 1) * CH)
            read, mark_s, erase_s, key_s, scores, to_start, to_end, whole = stage[d, c]
            val_s = stacked(values[rows]).astype(BF)
            cross = jnp.where(strict[d], scores[: 2 * CH, 2 * CH :], 0.0)
            read_e = jnp.where(within[d], scores[2 * CH :, : 2 * CH], 0.0)
            read_k = jnp.where(within[d], scores[2 * CH :, 2 * CH :], 0.0)
            solved = mm3(inverse[d, c], jnp.concatenate([mark_s, mm2(cross, val_s)], axis=1))
            solved = jnp.concatenate([solved[:, :PAIR] * to_start, solved[:, PAIR:]], axis=1)
            taken = mm3(read_e, solved)
            reads[d, c] = read * to_start - unstacked(taken[:, :PAIR])
            outs[d, c] = unstacked(mm2(read_k, val_s) - taken[:, PAIR:])
            ended = mm3(solved, erase_s * to_end, TN)
            k_hi, k_lo = split2(key_s * to_end)
            added = dot(jnp.concatenate([val_s, val_s], axis=0), jnp.concatenate([k_hi, k_lo], axis=0), TN)
            prod = jnp.where(eye, whole - 1.0, 0.0) - ended[:PAIR]
            maps[d, c] = (prod, added - ended[PAIR:])
        out_rows = [outs[0, 0] + outs[1, 0], outs[0, 1] + outs[1, 1]]
        for d in range(2):
            first, second = (0, 1) if d == 0 else (1, 0)
            (prod1, add1), (prod2, add2) = maps[d, first], maps[d, second]
            both = jnp.concatenate([prod1, add1], axis=0)
            through = mm3(reads[d, second], both, NT)
            q_ref[d, p, first * CH : (first + 1) * CH, :] = reads[d, first]
            q_ref[d, p, second * CH : (second + 1) * CH, :] = reads[d, second] + through[:, :PAIR]
            out_rows[second] = out_rows[second] + through[:, PAIR:]
            joined = mm3(both, prod2)
            prod = prod1 + prod2 + joined[:PAIR]
            add = add1 + joined[PAIR:] + add2
            for hh in range(2):
                for half in range(2):
                    message = jnp.concatenate(
                        [
                            folded(prod, hh, hh * HD, HD // 2),
                            folded(add, hh, hh * HD + half * (HD // 2), HD // 4),
                        ],
                        axis=0,
                    )
                    msg_ref[d * 16 + p * 4 + hh * 2 + half] = message.astype(msg_ref.dtype)
        for c in range(2):
            o_ref[p, c * CH : (c + 1) * CH, :] = out_rows[c]
        return carry

    lax.fori_loop(0, FOUR, one_pair, 0)
    for k in range(1, nx):
        x_copy(k, (x + nx - k) % nx).wait_recv()
    for k in range(1, nz):
        z_copy(k, z).wait_send()
    for k in range(1, nx):
        x_copy(k, x).wait_send()


def folded(x, hh, first, count):
    upper, lower = x[first : first + count], x[first + count : first + 2 * count]
    if hh == 0:
        return upper + pltpu.roll(lower, HD, 1)
    return pltpu.roll(upper, HD, 1) + lower


def peer_id(index):
    inner = lax.axis_size("sp_1")
    return {"sp_0": index // inner, "sp_1": index % inner}


def exchange_kernel(
    msg_ref, init_ref, reads_ref, local_ref, gain_ref, proj_ref, cos_ref, sin_ref, sink_ref,
    mix_ref,
    recv_ref, sent_ref, enter_ref, halo_ref,
    out_sem, in_sem, back_out_sem, back_in_sem, halo_out_sem, halo_in_sem,
):
    count = recv_ref.shape[0]
    place = lax.axis_index("sp_0") * lax.axis_size("sp_1") + lax.axis_index("sp_1")
    kv_first = 4 * PAIR
    barrier = pltpu.get_barrier_semaphore()

    def greet(k, carry):
        pl.semaphore_signal(barrier, inc=1, device_id=peer_id((place + k) % count), device_id_type=MESH)
        return carry

    lax.fori_loop(1, count, greet, 0)
    pl.semaphore_wait(barrier, count - 1)

    def halo_copy(side):
        target = (place + count - 1 + 2 * side) % count
        return pltpu.make_async_remote_copy(
            src_ref=proj_ref.at[:, :, kv_first : kv_first + PAIR],
            dst_ref=halo_ref.at[1 - side],
            send_sem=halo_out_sem.at[side],
            recv_sem=halo_in_sem.at[1 - side],
            device_id=peer_id(target),
            device_id_type=MESH,
        )

    def map_copy(target):
        return pltpu.make_async_remote_copy(
            src_ref=msg_ref.at[target],
            dst_ref=recv_ref.at[place],
            send_sem=out_sem.at[target],
            recv_sem=in_sem.at[place],
            device_id=peer_id(target),
            device_id_type=MESH,
        )

    def map_arrival(source):
        return pltpu.make_async_remote_copy(
            src_ref=msg_ref.at[source],
            dst_ref=recv_ref.at[source],
            send_sem=out_sem.at[source],
            recv_sem=in_sem.at[source],
            device_id=peer_id(source),
            device_id_type=MESH,
        )

    def entry_copy(target):
        return pltpu.make_async_remote_copy(
            src_ref=sent_ref.at[target],
            dst_ref=enter_ref.at[place],
            send_sem=back_out_sem.at[target],
            recv_sem=back_in_sem.at[place],
            device_id=peer_id(target),
            device_id_type=MESH,
        )

    def entry_arrival(source):
        return pltpu.make_async_remote_copy(
            src_ref=sent_ref.at[source],
            dst_ref=enter_ref.at[source],
            send_sem=back_out_sem.at[source],
            recv_sem=back_in_sem.at[source],
            device_id=peer_id(source),
            device_id_type=MESH,
        )

    halo_copy(0).start()
    halo_copy(1).start()

    def send_map(k, carry):
        map_copy((place + k) % count).start()
        return carry

    lax.fori_loop(1, count, send_map, 0)
    recv_ref[place] = msg_ref[place]

    tokens = local_ref.shape[1]
    for side in range(2):
        halo_copy(side).wait()
    lane = iota((1, PAIR), 1)
    low = lane < HD
    front = lane % 32 < 16

    def turned(v, first, last):
        other = jnp.where(front, -pltpu.roll(v, PAIR - 16, 1), pltpu.roll(v, 16, 1))
        return v * cos_ref[first:last, :] + other * sin_ref[first:last, :]

    reach = 3 * tokens
    q_pos = place * tokens + iota((2 * tokens, reach), 0) % tokens
    k_pos = (place - 1) * tokens + iota((2 * tokens, reach), 1)
    allowed = (jnp.abs(q_pos - k_pos) <= WINDOW) & (k_pos >= 0) & (k_pos < count * tokens)
    upper = iota((2 * tokens, 1), 0) < tokens
    pair = lax.axis_index("fs")
    first_head = lax.axis_index("tp") * (2 * FOUR) + 2 * pair
    sink = jnp.where(upper, sink_ref[first_head], sink_ref[first_head + 1])

    def attend(p, carry):
        kv = jnp.concatenate(
            [halo_ref[0, p], proj_ref[p, :, kv_first : kv_first + PAIR], halo_ref[1, p]], axis=0
        ).astype(F32)
        roped = turned(kv, 0, reach)
        swapped = pltpu.roll(kv, HD, 1)
        key = jnp.where(low, roped, pltpu.roll(roped, HD, 1)).astype(BF)
        value = jnp.where(low, swapped, kv).astype(BF)
        query = turned(proj_ref[p, :, kv_first - PAIR : kv_first].astype(F32), tokens, 2 * tokens)
        query = jnp.concatenate([jnp.where(low, query, 0.0), jnp.where(low, 0.0, query)], axis=0)
        scores = dot(query.astype(BF), key, NT) * HD**-0.5
        scores = jnp.where(allowed, scores, -jnp.inf)
        top = jnp.maximum(jnp.max(scores, axis=-1, keepdims=True), sink)
        raised = jnp.exp(scores - top)
        total = jnp.exp(sink - top) + jnp.sum(raised, axis=-1, keepdims=True)
        mixed = dot((raised / total).astype(BF), value)
        mix_ref[p, :, PAIR:] = jnp.where(low, mixed[:tokens], mixed[tokens:]).astype(BF)
        return carry

    lax.fori_loop(0, FOUR, attend, 0)

    def await_map(k, carry):
        map_arrival((place + k) % count).wait()
        return carry

    lax.fori_loop(1, count, await_map, 0)

    unit_idx = place // 2
    direction, half = unit_idx // 8, place % 2
    rows = HD // 2
    quarter = rows // 2
    start = pl.multiple_of(half * rows, rows)

    def unfolded(x):
        return jnp.concatenate([x[:, :HD], x[:, HD:]], axis=0)

    def nth(step):
        return direction * (count - 1) + step * (1 - 2 * direction)

    def advance(step, state):
        idx = nth(step)
        sent_ref[idx] = jnp.concatenate([state[:quarter], state[quarter:]], axis=1).astype(BF)
        before = nth(step - 1)

        @pl.when((step > 0) & (before != place))
        def _():
            entry_copy(before).start()

        message = recv_ref[idx].astype(F32)
        return state + mm3(state, unfolded(message[:rows])) + unfolded(message[rows:])

    state = init_ref[direction, first_head + unit_idx % 2, pl.ds(start, rows), :]
    lax.fori_loop(0, count, advance, state)
    final = nth(count - 1)
    enter_ref[place] = sent_ref[place]

    @pl.when(final != place)
    def _():
        entry_copy(final).start()

    def await_entry(k, carry):
        entry_arrival((place + k) % count).wait()
        return carry

    lax.fori_loop(1, count, await_entry, 0)
    finish(reads_ref, local_ref, enter_ref, gain_ref, mix_ref)


def finish(q_ref, o_ref, enter_ref, gain_ref, mix_ref):
    row = iota((PAIR, PAIR), 0)
    col = iota((PAIR, PAIR), 1)
    same_head = ones_where(row // HD == col // HD)
    low = iota((HD // 4, PAIR), 1) < HD
    start = (lax.axis_index("tp") * FOUR + lax.axis_index("fs")) * PAIR
    gain = gain_ref[:, pl.ds(pl.multiple_of(start, PAIR), PAIR)]
    for p in range(FOUR):
        out = o_ref[p]
        for d in range(2):
            pieces = []
            for hh in range(2):
                for half in range(2):
                    m = enter_ref[d * 16 + p * 4 + hh * 2 + half].astype(F32)
                    turned = pltpu.roll(m, HD, 1)
                    if hh == 0:
                        pieces += [jnp.where(low, m, 0.0), jnp.where(low, turned, 0.0)]
                    else:
                        pieces += [jnp.where(low, 0.0, turned), jnp.where(low, 0.0, m)]
            out = out + mm2(q_ref[d, p], jnp.concatenate(pieces, axis=0).astype(BF), NT)
        centred = out - mm2(out, same_head) * (1.0 / HD)
        spread = mm2(centred * centred, same_head) * (1.0 / HD)
        mix_ref[p, :, :PAIR] = (centred * lax.rsqrt(spread + GROUP_EPS) * gain).astype(BF)


def out_kernel(
    mix_ref, rows_ref, out_ref, all_ref, total_ref, other_ref, ready_ref, got_ref,
    mix_out, mix_in, half_out, half_in, back_out, back_in,
):
    f, c = lax.axis_index("fs"), lax.axis_index("tp")
    tokens = mix_ref.shape[1]
    barrier = pltpu.get_barrier_semaphore()
    peers = [{"fs": (f + k) % FOUR} for k in range(1, FOUR)] + [{"tp": 1 - c}]
    for peer in peers:
        pl.semaphore_signal(barrier, inc=1, device_id=peer, device_id_type=MESH)
    all_ref[f] = mix_ref[...]
    pl.semaphore_wait(barrier, len(peers))
    start, relay, arrive_near, arrive_far, finish_sends = ring_of_four(all_ref, mix_out, mix_in)
    start()
    columns = total_ref.shape[2]
    weight_rows = rows_ref.shape[0] * rows_ref.shape[1] * rows_ref.shape[2]

    def product(g):
        weight = rows_ref[:, :, :, pl.ds(pl.multiple_of(g * 2 * PAIR, 2 * PAIR), 2 * PAIR)]
        left = all_ref[g].reshape(FOUR * tokens, 2 * PAIR)
        return dot(left, weight.reshape(weight_rows, 2 * PAIR), NT).reshape(FOUR, tokens, columns)

    total_ref[...] = product(f)
    relay()
    arrive_near()
    total_ref[...] += product((f + 1) % FOUR) + product((f + 3) % FOUR)
    arrive_far()
    total_ref[...] += product((f + 2) % FOUR)
    half = tokens // 2
    theirs = pl.ds(pl.multiple_of((1 - c) * half, half), half)
    ours = pl.ds(pl.multiple_of(c * half, half), half)
    half_copy = pltpu.make_async_remote_copy(
        src_ref=total_ref.at[:, theirs, :], dst_ref=other_ref, send_sem=half_out, recv_sem=half_in,
        device_id={"tp": 1 - c}, device_id_type=MESH,
    )
    half_copy.start()
    half_copy.wait_recv()
    ready_ref[...] = (total_ref[:, ours, :] + other_ref[...]).astype(BF)

    def back_copy(k, source):
        g = (f + k) % FOUR
        return pltpu.make_async_remote_copy(
            src_ref=ready_ref.at[g], dst_ref=got_ref.at[source], send_sem=back_out.at[k], recv_sem=back_in.at[k],
            device_id={"fs": g}, device_id_type=MESH,
        )

    for k in range(1, FOUR):
        back_copy(k, f).start()
    got_ref[f] = ready_ref[f]
    finish_sends()
    half_copy.wait_send()
    wide = FOUR * PAIR
    source, target = iota((wide, wide), 0), iota((wide, wide), 1)
    place = source % PAIR // 16 * (FOUR * 16) + source // PAIR * 16 + source % 16
    shuffle = ones_where(place == target)
    for k in range(1, FOUR):
        back_copy(k, (f + FOUR - k) % FOUR).wait_recv()
    for b in range(columns // PAIR):
        lanes = slice(b * PAIR, (b + 1) * PAIR)
        joined = jnp.concatenate([got_ref[g, :, lanes] for g in range(FOUR)], axis=1)
        out_ref[:, b * wide : (b + 1) * wide] = dot(joined, shuffle).astype(BF)
    for k in range(1, FOUR):
        back_copy(k, f).wait_send()


def local(
    inputs, input_norm_gain, receptance_weight, linear_key_weight, linear_value_weight,
    window_query_weight, window_key_weight, window_value_weight, decay_down_weight, decay_up_weight,
    decay_offset, decay_log_extra, erasure_down_weight, erasure_up_weight, erasure_offset,
    initial_state, head_norm_gain, query_sink_logit, linear_output_weight, window_output_weight,
):
    tokens, model = inputs.shape[1], 2 * inputs.shape[2]
    places = lax.axis_size(SP)
    nz, nx = lax.axis_size("sp_0"), lax.axis_size("sp_1")
    offset = lax.axis_index(SP) * tokens
    rows = receptance_weight.shape[0]
    out_rows = linear_output_weight.shape[1]
    vmem = pl.BlockSpec(memory_space=pltpu.VMEM)
    dma = pltpu.SemaphoreType.DMA

    def params(number):
        return pltpu.CompilerParams(
            collective_id=number, has_side_effects=True, vmem_limit_bytes=48 * 2**20
        )

    proj, logd, learn = pl.pallas_call(
        front_kernel,
        out_shape=[
            jax.ShapeDtypeStruct((FOUR, tokens, 5 * PAIR), BF),
            jax.ShapeDtypeStruct((2, FOUR, tokens, PAIR), F32),
            jax.ShapeDtypeStruct((2, FOUR, tokens, PAIR), F32),
        ],
        in_specs=[vmem] * 15,
        out_specs=[vmem] * 3,
        scratch_shapes=[
            pltpu.VMEM((2, tokens, model // 2), BF),
            pltpu.VMEM((FOUR, tokens, model), BF),
            pltpu.VMEM((FOUR, rows, 5 * PAIR), BF),
            pltpu.VMEM((places, FOUR * rows, 5 * PAIR), BF),
            pltpu.VMEM((FOUR, *decay_log_extra.shape[1:]), F32),
            dma, dma, dma((6,)), dma((6,)), dma((FOUR,)), dma((FOUR,)), dma((FOUR,)), dma((FOUR,)),
            dma((2, nz // 2)), dma((2, nz // 2)), dma((nz, 2)), dma((nz, 2)), dma((nz,)), dma((nz,)),
        ],
        compiler_params=params(1),
        name="front",
        cost_estimate=pl.CostEstimate(flops=10**9, bytes_accessed=2**21, transcendentals=0),
    )(
        inputs[0], input_norm_gain[None], receptance_weight, linear_key_weight, linear_value_weight,
        window_query_weight, window_key_weight, window_value_weight, decay_down_weight,
        erasure_down_weight, decay_up_weight, erasure_up_weight, decay_offset, erasure_offset,
        decay_log_extra,
    )
    both = jnp.stack([linear_output_weight, window_output_weight])
    both = both.reshape(2, FOUR, PAIR, out_rows)
    out_weight = jnp.transpose(both, (3, 1, 0, 2)).reshape(out_rows, 2 * FOUR * PAIR)
    reads, local_out, messages, weight_rows = pl.pallas_call(
        local_kernel,
        out_shape=[
            jax.ShapeDtypeStruct((2, FOUR, tokens, PAIR), F32),
            jax.ShapeDtypeStruct((FOUR, tokens, PAIR), F32),
            jax.ShapeDtypeStruct((places, 48, PAIR), BF),
            jax.ShapeDtypeStruct((nz, nx, *out_weight.shape), BF),
        ],
        in_specs=[vmem] * 4,
        out_specs=[vmem] * 4,
        scratch_shapes=[dma((nz,)), dma((nz,)), dma((nx,)), dma((nx,))],
        compiler_params=params(2),
        name="local_maps",
        cost_estimate=pl.CostEstimate(flops=10**9, bytes_accessed=2**21, transcendentals=0),
    )(proj, logd, learn, out_weight)
    angle_pos = offset - WINDOW + jnp.arange(tokens + 2 * WINDOW, dtype=jnp.int32)
    inverse = ROPE_BASE ** (-jnp.arange(HD // 4, dtype=jnp.float32) / (HD // 4))
    row_angles = (angle_pos // GRID_W).astype(F32)[:, None] * inverse[None, :]
    col_angles = (angle_pos % GRID_W).astype(F32)[:, None] * inverse[None, :]
    angles = jnp.concatenate([row_angles, row_angles, col_angles, col_angles] * 2, axis=1)
    mix = pl.pallas_call(
        exchange_kernel,
        out_shape=jax.ShapeDtypeStruct((FOUR, tokens, 2 * PAIR), BF),
        in_specs=[vmem] * 8 + [pl.BlockSpec(memory_space=pltpu.SMEM)],
        out_specs=vmem,
        scratch_shapes=[
            pltpu.VMEM((places, 48, PAIR), BF),
            pltpu.VMEM((places, 16, PAIR), BF),
            pltpu.VMEM((places, 16, PAIR), BF),
            pltpu.VMEM((2, FOUR, tokens, PAIR), BF),
            dma((places,)), dma((places,)), dma((places,)), dma((places,)), dma((2,)), dma((2,)),
        ],
        compiler_params=params(3),
        name="exchange",
        cost_estimate=pl.CostEstimate(flops=10**9, bytes_accessed=2**21, transcendentals=0),
    )(
        messages, initial_state, reads, local_out, head_norm_gain[None], proj,
        jnp.cos(angles), jnp.sin(angles), query_sink_logit,
    )
    columns = places * out_rows
    out = pl.pallas_call(
        out_kernel,
        out_shape=jax.ShapeDtypeStruct((tokens // 2, FOUR * columns), BF),
        in_specs=[vmem] * 2,
        out_specs=vmem,
        scratch_shapes=[
            pltpu.VMEM((FOUR, FOUR, tokens, 2 * PAIR), BF),
            pltpu.VMEM((FOUR, tokens, columns), F32),
            pltpu.VMEM((FOUR, tokens // 2, columns), F32),
            pltpu.VMEM((FOUR, tokens // 2, columns), BF),
            pltpu.VMEM((FOUR, tokens // 2, columns), BF),
            dma((6,)), dma((6,)), dma, dma, dma((FOUR,)), dma((FOUR,)),
        ],
        compiler_params=params(4),
        name="project_out",
        cost_estimate=pl.CostEstimate(flops=10**9, bytes_accessed=2**21, transcendentals=0),
    )(mix, weight_rows)
    return out[None]


def solution(mesh):
    finer = Mesh(
        mesh.devices.reshape(8, 4, mesh.shape["fs"], mesh.shape["tp"]), ("sp_0", "sp_1", "fs", "tp")
    )
    placed = (
        P("fs", SP, "tp"),
        P(),
        P(SP_FS, "tp"),
        P(SP_FS, "tp"),
        P(SP_FS, "tp"),
        P(SP_FS, "tp"),
        P(SP_FS, "tp"),
        P(SP_FS, "tp"),
        P(),
        P(),
        P(),
        P("fs", "tp", SP),
        P(),
        P(),
        P(),
        P(),
        P(),
        P(),
        P("tp", SP_FS),
        P("tp", SP_FS),
    )
    return jax.shard_map(
        local, mesh=finer, in_specs=placed, out_specs=P("fs", SP_TP, None), check_vma=False
    )
```

time: 216 us -> 132 us (0.61)
  waiting for transfers between devices: 65.2 us -> 0 us
  Pallas kernels: 65.5 us -> 121 us
  blocking collectives: 37.9 us -> 0 us
  between operations: 13.6 us -> 0.32 us
  matrix products: 8.05 us -> 0 us
  starting transfers between devices: 7.44 us -> 0 us
  local copies, waits for them, and re-layouts: 14.2 us -> 10.3 us
  other arithmetic: 2.8 us -> 0.27 us
    pallas_call x3 -> x4, Pallas kernels: 65.5 us -> 121 us  [the longest x1 39 us: local(): pl.pallas_call(front_kernel, out_shape=[jax.ShapeDtypeStruct((FOUR, token...]
    all_gather x2 -> x0, waiting for transfers between devices: 39.9 us -> none  [the longest x1 39.9 us: turned_gather(): out, at, gathered = (lax.all_gather(both, axis, axis=0, tiled=True), 0, [])]
    all_to_all x3 -> x0, blocking collectives: 27.3 us -> none  [the longest x1 9.37 us: local(): lax.all_to_all(joined, 'fs', split_axis=1, concat_axis=0, tiled=True)]
    all_to_all x2 -> x0, waiting for transfers between devices: 25.3 us -> none  [the longest x1 23.9 us: from_everyone(): return lax.all_to_all(copies, axis, split_axis=0, concat_axis=0, tiled=True)]
    all_gather x1 -> x0, blocking collectives: 10.6 us -> none  [whole_of(): out = lax.all_gather(out, axes[number], axis=dim, tiled=True)]
    dot_general x3 -> x0, matrix products: 8.05 us -> none  [the longest x1 3.16 us: local(): jnp.dot(every_seq, whole_cols, preferred_element_type=jnp.float32)]
    all_to_all x2 -> x0, starting transfers between devices: 7.39 us -> none  [the longest x1 3.74 us: from_everyone(): return lax.all_to_all(copies, axis, split_axis=0, concat_axis=0, tiled=True)]
    unnamed x18 -> x53, local copies, waits for them, and re-layouts: 5.96 us -> 9.13 us
  transfers between devices with their start and end apart: 4 -> 0, of which waited for: 3 -> 0; matrix products, arithmetic and copies ran while one was open for 7% -> 0% of each run, Pallas kernels for 31% -> 0%
where the time goes in v3:
time: 132 us
  Pallas kernels  121 us (92%)
  local copies, waits for them, and re-layouts  10.3 us (8%)
    pallas_call x1, Pallas kernels, local(): pl.pallas_call(front_kernel, out_shape=[jax.ShapeDtypeStruct((FOUR, token...  39 us
    pallas_call x1, Pallas kernels, local(): pl.pallas_call(exchange_kernel, out_shape=jax.ShapeDtypeStruct((FOUR, tok...  33.3 us
    pallas_call x1, Pallas kernels, local(): pl.pallas_call(out_kernel, out_shape=jax.ShapeDtypeStruct((tokens // 2, F...  25.4 us
    pallas_call x1, Pallas kernels, local(): pl.pallas_call(local_kernel, out_shape=[jax.ShapeDtypeStruct((2, FOUR, to...  23.3 us
    unnamed x53, local copies, waits for them, and re-layouts  9.13 us

profile of v3, /device:TPU:1, one launch (start us, length us, event | category | flops | bytes accessed | tf_op | source)
XLA Modules:
  0.0 131.9 jit_solution(1152448379326227541)
XLA Ops:
  0.0 1.3 %copy.21.down_d_ref = bf16[2048,96]{1,0:T(8,128)(2,1)S(1)} copy(bf16[2048,96]{0,1:T(8,128)(2,1)} %param.28) | data formatting | bytes 786432 | tf_op args[8]
  1.4 0.0 copy-start.1
  1.4 0.0 copy-start.2
  1.4 0.0 copy-start.4
  1.4 0.0 copy-start.5
  1.4 0.0 copy-start.6
  1.4 0.0 copy-start.7
  1.4 0.0 copy-start.8
  1.4 0.0 copy-start.9
  1.4 0.0 copy-start.10
  1.5 0.0 copy-start.13
  1.5 0.3 copy.22.down_e_ref
  1.8 0.6 copy-done.1
  2.4 0.1 copy-done.2
  2.5 0.0 copy-start.23
  2.6 39.0 %front.1 = (bf16[4,128,640]{2,1,0:T(8,128)(2,1)S(1)}, f32[2,4,128,128]{3,2,1,0:T(8,128)S(1)}, f32[2,4,128,128]{3,2,1,0:T(8,128)S(1)}) custom-call(bf16[128,1024]{1,0:T(8,128)(2,1)S(1)} %bitcast.11, f32[1,2048]{1,0:T(1,128)S(1)} %bitcast.12, bf16[16,512]{1,0:T(8,128)(2,1)S(1)} %copy-done.4, bf16[16,512]{1,0:T(8,128)(2,1)S(1)} %copy-done.5, ...), custom_call_target="tpu_custom_call" | custom-call | flops 1000000000 | bytes 2097152 | tf_op jit(solution)/shard_map/front/pallas_call | solution.py:744
  41.6 0.8 copy-done.18
  42.4 0.8 copy-done.20
  43.2 0.7 copy-done.24
  43.9 0.1 maximum_bitcast_fusion
  44.0 1.0 copy-done.19
  45.1 1.0 copy-done.21
  46.1 23.3 %local_maps.1 = (f32[2,4,128,128]{3,2,1,0:T(8,128)S(1)}, f32[4,128,128]{2,1,0:T(8,128)S(1)}, bf16[32,48,128]{2,1,0:T(8,128)(2,1)S(1)}, bf16[8,4,16,1024]{3,2,1,0:T(8,128)(2,1)S(1)}) custom-call(bf16[4,128,640]{2,1,0:T(8,128)(2,1)S(1)} %get-tuple-element.12.proj_ref, f32[2,4,128,128]{3,2,1,0:T(8,128)S(1)} %copy-done.19, f32[2,4,128,128]{3,2,1,0:T(8,128)S(1)} %copy-done.21, ...), custom_call_target="tpu_custom_call" | custom-call | flops 1000000000 | bytes 2097152 | tf_op jit(solution)/shard_map/local_maps/pallas_call | solution.py:774
  69.4 1.0 copy-done.16
  70.4 0.2 broadcast_multiply_fusion
  70.6 0.4 concatenate.4
  71.1 0.7 fusion.5
  71.8 0.0 copy-done
  71.8 0.6 copy-done.15
  72.4 33.3 %exchange.1.mix_ref = bf16[4,128,256]{2,1,0:T(8,128)(2,1)S(1)} custom-call(bf16[32,48,128]{2,1,0:T(8,128)(2,1)S(1)} %get-tuple-element.15.msg_ref, f32[2,16,64,64]{3,2,1,0:T(8,128)S(1)} %copy-done, f32[2,4,128,128]{3,2,1,0:T(8,128)S(1)} %get-tuple-element.16.reads_ref, f32[4,128,128]{2,1,0:T(8,128)S(1)} %get-tuple-element.17.local_ref, ...), custom_call_target="tpu_custom_call" | custom-call | flops 1000000000 | bytes 2097152 | tf_op jit(solution)/shard_map/exchange/pallas_call | solution.py:794
  105.7 25.4 %project_out.1 = bf16[64,2048]{1,0:T(8,128)(2,1)S(1)} custom-call(bf16[4,128,256]{2,1,0:T(8,128)(2,1)S(1)} %exchange.1.mix_ref, bf16[8,4,16,1024]{3,2,1,0:T(8,128)(2,1)S(1)} %copy-done.17), custom_call_target="tpu_custom_call" | custom-call | flops 1000000000 | bytes 2097152 | tf_op jit(solution)/shard_map/project_out/pallas_call | solution.py:814
  131.2 0.7 copy.26
  (34 shorter events, 0.1 us)
Async XLA Ops:
  0.0 1.3 %copy-start.22 = (bf16[2048,96]{0,1:T(8,128)(2,1)S(1)}, bf16[2048,96]{0,1:T(8,128)(2,1)}, u32[]{:S(2)}) copy-start(bf16[2048,96]{0,1:T(8,128)(2,1)} %param.32) | copy-start | bytes 1179652
  0.0 1.8 %copy-start.3 = (bf16[1,128,1024]{2,1,0:T(8,128)(2,1)S(1)}, bf16[1,128,1024]{2,1,0:T(8,128)(2,1)}, u32[]{:S(2)}) copy-start(bf16[1,128,1024]{2,1,0:T(8,128)(2,1)} %param.20) | copy-start | bytes 786436
  1.4 1.0 copy-start.1
  1.4 1.1 copy-start.2
  1.4 1.1 copy-start.4
  1.4 1.1 copy-start.5
  1.4 1.1 copy-start.6
  1.4 1.1 copy-start.7
  1.4 1.1 copy-start.8
  1.4 1.1 copy-start.9
  1.4 1.1 copy-start.10
  1.5 1.1 copy-start.11
  1.5 1.1 copy-start.12
  1.5 1.1 copy-start.13
  2.5 40.6 %copy-start.23 = (bf16[512,16]{0,1:T(8,128)(2,1)S(1)}, bf16[512,16]{0,1:T(8,128)(2,1)}, u32[]{:S(2)}) copy-start(bf16[512,16]{0,1:T(8,128)(2,1)} %param.39) | copy-start | bytes 49156
  41.6 0.8 copy-start.18
  42.4 0.8 copy-start.20
  43.2 0.7 copy-start.24
  44.0 1.0 copy-start.19
  45.1 1.0 copy-start.21
  69.4 1.0 copy-start.16
  70.6 1.2 copy-start
  71.1 0.8 copy-start.14
  71.8 0.7 copy-start.15
  72.4 33.3 %copy-start.17 = (bf16[8,4,16,1024]{3,2,1,0:T(8,128)(2,1)S(1)}, bf16[8,4,16,1024]{3,2,1,0:T(8,128)(2,1)}, u32[]{:S(2)}) copy-start(bf16[8,4,16,1024]{3,2,1,0:T(8,128)(2,1)} %copy-done.16) | copy-start | bytes 3145732

commit v4 on v3

--- a/solution.py
+++ b/solution.py
@@ -1,3 +1,4 @@
+import math
 import functools
 import jax
 import jax.numpy as jnp
@@ -50,6 +51,14 @@
     (ka,), (kb,) = dims[0]
     a_hi, a_lo = split2(a)
     b_hi, b_lo = split2(b)
+    free = 1 - kb
+    if b.shape[free] == PAIR:
+        upper = jnp.concatenate([b_hi, b_lo], axis=free)
+        lower = jnp.concatenate([b_hi, jnp.zeros_like(b_lo)], axis=free)
+        wide = dot(
+            jnp.concatenate([a_hi, a_lo], axis=ka), jnp.concatenate([upper, lower], axis=kb), dims
+        )
+        return wide[:, :PAIR] + wide[:, PAIR:]
     main = dot(
         jnp.concatenate([a_hi, a_lo], axis=ka), jnp.concatenate([b_hi, b_hi], axis=kb), dims
     )
@@ -115,23 +124,66 @@
     return start, relay, arrive_near, arrive_far, finish_sends
 
 
-def front_kernel(
-    x_ref, gain_ref, wr_ref, wk_ref, wv_ref, wq_ref, wak_ref, wav_ref,
-    down_d_ref, down_e_ref, up_d_ref, up_e_ref, off_d_ref, off_e_ref, extra_ref,
-    proj_ref, logd_ref, learn_ref,
-    both_ref, hid_ref, stage_ref, cols_ref, ext_ref,
-    x_out, x_in, hid_out, hid_in, stage_out, stage_in, ext_out, ext_in,
-    z_out, z_in, near_out, near_in, far_out, far_in,
-):
-    z, x, f, c = (lax.axis_index(a) for a in ("sp_0", "sp_1", "fs", "tp"))
+def peer_id(index):
+    inner = lax.axis_size("sp_1")
+    return {"sp_0": index // inner, "sp_1": index % inner}
+
+
+def meet(place_of):
+    z, x, f, c = place_of
+    nz, nx = lax.axis_size("sp_0"), lax.axis_size("sp_1")
+    count = nz * nx
+    barrier = pltpu.get_barrier_semaphore()
+    for k in range(1, FOUR):
+        pl.semaphore_signal(barrier, inc=1, device_id={"fs": (f + k) % FOUR}, device_id_type=MESH)
+    pl.semaphore_signal(barrier, inc=1, device_id={"tp": 1 - c}, device_id_type=MESH)
+
+    def greet(k, carry):
+        pl.semaphore_signal(barrier, inc=1, device_id=peer_id((z * nx + x + k) % count), device_id_type=MESH)
+        return carry
+
+    lax.fori_loop(1, count, greet, 0)
+    pl.semaphore_wait(barrier, count - 1 + FOUR)
+
+
+def rope_tables(place, cos_ref, sin_ref):
+    reach = cos_ref.shape[0]
+    block = reach // 3
+    spot = iota((reach, PAIR), 0)
+    lane = iota((reach, PAIR), 1)
+    grid_row = ((place - 1) * (block // GRID_W) + spot // GRID_W).astype(F32)
+    grid_col = (spot % GRID_W).astype(F32)
+    power = (lane % 16).astype(F32) * (1.0 / 16)
+    angle = jnp.where(lane % HD < HD // 2, grid_row, grid_col) * jnp.exp(power * -math.log(ROPE_BASE))
+    cos_ref[...] = jnp.cos(angle)
+    sin_ref[...] = jnp.sin(angle)
+
+
+def front(refs, place_of):
+    (
+        x_ref, gain_ref, wr_ref, wk_ref, wv_ref, wq_ref, wak_ref, wav_ref, down_d_ref, down_e_ref,
+        up_d_ref, up_e_ref, off_d_ref, off_e_ref, extra_ref, proj_ref, logd_ref, learn_ref,
+        both_ref, hid_ref, stage_ref, cols_ref, ext_ref, load_sem,
+        x_out, x_in, hid_out, hid_in, stage_out, stage_in, ext_out, ext_in,
+        z_out, z_in, near_out, near_in, far_out, far_in, cos_ref, sin_ref, late,
+    ) = refs
+    z, x, f, c = place_of
     nz, nx = lax.axis_size("sp_0"), lax.axis_size("sp_1")
     mine = z * nx + x
     rows = wr_ref.shape[0]
-    barrier = pltpu.get_barrier_semaphore()
-    peers = [{"fs": (f + k) % FOUR} for k in range(1, FOUR)] + [{"tp": 1 - c}]
-    peers += [{"sp_0": (z + k) % nz} for k in (1, nz - 1)] + [{"sp_1": (x + k) % nx} for k in (1, nx - 1)]
-    for peer in peers:
-        pl.semaphore_signal(barrier, inc=1, device_id=peer, device_id_type=MESH)
+    loads = []
+    for g in range(FOUR):
+        for k, ref in enumerate((wr_ref, wk_ref, wv_ref, wq_ref)):
+            loads.append((ref.at[:, g * PAIR : (g + 1) * PAIR], stage_ref.at[g, :, k * PAIR : (k + 1) * PAIR]))
+    loads.append((x_ref, both_ref.at[c]))
+    loads.append((extra_ref.at[0], ext_ref.at[f]))
+    loads = [
+        pltpu.make_async_copy(start, end, load_sem.at[number]) for number, (start, end) in enumerate(loads)
+    ]
+    for load in loads:
+        load.start()
+    for load in late:
+        load.start()
     low = iota((rows, PAIR), 1) < HD
     keys, values = wak_ref[...].astype(F32), wav_ref[...].astype(F32)
     shared = [
@@ -139,18 +191,15 @@
         jnp.where(low, pltpu.roll(keys, HD, 1), values).astype(BF),
     ]
     for g in range(FOUR):
-        lanes = slice(g * PAIR, (g + 1) * PAIR)
-        for k, ref in enumerate((wr_ref, wk_ref, wv_ref, wq_ref)):
-            stage_ref[g, :, k * PAIR : (k + 1) * PAIR] = ref[:, lanes]
         stage_ref[g, :, 4 * PAIR :] = shared[g // 2]
-    both_ref[c] = x_ref[...]
-    ext_ref[f] = extra_ref[0]
+    for load in loads:
+        load.wait()
     my_rows = pl.ds(pl.multiple_of(f * rows, rows), rows)
     cols_ref[mine, my_rows, :] = stage_ref[f]
-    pl.semaphore_wait(barrier, len(peers))
+    meet(place_of)
 
     half_copy = pltpu.make_async_remote_copy(
-        src_ref=x_ref, dst_ref=both_ref.at[c], send_sem=x_out, recv_sem=x_in,
+        src_ref=both_ref.at[c], dst_ref=both_ref.at[c], send_sem=x_out, recv_sem=x_in,
         device_id={"tp": 1 - c}, device_id_type=MESH,
     )
     half_copy.start()
@@ -171,7 +220,7 @@
 
     def ext_copy(k, source):
         return pltpu.make_async_remote_copy(
-            src_ref=extra_ref.at[0], dst_ref=ext_ref.at[source],
+            src_ref=ext_ref.at[source], dst_ref=ext_ref.at[source],
             send_sem=ext_out.at[k], recv_sem=ext_in.at[k], device_id={"fs": (f + k) % FOUR}, device_id_type=MESH,
         )
 
@@ -230,6 +279,7 @@
     for k in range(1, FOUR):
         ext_copy(k, f).start()
     start()
+    rope_tables(mine, cos_ref, sin_ref)
 
     steps = nz // 2
     for step in range(steps):
@@ -256,12 +306,14 @@
     for k in range(1, FOUR):
         ext_copy(k, (f + FOUR - k) % FOUR).wait_recv()
 
+    for load in late:
+        load.wait()
     tokens = hid_ref.shape[1]
     hidden = hid_ref[...].reshape(FOUR * tokens, hid_ref.shape[2])
-    decay_low = dot(hidden, down_d_ref[...]).astype(BF)
-    learn_low = dot(hidden, down_e_ref[...]).astype(BF)
+    decay_low = dot(hidden, down_d_ref[...], NT).astype(BF)
+    learn_low = dot(hidden, down_e_ref[...], NT).astype(BF)
     decay_act = jnp.tanh(decay_low.astype(F32)).astype(BF)
-    heads = extra_ref.shape[1]
+    heads = ext_ref.shape[1]
     first = c * heads * HD + f * PAIR
     chosen = pl.ds(pl.multiple_of(first, PAIR), PAIR)
     select = ones_where(iota((heads, PAIR), 0) == 2 * f + iota((heads, PAIR), 1) // HD).astype(F32)
@@ -314,18 +366,11 @@
     return x[:CH] + x[CH:]
 
 
-def local_kernel(
-    proj_ref, logd_ref, learn_ref, wout_ref, q_ref, o_ref, msg_ref, rows_ref,
-    z_out, z_in, x_out, x_in,
-):
-    z, x = lax.axis_index("sp_0"), lax.axis_index("sp_1")
+def local_maps(refs, place_of, send_halo, send_maps):
+    proj_ref, logd_ref, learn_ref, wout_ref, q_ref, o_ref, msg_ref, rows_ref, z_out, z_in, x_out, x_in = refs
+    z, x = place_of[:2]
     nz, nx = lax.axis_size("sp_0"), lax.axis_size("sp_1")
-    barrier = pltpu.get_barrier_semaphore()
-    peers = [{"sp_0": (z + k) % nz} for k in range(1, nz)] + [{"sp_1": (x + k) % nx} for k in range(1, nx)]
-    for peer in peers:
-        pl.semaphore_signal(barrier, inc=1, device_id=peer, device_id_type=MESH)
     rows_ref[z, x] = wout_ref[...]
-    pl.semaphore_wait(barrier, len(peers))
 
     def z_copy(k, source):
         return pltpu.make_async_remote_copy(
@@ -352,6 +397,10 @@
     within = [t >= s, t <= s]
 
     def one_pair(p, carry):
+        @pl.when(p == 1)
+        def _():
+            send_halo()
+
         @pl.when(p == FOUR // 2)
         def _():
             for k in range(1, nz):
@@ -441,11 +490,17 @@
                     msg_ref[d * 16 + p * 4 + hh * 2 + half] = message.astype(msg_ref.dtype)
         for c in range(2):
             o_ref[p, c * CH : (c + 1) * CH, :] = out_rows[c]
+
+        @pl.when(p > 0)
+        def _():
+            send_maps(p - 1)
+
         return carry
 
     lax.fori_loop(0, FOUR, one_pair, 0)
     for k in range(1, nx):
         x_copy(k, (x + nx - k) % nx).wait_recv()
+    send_maps(FOUR - 1)
     for k in range(1, nz):
         z_copy(k, z).wait_send()
     for k in range(1, nx):
@@ -459,28 +514,15 @@
     return pltpu.roll(upper, HD, 1) + lower
 
 
-def peer_id(index):
-    inner = lax.axis_size("sp_1")
-    return {"sp_0": index // inner, "sp_1": index % inner}
-
-
-def exchange_kernel(
-    msg_ref, init_ref, reads_ref, local_ref, gain_ref, proj_ref, cos_ref, sin_ref, sink_ref,
-    mix_ref,
-    recv_ref, sent_ref, enter_ref, halo_ref,
-    out_sem, in_sem, back_out_sem, back_in_sem, halo_out_sem, halo_in_sem,
-):
+def exchange(refs, place_of):
+    (
+        msg_ref, init_ref, reads_ref, local_ref, gain_ref, proj_ref, cos_ref, sin_ref, sink_ref, mix_ref,
+        recv_ref, sent_ref, enter_ref, halo_ref, comp_ref,
+        out_sem, in_sem, back_out_sem, back_in_sem, halo_out_sem, halo_in_sem,
+    ) = refs
     count = recv_ref.shape[0]
-    place = lax.axis_index("sp_0") * lax.axis_size("sp_1") + lax.axis_index("sp_1")
+    place = place_of[0] * lax.axis_size("sp_1") + place_of[1]
     kv_first = 4 * PAIR
-    barrier = pltpu.get_barrier_semaphore()
-
-    def greet(k, carry):
-        pl.semaphore_signal(barrier, inc=1, device_id=peer_id((place + k) % count), device_id_type=MESH)
-        return carry
-
-    lax.fori_loop(1, count, greet, 0)
-    pl.semaphore_wait(barrier, count - 1)
 
     def halo_copy(side):
         target = (place + count - 1 + 2 * side) % count
@@ -533,102 +575,129 @@
             device_id_type=MESH,
         )
 
-    halo_copy(0).start()
-    halo_copy(1).start()
-
-    def send_map(k, carry):
-        map_copy((place + k) % count).start()
-        return carry
-
-    lax.fori_loop(1, count, send_map, 0)
-    recv_ref[place] = msg_ref[place]
-
-    tokens = local_ref.shape[1]
-    for side in range(2):
-        halo_copy(side).wait()
-    lane = iota((1, PAIR), 1)
-    low = lane < HD
-    front = lane % 32 < 16
-
-    def turned(v, first, last):
-        other = jnp.where(front, -pltpu.roll(v, PAIR - 16, 1), pltpu.roll(v, 16, 1))
-        return v * cos_ref[first:last, :] + other * sin_ref[first:last, :]
-
-    reach = 3 * tokens
-    q_pos = place * tokens + iota((2 * tokens, reach), 0) % tokens
-    k_pos = (place - 1) * tokens + iota((2 * tokens, reach), 1)
-    allowed = (jnp.abs(q_pos - k_pos) <= WINDOW) & (k_pos >= 0) & (k_pos < count * tokens)
-    upper = iota((2 * tokens, 1), 0) < tokens
-    pair = lax.axis_index("fs")
-    first_head = lax.axis_index("tp") * (2 * FOUR) + 2 * pair
-    sink = jnp.where(upper, sink_ref[first_head], sink_ref[first_head + 1])
-
-    def attend(p, carry):
-        kv = jnp.concatenate(
-            [halo_ref[0, p], proj_ref[p, :, kv_first : kv_first + PAIR], halo_ref[1, p]], axis=0
-        ).astype(F32)
-        roped = turned(kv, 0, reach)
-        swapped = pltpu.roll(kv, HD, 1)
-        key = jnp.where(low, roped, pltpu.roll(roped, HD, 1)).astype(BF)
-        value = jnp.where(low, swapped, kv).astype(BF)
-        query = turned(proj_ref[p, :, kv_first - PAIR : kv_first].astype(F32), tokens, 2 * tokens)
-        query = jnp.concatenate([jnp.where(low, query, 0.0), jnp.where(low, 0.0, query)], axis=0)
-        scores = dot(query.astype(BF), key, NT) * HD**-0.5
-        scores = jnp.where(allowed, scores, -jnp.inf)
-        top = jnp.maximum(jnp.max(scores, axis=-1, keepdims=True), sink)
-        raised = jnp.exp(scores - top)
-        total = jnp.exp(sink - top) + jnp.sum(raised, axis=-1, keepdims=True)
-        mixed = dot((raised / total).astype(BF), value)
-        mix_ref[p, :, PAIR:] = jnp.where(low, mixed[:tokens], mixed[tokens:]).astype(BF)
-        return carry
-
-    lax.fori_loop(0, FOUR, attend, 0)
-
-    def await_map(k, carry):
-        map_arrival((place + k) % count).wait()
-        return carry
-
-    lax.fori_loop(1, count, await_map, 0)
-
-    unit_idx = place // 2
-    direction, half = unit_idx // 8, place % 2
-    rows = HD // 2
-    quarter = rows // 2
-    start = pl.multiple_of(half * rows, rows)
-
-    def unfolded(x):
-        return jnp.concatenate([x[:, :HD], x[:, HD:]], axis=0)
-
-    def nth(step):
-        return direction * (count - 1) + step * (1 - 2 * direction)
-
-    def advance(step, state):
-        idx = nth(step)
-        sent_ref[idx] = jnp.concatenate([state[:quarter], state[quarter:]], axis=1).astype(BF)
-        before = nth(step - 1)
-
-        @pl.when((step > 0) & (before != place))
-        def _():
-            entry_copy(before).start()
-
-        message = recv_ref[idx].astype(F32)
-        return state + mm3(state, unfolded(message[:rows])) + unfolded(message[rows:])
-
-    state = init_ref[direction, first_head + unit_idx % 2, pl.ds(start, rows), :]
-    lax.fori_loop(0, count, advance, state)
-    final = nth(count - 1)
-    enter_ref[place] = sent_ref[place]
-
-    @pl.when(final != place)
-    def _():
-        entry_copy(final).start()
-
-    def await_entry(k, carry):
-        entry_arrival((place + k) % count).wait()
-        return carry
-
-    lax.fori_loop(1, count, await_entry, 0)
-    finish(reads_ref, local_ref, enter_ref, gain_ref, mix_ref)
+    def send_halo():
+        halo_copy(0).start()
+        halo_copy(1).start()
+
+    def send_maps(p):
+        for d in range(2):
+            for q in range(4):
+                target = d * 16 + p * 4 + q
+
+                @pl.when(target != place)
+                def _():
+                    map_copy(target).start()
+
+    def run():
+        tokens = local_ref.shape[1]
+        for side in range(2):
+            halo_copy(side).wait()
+        lane = iota((1, PAIR), 1)
+        low = lane < HD
+        front = lane % 32 < 16
+
+        def turned(v, first, last):
+            other = jnp.where(front, -pltpu.roll(v, PAIR - 16, 1), pltpu.roll(v, 16, 1))
+            return v * cos_ref[first:last, :] + other * sin_ref[first:last, :]
+
+        reach = 3 * tokens
+        q_pos = place * tokens + iota((2 * tokens, reach), 0) % tokens
+        k_pos = (place - 1) * tokens + iota((2 * tokens, reach), 1)
+        allowed = (jnp.abs(q_pos - k_pos) <= WINDOW) & (k_pos >= 0) & (k_pos < count * tokens)
+        upper = iota((2 * tokens, 1), 0) < tokens
+        pair = lax.axis_index("fs")
+        first_head = lax.axis_index("tp") * (2 * FOUR) + 2 * pair
+        sink = jnp.where(upper, sink_ref[first_head], sink_ref[first_head + 1])
+
+        def attend(p, carry):
+            kv = jnp.concatenate(
+                [halo_ref[0, p], proj_ref[p, :, kv_first : kv_first + PAIR], halo_ref[1, p]], axis=0
+            ).astype(F32)
+            roped = turned(kv, 0, reach)
+            swapped = pltpu.roll(kv, HD, 1)
+            key = jnp.where(low, roped, pltpu.roll(roped, HD, 1)).astype(BF)
+            value = jnp.where(low, swapped, kv).astype(BF)
+            query = turned(proj_ref[p, :, kv_first - PAIR : kv_first].astype(F32), tokens, 2 * tokens)
+            query = jnp.concatenate([jnp.where(low, query, 0.0), jnp.where(low, 0.0, query)], axis=0)
+            scores = dot(query.astype(BF), key, NT) * HD**-0.5
+            scores = jnp.where(allowed, scores, -jnp.inf)
+            top = jnp.maximum(jnp.max(scores, axis=-1, keepdims=True), sink)
+            raised = jnp.exp(scores - top)
+            total = jnp.exp(sink - top) + jnp.sum(raised, axis=-1, keepdims=True)
+            mixed = dot((raised / total).astype(BF), value)
+            mix_ref[pair, p, :, PAIR:] = jnp.where(low, mixed[:tokens], mixed[tokens:]).astype(BF)
+            return carry
+
+        lax.fori_loop(0, FOUR, attend, 0)
+
+        recv_ref[place] = msg_ref[place]
+
+        def await_map(k, carry):
+            map_arrival((place + k) % count).wait()
+            return carry
+
+        lax.fori_loop(1, count, await_map, 0)
+
+        unit_idx = place // 2
+        direction, half = unit_idx // 8, place % 2
+        rows = HD // 2
+        quarter = rows // 2
+        start = pl.multiple_of(half * rows, rows)
+        groups = 4
+        length = count // groups
+
+        def nth(step):
+            return direction * (count - 1) + step * (1 - 2 * direction)
+
+        def message(step):
+            m = recv_ref[nth(step)].astype(F32)
+            return jnp.concatenate([m[:rows, :HD], m[:rows, HD:], m[rows:, :HD], m[rows:, HD:]], axis=0)
+
+        def extend(s, maps):
+            longer = []
+            for g in range(groups):
+                step = message(g * length + s)
+                comp_ref[g, s] = maps[g]
+                longer.append(maps[g] + mm3(maps[g], step[:HD]) + step)
+            return tuple(longer)
+
+        nothing = jnp.zeros((3 * rows, HD), F32)
+        maps = lax.fori_loop(0, length, extend, (nothing,) * groups)
+        state = init_ref[direction, first_head + unit_idx % 2, pl.ds(start, rows), :]
+
+        def dispatch(g):
+            def one(s, carry):
+                target = nth(g * length + s)
+
+                @pl.when(target != place)
+                def _():
+                    entry_copy(target).start()
+
+                return carry
+
+            lax.fori_loop(0, length, one, 0)
+
+        for g in range(groups):
+            for s in range(length):
+                before = comp_ref[g, s]
+                entry = state + mm3(state, before[:HD]) + before[HD:] if s else state
+                sent_ref[nth(g * length + s)] = jnp.concatenate(
+                    [entry[:quarter], entry[quarter:]], axis=1
+                ).astype(BF)
+            state = state + mm3(state, maps[g][:HD]) + maps[g][HD:]
+            if g:
+                dispatch(g - 1)
+        enter_ref[place] = sent_ref[place]
+        dispatch(groups - 1)
+
+        def await_entry(k, carry):
+            entry_arrival((place + k) % count).wait()
+            return carry
+
+        lax.fori_loop(1, count, await_entry, 0)
+        finish(reads_ref, local_ref, enter_ref, gain_ref, mix_ref.at[pair])
+
+    return send_halo, send_maps, run
 
 
 def finish(q_ref, o_ref, enter_ref, gain_ref, mix_ref):
@@ -656,18 +725,13 @@
         mix_ref[p, :, :PAIR] = (centred * lax.rsqrt(spread + GROUP_EPS) * gain).astype(BF)
 
 
-def out_kernel(
-    mix_ref, rows_ref, out_ref, all_ref, total_ref, other_ref, ready_ref, got_ref,
-    mix_out, mix_in, half_out, half_in, back_out, back_in,
-):
-    f, c = lax.axis_index("fs"), lax.axis_index("tp")
-    tokens = mix_ref.shape[1]
-    barrier = pltpu.get_barrier_semaphore()
-    peers = [{"fs": (f + k) % FOUR} for k in range(1, FOUR)] + [{"tp": 1 - c}]
-    for peer in peers:
-        pl.semaphore_signal(barrier, inc=1, device_id=peer, device_id_type=MESH)
-    all_ref[f] = mix_ref[...]
-    pl.semaphore_wait(barrier, len(peers))
+def project_out(refs, place_of):
+    (
+        rows_ref, out_ref, all_ref, total_ref, other_ref, ready_ref, got_ref,
+        mix_out, mix_in, half_out, half_in, back_out, back_in,
+    ) = refs
+    f, c = place_of[2:]
+    tokens = all_ref.shape[2]
     start, relay, arrive_near, arrive_far, finish_sends = ring_of_four(all_ref, mix_out, mix_in)
     start()
     columns = total_ref.shape[2]
@@ -721,6 +785,68 @@
         back_copy(k, f).wait_send()
 
 
+def layer_kernel(
+    x_ref, gain_ref, wr_ref, wk_ref, wv_ref, wq_ref, wak_ref, wav_ref, down_d_hbm, down_e_hbm,
+    up_d_hbm, up_e_hbm, off_d_ref, off_e_ref, extra_ref, init_hbm, head_gain_ref, sink_ref,
+    lin_out_ref, att_out_ref,
+    out_ref,
+    both_ref, hid_ref, stage_ref, cols_ref, ext_ref, down_d_ref, down_e_ref, up_d_ref, up_e_ref, init_ref,
+    proj_ref, logd_ref, learn_ref, cos_ref, sin_ref, wout_ref,
+    reads_ref, local_ref, msg_ref, rows_ref,
+    recv_ref, sent_ref, enter_ref, halo_ref, comp_ref,
+    all_ref, total_ref, other_ref, ready_ref, got_ref,
+    load_sem, late_sem, x_out, x_in, hid_out, hid_in, stage_out, stage_in, ext_out, ext_in,
+    z_out, z_in, near_out, near_in, far_out, far_in,
+    wz_out, wz_in, wx_out, wx_in,
+    out_sem, in_sem, back_out_sem, back_in_sem, halo_out_sem, halo_in_sem,
+    mix_out, mix_in, half_out, half_in, back_out, back_in,
+):
+    place_of = tuple(lax.axis_index(a) for a in ("sp_0", "sp_1", "fs", "tp"))
+    pairs = (
+        (down_d_hbm, down_d_ref), (down_e_hbm, down_e_ref), (up_d_hbm, up_d_ref), (up_e_hbm, up_e_ref),
+        (init_hbm, init_ref),
+    )
+    late = [pltpu.make_async_copy(a, b, late_sem.at[k]) for k, (a, b) in enumerate(pairs)]
+    for g in range(FOUR):
+        for k, ref in enumerate((lin_out_ref, att_out_ref)):
+            wout_ref[:, (2 * g + k) * PAIR : (2 * g + k + 1) * PAIR] = ref[:, g * PAIR : (g + 1) * PAIR]
+    front(
+        (
+            x_ref, gain_ref, wr_ref, wk_ref, wv_ref, wq_ref, wak_ref, wav_ref, down_d_ref, down_e_ref,
+            up_d_ref, up_e_ref, off_d_ref, off_e_ref, extra_ref, proj_ref, logd_ref, learn_ref,
+            both_ref, hid_ref, stage_ref, cols_ref, ext_ref, load_sem,
+            x_out, x_in, hid_out, hid_in, stage_out, stage_in, ext_out, ext_in,
+            z_out, z_in, near_out, near_in, far_out, far_in, cos_ref, sin_ref, late,
+        ),
+        place_of,
+    )
+    send_halo, send_maps, run = exchange(
+        (
+            msg_ref, init_ref, reads_ref, local_ref, head_gain_ref, proj_ref, cos_ref, sin_ref, sink_ref,
+            all_ref, recv_ref, sent_ref, enter_ref, halo_ref, comp_ref,
+            out_sem, in_sem, back_out_sem, back_in_sem, halo_out_sem, halo_in_sem,
+        ),
+        place_of,
+    )
+    local_maps(
+        (
+            proj_ref, logd_ref, learn_ref, wout_ref, reads_ref, local_ref, msg_ref, rows_ref,
+            wz_out, wz_in, wx_out, wx_in,
+        ),
+        place_of,
+        send_halo,
+        send_maps,
+    )
+    run()
+    project_out(
+        (
+            rows_ref, out_ref, all_ref, total_ref, other_ref, ready_ref, got_ref,
+            mix_out, mix_in, half_out, half_in, back_out, back_in,
+        ),
+        place_of,
+    )
+
+
 def local(
     inputs, input_norm_gain, receptance_weight, linear_key_weight, linear_value_weight,
     window_query_weight, window_key_weight, window_value_weight, decay_down_weight, decay_up_weight,
@@ -730,104 +856,72 @@
     tokens, model = inputs.shape[1], 2 * inputs.shape[2]
     places = lax.axis_size(SP)
     nz, nx = lax.axis_size("sp_0"), lax.axis_size("sp_1")
-    offset = lax.axis_index(SP) * tokens
     rows = receptance_weight.shape[0]
     out_rows = linear_output_weight.shape[1]
+    columns = places * out_rows
     vmem = pl.BlockSpec(memory_space=pltpu.VMEM)
+    hbm = pl.BlockSpec(memory_space=pl.ANY)
+    smem = pl.BlockSpec(memory_space=pltpu.SMEM)
     dma = pltpu.SemaphoreType.DMA
-
-    def params(number):
-        return pltpu.CompilerParams(
-            collective_id=number, has_side_effects=True, vmem_limit_bytes=48 * 2**20
-        )
-
-    proj, logd, learn = pl.pallas_call(
-        front_kernel,
-        out_shape=[
-            jax.ShapeDtypeStruct((FOUR, tokens, 5 * PAIR), BF),
-            jax.ShapeDtypeStruct((2, FOUR, tokens, PAIR), F32),
-            jax.ShapeDtypeStruct((2, FOUR, tokens, PAIR), F32),
-        ],
-        in_specs=[vmem] * 15,
-        out_specs=[vmem] * 3,
+    down_d, down_e = decay_down_weight.T, erasure_down_weight.T
+
+    def space(kind, *shape):
+        return pltpu.VMEM(shape, kind)
+
+    out = pl.pallas_call(
+        layer_kernel,
+        out_shape=jax.ShapeDtypeStruct((tokens // 2, FOUR * columns), BF),
+        in_specs=[hbm, vmem, hbm, hbm, hbm, hbm, vmem, vmem, hbm, hbm, hbm, hbm, vmem, vmem, hbm, hbm, vmem, smem, vmem, vmem],
+        out_specs=vmem,
         scratch_shapes=[
-            pltpu.VMEM((2, tokens, model // 2), BF),
-            pltpu.VMEM((FOUR, tokens, model), BF),
-            pltpu.VMEM((FOUR, rows, 5 * PAIR), BF),
-            pltpu.VMEM((places, FOUR * rows, 5 * PAIR), BF),
-            pltpu.VMEM((FOUR, *decay_log_extra.shape[1:]), F32),
+            space(BF, 2, tokens, model // 2),
+            space(BF, FOUR, tokens, model),
+            space(BF, FOUR, rows, 5 * PAIR),
+            space(BF, places, FOUR * rows, 5 * PAIR),
+            space(F32, FOUR, *decay_log_extra.shape[1:]),
+            space(BF, *down_d.shape),
+            space(BF, *down_e.shape),
+            space(BF, *decay_up_weight.shape),
+            space(BF, *erasure_up_weight.shape),
+            space(F32, *initial_state.shape),
+            space(BF, FOUR, tokens, 5 * PAIR),
+            space(F32, 2, FOUR, tokens, PAIR),
+            space(F32, 2, FOUR, tokens, PAIR),
+            space(F32, tokens + 2 * WINDOW, PAIR),
+            space(F32, tokens + 2 * WINDOW, PAIR),
+            space(BF, out_rows, 2 * FOUR * PAIR),
+            space(F32, 2, FOUR, tokens, PAIR),
+            space(F32, FOUR, tokens, PAIR),
+            space(BF, places, 48, PAIR),
+            space(BF, nz, nx, out_rows, 2 * FOUR * PAIR),
+            space(BF, places, 48, PAIR),
+            space(BF, places, 16, PAIR),
+            space(BF, places, 16, PAIR),
+            space(BF, 2, FOUR, tokens, PAIR),
+            space(F32, 4, places // 4, 3 * HD // 2, HD),
+            space(BF, FOUR, FOUR, tokens, 2 * PAIR),
+            space(F32, FOUR, tokens, columns),
+            space(F32, FOUR, tokens // 2, columns),
+            space(BF, FOUR, tokens // 2, columns),
+            space(BF, FOUR, tokens // 2, columns),
+            dma((18,)), dma((5,)),
             dma, dma, dma((6,)), dma((6,)), dma((FOUR,)), dma((FOUR,)), dma((FOUR,)), dma((FOUR,)),
             dma((2, nz // 2)), dma((2, nz // 2)), dma((nz, 2)), dma((nz, 2)), dma((nz,)), dma((nz,)),
+            dma((nz,)), dma((nz,)), dma((nx,)), dma((nx,)),
+            dma((places,)), dma((places,)), dma((places,)), dma((places,)), dma((2,)), dma((2,)),
+            dma((6,)), dma((6,)), dma, dma, dma((FOUR,)), dma((FOUR,)),
         ],
-        compiler_params=params(1),
-        name="front",
-        cost_estimate=pl.CostEstimate(flops=10**9, bytes_accessed=2**21, transcendentals=0),
+        compiler_params=pltpu.CompilerParams(
+            collective_id=0, has_side_effects=True, vmem_limit_bytes=48 * 2**20
+        ),
+        name="layer",
     )(
         inputs[0], input_norm_gain[None], receptance_weight, linear_key_weight, linear_value_weight,
-        window_query_weight, window_key_weight, window_value_weight, decay_down_weight,
-        erasure_down_weight, decay_up_weight, erasure_up_weight, decay_offset, erasure_offset,
-        decay_log_extra,
-    )
-    both = jnp.stack([linear_output_weight, window_output_weight])
-    both = both.reshape(2, FOUR, PAIR, out_rows)
-    out_weight = jnp.transpose(both, (3, 1, 0, 2)).reshape(out_rows, 2 * FOUR * PAIR)
-    reads, local_out, messages, weight_rows = pl.pallas_call(
-        local_kernel,
-        out_shape=[
-            jax.ShapeDtypeStruct((2, FOUR, tokens, PAIR), F32),
-            jax.ShapeDtypeStruct((FOUR, tokens, PAIR), F32),
-            jax.ShapeDtypeStruct((places, 48, PAIR), BF),
-            jax.ShapeDtypeStruct((nz, nx, *out_weight.shape), BF),
-        ],
-        in_specs=[vmem] * 4,
-        out_specs=[vmem] * 4,
-        scratch_shapes=[dma((nz,)), dma((nz,)), dma((nx,)), dma((nx,))],
-        compiler_params=params(2),
-        name="local_maps",
-        cost_estimate=pl.CostEstimate(flops=10**9, bytes_accessed=2**21, transcendentals=0),
-    )(proj, logd, learn, out_weight)
-    angle_pos = offset - WINDOW + jnp.arange(tokens + 2 * WINDOW, dtype=jnp.int32)
-    inverse = ROPE_BASE ** (-jnp.arange(HD // 4, dtype=jnp.float32) / (HD // 4))
-    row_angles = (angle_pos // GRID_W).astype(F32)[:, None] * inverse[None, :]
-    col_angles = (angle_pos % GRID_W).astype(F32)[:, None] * inverse[None, :]
-    angles = jnp.concatenate([row_angles, row_angles, col_angles, col_angles] * 2, axis=1)
-    mix = pl.pallas_call(
-        exchange_kernel,
-        out_shape=jax.ShapeDtypeStruct((FOUR, tokens, 2 * PAIR), BF),
-        in_specs=[vmem] * 8 + [pl.BlockSpec(memory_space=pltpu.SMEM)],
-        out_specs=vmem,
-        scratch_shapes=[
-            pltpu.VMEM((places, 48, PAIR), BF),
-            pltpu.VMEM((places, 16, PAIR), BF),
-            pltpu.VMEM((places, 16, PAIR), BF),
-            pltpu.VMEM((2, FOUR, tokens, PAIR), BF),
-            dma((places,)), dma((places,)), dma((places,)), dma((places,)), dma((2,)), dma((2,)),
-        ],
-        compiler_params=params(3),
-        name="exchange",
-        cost_estimate=pl.CostEstimate(flops=10**9, bytes_accessed=2**21, transcendentals=0),
-    )(
-        messages, initial_state, reads, local_out, head_norm_gain[None], proj,
-        jnp.cos(angles), jnp.sin(angles), query_sink_logit,
-    )
-    columns = places * out_rows
-    out = pl.pallas_call(
-        out_kernel,
-        out_shape=jax.ShapeDtypeStruct((tokens // 2, FOUR * columns), BF),
-        in_specs=[vmem] * 2,
-        out_specs=vmem,
-        scratch_shapes=[
-            pltpu.VMEM((FOUR, FOUR, tokens, 2 * PAIR), BF),
-            pltpu.VMEM((FOUR, tokens, columns), F32),
-            pltpu.VMEM((FOUR, tokens // 2, columns), F32),
-            pltpu.VMEM((FOUR, tokens // 2, columns), BF),
-            pltpu.VMEM((FOUR, tokens // 2, columns), BF),
-            dma((6,)), dma((6,)), dma, dma, dma((FOUR,)), dma((FOUR,)),
-        ],
-        compiler_params=params(4),
-        name="project_out",
-        cost_estimate=pl.CostEstimate(flops=10**9, bytes_accessed=2**21, transcendentals=0),
-    )(mix, weight_rows)
+        window_query_weight, window_key_weight, window_value_weight, down_d, down_e,
+        decay_up_weight, erasure_up_weight, decay_offset, erasure_offset, decay_log_extra,
+        initial_state, head_norm_gain[None], query_sink_logit, linear_output_weight.T,
+        window_output_weight.T,
+    )
     return out[None]
 
 

time: 132 us -> 123 us (0.932)
  Pallas kernels: 121 us -> 106 us
  local copies, waits for them, and re-layouts: 10.3 us -> 15.3 us
    pallas_call x4 -> x1, Pallas kernels: 121 us -> 106 us  [local(): pl.pallas_call(layer_kernel, out_shape=jax.ShapeDtypeStruct((tokens // 2,...]
    unnamed x53 -> x41, local copies, waits for them, and re-layouts: 9.13 us -> 15.3 us
where the time goes in v4:
time: 123 us; the launch traced here: 122 us
  Pallas kernels  106 us (86%)
  local copies, waits for them, and re-layouts  15.3 us (12%)
    pallas_call x1, Pallas kernels, local(): pl.pallas_call(layer_kernel, out_shape=jax.ShapeDtypeStruct((tokens // 2,...  106 us
    unnamed x41, local copies, waits for them, and re-layouts  15.3 us

profile of v4, /device:TPU:1, one launch (start us, length us, event | category | flops | bytes accessed | tf_op | source)
XLA Modules:
  0.0 121.8 jit_solution(15345901131885570646)
XLA Ops:
  0.0 0.0 copy-start.12
  0.0 0.0 copy-start.15
  0.0 0.0 copy-start.19
  0.0 0.7 copy-done.12
  0.7 0.0 copy-done.15
  0.7 0.0 copy-done.19
  0.7 0.0 copy-start
  0.7 1.2 %copy-done = f32[2,16,64,64]{3,2,1,0:T(8,128)S(1)} copy-done((f32[2,16,64,64]{3,2,1,0:T(8,128)S(1)}, f32[2,16,64,64]{3,2,1,0:T(8,128)}, u32[]{:S(2)}) %copy-start) | copy-done | bytes 524312
  1.9 0.0 copy-start.1
  1.9 1.0 copy-done.1
  2.9 0.0 copy-start.2
  2.9 1.0 copy-done.2
  3.9 0.0 copy-start.3
  3.9 1.0 copy-done.3
  4.9 0.0 copy-start.4
  4.9 1.0 copy-done.4
  5.9 0.0 copy-start.5
  5.9 0.9 copy-done.5
  6.9 0.0 copy-start.6
  6.9 0.7 copy-done.6
  7.6 0.7 copy-done.7
  8.3 0.7 copy-done.8
  9.0 0.7 copy-done.9
  9.7 0.7 copy-done.10
  10.5 0.7 copy-done.11
  11.2 0.7 copy-done.13
  11.9 0.7 copy-done.14
  12.6 0.7 copy-done.16
  13.3 0.7 copy-done.17
  13.9 0.7 copy-done.18
  14.6 106.4 %layer.1 = bf16[64,2048]{1,0:T(8,128)(2,1)S(1)} custom-call(bf16[128,1024]{1,0:T(8,128)(2,1)S(1)} %bitcast.11, f32[1,2048]{1,0:T(1,128)S(1)} %bitcast.14, bf16[16,512]{1,0:T(8,128)(2,1)S(1)} %copy-done.6, bf16[16,512]{1,0:T(8,128)(2,1)S(1)} %copy-done.7, bf16[16,512]{1,0:T(8,128)(2,1)S(1)} %copy-done.8, bf16[16,512]{1,0:T(8,128)(2,1)S(1)} %copy-done.9, ...), custom_call_target="tpu_custom_call" | custom-call | tf_op jit(solution)/shard_map/layer/pallas_call | solution.py:871
  121.0 0.7 copy.22
  (10 shorter events, 0.0 us)
Async XLA Ops:
  0.0 0.7 copy-start.12
  0.0 0.7 copy-start.15
  0.0 0.7 copy-start.19
  0.7 1.2 %copy-start = (f32[2,16,64,64]{3,2,1,0:T(8,128)S(1)}, f32[2,16,64,64]{3,2,1,0:T(8,128)}, u32[]{:S(2)}) copy-start(f32[2,16,64,64]{3,2,1,0:T(8,128)} %init_hbm.1) | copy-start | bytes 1572868
  1.9 1.0 copy-start.1
  2.9 1.0 copy-start.2
  3.9 1.0 copy-start.3
  4.9 1.0 copy-start.4
  5.9 0.9 copy-start.5
  6.9 0.7 copy-start.6
  7.6 0.7 copy-start.7
  8.3 0.7 copy-start.8
  9.0 0.7 copy-start.9
  9.7 0.7 copy-start.10
  10.5 0.7 copy-start.11
  11.2 0.7 copy-start.13
  11.9 0.7 copy-start.14
  12.6 0.7 copy-start.16
  13.3 0.7 copy-start.17
  13.9 0.7 copy-start.18

commit v5 on v4

--- a/solution.py
+++ b/solution.py
@@ -129,21 +129,12 @@
     return {"sp_0": index // inner, "sp_1": index % inner}
 
 
-def meet(place_of):
+def neighbours(place_of):
     z, x, f, c = place_of
     nz, nx = lax.axis_size("sp_0"), lax.axis_size("sp_1")
-    count = nz * nx
-    barrier = pltpu.get_barrier_semaphore()
-    for k in range(1, FOUR):
-        pl.semaphore_signal(barrier, inc=1, device_id={"fs": (f + k) % FOUR}, device_id_type=MESH)
-    pl.semaphore_signal(barrier, inc=1, device_id={"tp": 1 - c}, device_id_type=MESH)
-
-    def greet(k, carry):
-        pl.semaphore_signal(barrier, inc=1, device_id=peer_id((z * nx + x + k) % count), device_id_type=MESH)
-        return carry
-
-    lax.fori_loop(1, count, greet, 0)
-    pl.semaphore_wait(barrier, count - 1 + FOUR)
+    peers = [{"fs": (f + k) % FOUR} for k in range(1, FOUR)] + [{"tp": 1 - c}]
+    peers += [{"sp_0": (z + k) % nz} for k in (1, nz - 1)]
+    return peers + [{"sp_1": (x + k) % nx} for k in (1, nx - 1)]
 
 
 def rope_tables(place, cos_ref, sin_ref):
@@ -192,11 +183,13 @@
     ]
     for g in range(FOUR):
         stage_ref[g, :, 4 * PAIR :] = shared[g // 2]
-    for load in loads:
-        load.wait()
+    with jax.named_scope("f_load"):
+        for load in loads:
+            load.wait()
     my_rows = pl.ds(pl.multiple_of(f * rows, rows), rows)
     cols_ref[mine, my_rows, :] = stage_ref[f]
-    meet(place_of)
+    with jax.named_scope("f_meet"):
+        pl.semaphore_wait(pltpu.get_barrier_semaphore(), len(neighbours(place_of)))
 
     half_copy = pltpu.make_async_remote_copy(
         src_ref=both_ref.at[c], dst_ref=both_ref.at[c], send_sem=x_out, recv_sem=x_in,
@@ -265,82 +258,91 @@
         near_copy(k, 1, right).wait_recv()
         far_copy(k, left if k % 2 == 0 else right).start()
 
-    for k in range(1, FOUR):
-        stage_arrival(k).wait_recv()
+    with jax.named_scope("f_stage_wait"):
+        for k in range(1, FOUR):
+            stage_arrival(k).wait_recv()
     z_copy(0, 0, 0).start()
     z_copy(0, 1, 0).start()
     spread(0)
 
-    half_copy.wait_recv()
-    full = jnp.concatenate([both_ref[0], both_ref[1]], axis=1).astype(F32)
-    scale = lax.rsqrt(jnp.mean(full * full, axis=-1, keepdims=True) + NORM_EPS)
-    hid_ref[f] = (full * scale * gain_ref[...]).astype(BF)
+    with jax.named_scope("f_norm"):
+        half_copy.wait_recv()
+        full = jnp.concatenate([both_ref[0], both_ref[1]], axis=1).astype(F32)
+        scale = lax.rsqrt(jnp.mean(full * full, axis=-1, keepdims=True) + NORM_EPS)
+        hid_ref[f] = (full * scale * gain_ref[...]).astype(BF)
     start, relay, arrive_near, arrive_far, finish_sends = ring_of_four(hid_ref, hid_out, hid_in)
     for k in range(1, FOUR):
         ext_copy(k, f).start()
     start()
-    rope_tables(mine, cos_ref, sin_ref)
+    with jax.named_scope("f_rope"):
+        rope_tables(mine, cos_ref, sin_ref)
 
     steps = nz // 2
-    for step in range(steps):
-        k = 2 * step + 1
-        z_copy(k, 0, step).wait_recv()
-        if step < steps - 1:
-            z_copy(k, 0, step + 1).start()
-        spread(k)
-        if step < steps - 1:
-            z_copy(k + 1, 1, step).wait_recv()
-            if step < steps - 2:
-                z_copy(k + 1, 1, step + 1).start()
-            spread(k + 1)
-        if step == 0:
-            pass_on(0)
-        else:
-            pass_on(k - 2)
-            pass_on(k - 1)
-        if step == 1:
-            relay()
-    pass_on(nz - 1)
-    arrive_near()
-    arrive_far()
-    for k in range(1, FOUR):
-        ext_copy(k, (f + FOUR - k) % FOUR).wait_recv()
+    with jax.named_scope("f_ring"):
+        for step in range(steps):
+            k = 2 * step + 1
+            z_copy(k, 0, step).wait_recv()
+            if step < steps - 1:
+                z_copy(k, 0, step + 1).start()
+            spread(k)
+            if step < steps - 1:
+                z_copy(k + 1, 1, step).wait_recv()
+                if step < steps - 2:
+                    z_copy(k + 1, 1, step + 1).start()
+                spread(k + 1)
+            if step == 0:
+                pass_on(0)
+            else:
+                pass_on(k - 2)
+                pass_on(k - 1)
+            if step == 1:
+                relay()
+    with jax.named_scope("f_pass_last"):
+        pass_on(nz - 1)
+    with jax.named_scope("f_hid_wait"):
+        arrive_near()
+        arrive_far()
+        for k in range(1, FOUR):
+            ext_copy(k, (f + FOUR - k) % FOUR).wait_recv()
 
     for load in late:
         load.wait()
     tokens = hid_ref.shape[1]
     hidden = hid_ref[...].reshape(FOUR * tokens, hid_ref.shape[2])
-    decay_low = dot(hidden, down_d_ref[...], NT).astype(BF)
-    learn_low = dot(hidden, down_e_ref[...], NT).astype(BF)
-    decay_act = jnp.tanh(decay_low.astype(F32)).astype(BF)
-    heads = ext_ref.shape[1]
-    first = c * heads * HD + f * PAIR
-    chosen = pl.ds(pl.multiple_of(first, PAIR), PAIR)
-    select = ones_where(iota((heads, PAIR), 0) == 2 * f + iota((heads, PAIR), 1) // HD).astype(F32)
-    spikes = [
-        lax.dot_general(
-            ext_ref[p], select, TN, precision=lax.Precision.HIGHEST, preferred_element_type=F32
-        )
-        for p in range(FOUR)
-    ]
-    for d in range(2):
-        pre = off_d_ref[d : d + 1, chosen] + dot(decay_act, up_d_ref[d, :, chosen])
-        softplus = jnp.maximum(-pre, 0.0) + jnp.log1p(jnp.exp(-jnp.abs(pre)))
-        rate = jnp.exp(-softplus - 0.5)
-        learn = jax.nn.sigmoid(off_e_ref[d : d + 1, chosen] + dot(learn_low, up_e_ref[d, :, chosen]))
-        for p in range(FOUR):
-            part = slice(p * tokens, (p + 1) * tokens)
-            logd_ref[d, p] = spikes[p] - rate[part]
-            learn_ref[d, p] = learn[part]
-
-    for k in range(nz):
-        far_copy(k, across).wait_recv()
+    with jax.named_scope("f_rates"):
+        decay_low = dot(hidden, down_d_ref[...], NT).astype(BF)
+        learn_low = dot(hidden, down_e_ref[...], NT).astype(BF)
+        decay_act = jnp.tanh(decay_low.astype(F32)).astype(BF)
+        heads = ext_ref.shape[1]
+        first = c * heads * HD + f * PAIR
+        chosen = pl.ds(pl.multiple_of(first, PAIR), PAIR)
+        select = ones_where(iota((heads, PAIR), 0) == 2 * f + iota((heads, PAIR), 1) // HD).astype(F32)
+        spikes = [
+            lax.dot_general(
+                ext_ref[p], select, TN, precision=lax.Precision.HIGHEST, preferred_element_type=F32
+            )
+            for p in range(FOUR)
+        ]
+        for d in range(2):
+            pre = off_d_ref[d : d + 1, chosen] + dot(decay_act, up_d_ref[d, :, chosen])
+            softplus = jnp.maximum(-pre, 0.0) + jnp.log1p(jnp.exp(-jnp.abs(pre)))
+            rate = jnp.exp(-softplus - 0.5)
+            learn = jax.nn.sigmoid(off_e_ref[d : d + 1, chosen] + dot(learn_low, up_e_ref[d, :, chosen]))
+            for p in range(FOUR):
+                part = slice(p * tokens, (p + 1) * tokens)
+                logd_ref[d, p] = spikes[p] - rate[part]
+                learn_ref[d, p] = learn[part]
+
+    with jax.named_scope("f_far_wait"):
+        for k in range(nz):
+            far_copy(k, across).wait_recv()
     depth = cols_ref.shape[0] * cols_ref.shape[1]
-    for first_col, last_col in ((0, 256), (256, 512), (512, 640)):
-        weight = cols_ref[:, :, first_col:last_col].reshape(depth, last_col - first_col)
-        result = dot(hidden, weight).astype(BF)
-        for p in range(FOUR):
-            proj_ref[p, :, first_col:last_col] = result[p * tokens : (p + 1) * tokens]
+    with jax.named_scope("f_proj"):
+        for first_col, last_col in ((0, 256), (256, 512), (512, 640)):
+            weight = cols_ref[:, :, first_col:last_col].reshape(depth, last_col - first_col)
+            result = dot(hidden, weight).astype(BF)
+            for p in range(FOUR):
+                proj_ref[p, :, first_col:last_col] = result[p * tokens : (p + 1) * tokens]
 
     half_copy.wait_send()
     finish_sends()
@@ -497,14 +499,19 @@
 
         return carry
 
-    lax.fori_loop(0, FOUR, one_pair, 0)
-    for k in range(1, nx):
-        x_copy(k, (x + nx - k) % nx).wait_recv()
+    with jax.named_scope("l_loop"):
+        lax.fori_loop(0, FOUR, one_pair, 0)
     send_maps(FOUR - 1)
-    for k in range(1, nz):
-        z_copy(k, z).wait_send()
-    for k in range(1, nx):
-        x_copy(k, x).wait_send()
+
+    def await_rows():
+        for k in range(1, nx):
+            x_copy(k, (x + nx - k) % nx).wait_recv()
+        for k in range(1, nz):
+            z_copy(k, z).wait_send()
+        for k in range(1, nx):
+            x_copy(k, x).wait_send()
+
+    return await_rows
 
 
 def folded(x, hh, first, count):
@@ -516,7 +523,7 @@
 
 def exchange(refs, place_of):
     (
-        msg_ref, init_ref, reads_ref, local_ref, gain_ref, proj_ref, cos_ref, sin_ref, sink_ref, mix_ref,
+        msg_ref, init_ref, reads_ref, local_ref, gain_ref, proj_ref, cos_ref, sin_ref, sink_ref, lin_ref, att_ref,
         recv_ref, sent_ref, enter_ref, halo_ref, comp_ref,
         out_sem, in_sem, back_out_sem, back_in_sem, halo_out_sem, halo_in_sem,
     ) = refs
@@ -588,10 +595,11 @@
                 def _():
                     map_copy(target).start()
 
-    def run():
+    def run(after_attend, after_chain):
         tokens = local_ref.shape[1]
-        for side in range(2):
-            halo_copy(side).wait()
+        with jax.named_scope("x_halo"):
+            for side in range(2):
+                halo_copy(side).wait()
         lane = iota((1, PAIR), 1)
         low = lane < HD
         front = lane % 32 < 16
@@ -625,18 +633,21 @@
             raised = jnp.exp(scores - top)
             total = jnp.exp(sink - top) + jnp.sum(raised, axis=-1, keepdims=True)
             mixed = dot((raised / total).astype(BF), value)
-            mix_ref[pair, p, :, PAIR:] = jnp.where(low, mixed[:tokens], mixed[tokens:]).astype(BF)
+            att_ref[pair, p] = jnp.where(low, mixed[:tokens], mixed[tokens:]).astype(BF)
             return carry
 
-        lax.fori_loop(0, FOUR, attend, 0)
-
+        with jax.named_scope("x_attend"):
+            lax.fori_loop(0, FOUR, attend, 0)
+
+        after_attend()
         recv_ref[place] = msg_ref[place]
 
         def await_map(k, carry):
             map_arrival((place + k) % count).wait()
             return carry
 
-        lax.fori_loop(1, count, await_map, 0)
+        with jax.named_scope("x_await_map"):
+            lax.fori_loop(1, count, await_map, 0)
 
         unit_idx = place // 2
         direction, half = unit_idx // 8, place % 2
@@ -662,7 +673,8 @@
             return tuple(longer)
 
         nothing = jnp.zeros((3 * rows, HD), F32)
-        maps = lax.fori_loop(0, length, extend, (nothing,) * groups)
+        with jax.named_scope("x_compose"):
+            maps = lax.fori_loop(0, length, extend, (nothing,) * groups)
         state = init_ref[direction, first_head + unit_idx % 2, pl.ds(start, rows), :]
 
         def dispatch(g):
@@ -677,25 +689,29 @@
 
             lax.fori_loop(0, length, one, 0)
 
-        for g in range(groups):
-            for s in range(length):
-                before = comp_ref[g, s]
-                entry = state + mm3(state, before[:HD]) + before[HD:] if s else state
-                sent_ref[nth(g * length + s)] = jnp.concatenate(
-                    [entry[:quarter], entry[quarter:]], axis=1
-                ).astype(BF)
-            state = state + mm3(state, maps[g][:HD]) + maps[g][HD:]
-            if g:
-                dispatch(g - 1)
+        with jax.named_scope("x_chain"):
+            for g in range(groups):
+                for s in range(length):
+                    before = comp_ref[g, s]
+                    entry = state + mm3(state, before[:HD]) + before[HD:] if s else state
+                    sent_ref[nth(g * length + s)] = jnp.concatenate(
+                        [entry[:quarter], entry[quarter:]], axis=1
+                    ).astype(BF)
+                state = state + mm3(state, maps[g][:HD]) + maps[g][HD:]
+                if g:
+                    dispatch(g - 1)
         enter_ref[place] = sent_ref[place]
         dispatch(groups - 1)
+        after_chain()
 
         def await_entry(k, carry):
             entry_arrival((place + k) % count).wait()
             return carry
 
-        lax.fori_loop(1, count, await_entry, 0)
-        finish(reads_ref, local_ref, enter_ref, gain_ref, mix_ref.at[pair])
+        with jax.named_scope("x_await_entry"):
+            lax.fori_loop(1, count, await_entry, 0)
+        with jax.named_scope("x_finish"):
+            finish(reads_ref, local_ref, enter_ref, gain_ref, lin_ref.at[pair])
 
     return send_halo, send_maps, run
 
@@ -722,67 +738,74 @@
             out = out + mm2(q_ref[d, p], jnp.concatenate(pieces, axis=0).astype(BF), NT)
         centred = out - mm2(out, same_head) * (1.0 / HD)
         spread = mm2(centred * centred, same_head) * (1.0 / HD)
-        mix_ref[p, :, :PAIR] = (centred * lax.rsqrt(spread + GROUP_EPS) * gain).astype(BF)
-
-
-def project_out(refs, place_of):
+        mix_ref[p] = (centred * lax.rsqrt(spread + GROUP_EPS) * gain).astype(BF)
+
+
+def project_out(refs, place_of, weight):
     (
-        rows_ref, out_ref, all_ref, total_ref, other_ref, ready_ref, got_ref,
-        mix_out, mix_in, half_out, half_in, back_out, back_in,
+        out_ref, lin_ref, total_ref, other_ref, ready_ref, got_ref,
+        lin_out, lin_in, half_out, half_in, back_out, back_in,
     ) = refs
     f, c = place_of[2:]
-    tokens = all_ref.shape[2]
-    start, relay, arrive_near, arrive_far, finish_sends = ring_of_four(all_ref, mix_out, mix_in)
+    tokens, columns = total_ref.shape[1:]
+    start, relay, arrive_near, arrive_far, finish_sends = ring_of_four(lin_ref, lin_out, lin_in)
     start()
-    columns = total_ref.shape[2]
-    weight_rows = rows_ref.shape[0] * rows_ref.shape[1] * rows_ref.shape[2]
-
-    def product(g):
-        weight = rows_ref[:, :, :, pl.ds(pl.multiple_of(g * 2 * PAIR, 2 * PAIR), 2 * PAIR)]
-        left = all_ref[g].reshape(FOUR * tokens, 2 * PAIR)
-        return dot(left, weight.reshape(weight_rows, 2 * PAIR), NT).reshape(FOUR, tokens, columns)
-
-    total_ref[...] = product(f)
-    relay()
-    arrive_near()
-    total_ref[...] += product((f + 1) % FOUR) + product((f + 3) % FOUR)
-    arrive_far()
-    total_ref[...] += product((f + 2) % FOUR)
+    with jax.named_scope("o_lin_wait"):
+        relay()
+        arrive_near()
+        arrive_far()
     half = tokens // 2
     theirs = pl.ds(pl.multiple_of((1 - c) * half, half), half)
     ours = pl.ds(pl.multiple_of(c * half, half), half)
-    half_copy = pltpu.make_async_remote_copy(
-        src_ref=total_ref.at[:, theirs, :], dst_ref=other_ref, send_sem=half_out, recv_sem=half_in,
-        device_id={"tp": 1 - c}, device_id_type=MESH,
-    )
-    half_copy.start()
-    half_copy.wait_recv()
-    ready_ref[...] = (total_ref[:, ours, :] + other_ref[...]).astype(BF)
-
-    def back_copy(k, source):
-        g = (f + k) % FOUR
-        return pltpu.make_async_remote_copy(
-            src_ref=ready_ref.at[g], dst_ref=got_ref.at[source], send_sem=back_out.at[k], recv_sem=back_in.at[k],
-            device_id={"fs": g}, device_id_type=MESH,
-        )
-
-    for k in range(1, FOUR):
-        back_copy(k, f).start()
+
+    def half_copy(p):
+        return pltpu.make_async_remote_copy(
+            src_ref=total_ref.at[p, theirs, :], dst_ref=other_ref.at[p],
+            send_sem=half_out.at[p], recv_sem=half_in.at[p],
+            device_id={"tp": 1 - c}, device_id_type=MESH,
+        )
+
+    with jax.named_scope("o_lin"):
+        for p in range(FOUR):
+            joined = jnp.concatenate([lin_ref[g, p] for g in range(FOUR)], axis=1)
+            total_ref[p] += dot(joined, weight, NT)
+            half_copy(p).start()
+
+    def back_copy(target, source):
+        return pltpu.make_async_remote_copy(
+            src_ref=ready_ref.at[target], dst_ref=got_ref.at[source],
+            send_sem=back_out.at[target], recv_sem=back_in.at[source],
+            device_id={"fs": target}, device_id_type=MESH,
+        )
+
+    with jax.named_scope("o_half"):
+        for p in range(FOUR):
+            half_copy(p).wait_recv()
+            ready_ref[p] = (total_ref[p, ours, :] + other_ref[p]).astype(BF)
+
+            @pl.when(f != p)
+            def _():
+                back_copy(p, f).start()
+
     got_ref[f] = ready_ref[f]
     finish_sends()
-    half_copy.wait_send()
     wide = FOUR * PAIR
     source, target = iota((wide, wide), 0), iota((wide, wide), 1)
     place = source % PAIR // 16 * (FOUR * 16) + source // PAIR * 16 + source % 16
     shuffle = ones_where(place == target)
-    for k in range(1, FOUR):
-        back_copy(k, (f + FOUR - k) % FOUR).wait_recv()
-    for b in range(columns // PAIR):
-        lanes = slice(b * PAIR, (b + 1) * PAIR)
-        joined = jnp.concatenate([got_ref[g, :, lanes] for g in range(FOUR)], axis=1)
-        out_ref[:, b * wide : (b + 1) * wide] = dot(joined, shuffle).astype(BF)
-    for k in range(1, FOUR):
-        back_copy(k, f).wait_send()
+    with jax.named_scope("o_back"):
+        for k in range(1, FOUR):
+            back_copy((f + k) % FOUR, (f + k) % FOUR).wait_recv()
+    with jax.named_scope("o_shuffle"):
+        for b in range(columns // PAIR):
+            lanes = slice(b * PAIR, (b + 1) * PAIR)
+            joined = jnp.concatenate([got_ref[g, :, lanes] for g in range(FOUR)], axis=1)
+            out_ref[:, b * wide : (b + 1) * wide] = dot(joined, shuffle).astype(BF)
+    with jax.named_scope("o_drain"):
+        for p in range(FOUR):
+            half_copy(p).wait_send()
+        for k in range(1, FOUR):
+            back_copy((f + k) % FOUR, f).wait_send()
 
 
 def layer_kernel(
@@ -794,22 +817,26 @@
     proj_ref, logd_ref, learn_ref, cos_ref, sin_ref, wout_ref,
     reads_ref, local_ref, msg_ref, rows_ref,
     recv_ref, sent_ref, enter_ref, halo_ref, comp_ref,
-    all_ref, total_ref, other_ref, ready_ref, got_ref,
+    lin_ref, att_ref, total_ref, other_ref, ready_ref, got_ref,
     load_sem, late_sem, x_out, x_in, hid_out, hid_in, stage_out, stage_in, ext_out, ext_in,
     z_out, z_in, near_out, near_in, far_out, far_in,
     wz_out, wz_in, wx_out, wx_in,
     out_sem, in_sem, back_out_sem, back_in_sem, halo_out_sem, halo_in_sem,
-    mix_out, mix_in, half_out, half_in, back_out, back_in,
+    lin_out, lin_in, att_out, att_in, half_out, half_in, back_out, back_in,
 ):
     place_of = tuple(lax.axis_index(a) for a in ("sp_0", "sp_1", "fs", "tp"))
+    for peer in neighbours(place_of):
+        pl.semaphore_signal(
+            pltpu.get_barrier_semaphore(), inc=1, device_id=peer, device_id_type=MESH
+        )
     pairs = (
         (down_d_hbm, down_d_ref), (down_e_hbm, down_e_ref), (up_d_hbm, up_d_ref), (up_e_hbm, up_e_ref),
         (init_hbm, init_ref),
     )
     late = [pltpu.make_async_copy(a, b, late_sem.at[k]) for k, (a, b) in enumerate(pairs)]
-    for g in range(FOUR):
-        for k, ref in enumerate((lin_out_ref, att_out_ref)):
-            wout_ref[:, (2 * g + k) * PAIR : (2 * g + k + 1) * PAIR] = ref[:, g * PAIR : (g + 1) * PAIR]
+    width = lin_out_ref.shape[1]
+    wout_ref[:, :width] = lin_out_ref[...]
+    wout_ref[:, width:] = att_out_ref[...]
     front(
         (
             x_ref, gain_ref, wr_ref, wk_ref, wv_ref, wq_ref, wak_ref, wav_ref, down_d_ref, down_e_ref,
@@ -823,12 +850,12 @@
     send_halo, send_maps, run = exchange(
         (
             msg_ref, init_ref, reads_ref, local_ref, head_gain_ref, proj_ref, cos_ref, sin_ref, sink_ref,
-            all_ref, recv_ref, sent_ref, enter_ref, halo_ref, comp_ref,
+            lin_ref, att_ref, recv_ref, sent_ref, enter_ref, halo_ref, comp_ref,
             out_sem, in_sem, back_out_sem, back_in_sem, halo_out_sem, halo_in_sem,
         ),
         place_of,
     )
-    local_maps(
+    await_rows = local_maps(
         (
             proj_ref, logd_ref, learn_ref, wout_ref, reads_ref, local_ref, msg_ref, rows_ref,
             wz_out, wz_in, wx_out, wx_in,
@@ -837,13 +864,34 @@
         send_halo,
         send_maps,
     )
-    run()
+    att_ring = ring_of_four(att_ref, att_out, att_in)
+    width = wout_ref.shape[1] // 2
+    columns = total_ref.shape[2]
+
+    def weights(first):
+        return rows_ref[:, :, :, first : first + width].reshape(columns, width)
+
+    def after_chain():
+        start, relay, arrive_near, arrive_far, finish_sends = att_ring
+        with jax.named_scope("o_att_wait"):
+            relay()
+            await_rows()
+            arrive_near()
+            arrive_far()
+        with jax.named_scope("o_att"):
+            for p in range(FOUR):
+                joined = jnp.concatenate([att_ref[g, p] for g in range(FOUR)], axis=1)
+                total_ref[p] = dot(joined, weights(width), NT)
+
+    run(att_ring[0], after_chain)
+    att_ring[4]()
     project_out(
         (
-            rows_ref, out_ref, all_ref, total_ref, other_ref, ready_ref, got_ref,
-            mix_out, mix_in, half_out, half_in, back_out, back_in,
+            out_ref, lin_ref, total_ref, other_ref, ready_ref, got_ref,
+            lin_out, lin_in, half_out, half_in, back_out, back_in,
         ),
         place_of,
+        weights(0),
     )
 
 
@@ -899,7 +947,8 @@
             space(BF, places, 16, PAIR),
             space(BF, 2, FOUR, tokens, PAIR),
             space(F32, 4, places // 4, 3 * HD // 2, HD),
-            space(BF, FOUR, FOUR, tokens, 2 * PAIR),
+            space(BF, FOUR, FOUR, tokens, PAIR),
+            space(BF, FOUR, FOUR, tokens, PAIR),
             space(F32, FOUR, tokens, columns),
             space(F32, FOUR, tokens // 2, columns),
             space(BF, FOUR, tokens // 2, columns),
@@ -909,10 +958,10 @@
             dma((2, nz // 2)), dma((2, nz // 2)), dma((nz, 2)), dma((nz, 2)), dma((nz,)), dma((nz,)),
             dma((nz,)), dma((nz,)), dma((nx,)), dma((nx,)),
             dma((places,)), dma((places,)), dma((places,)), dma((places,)), dma((2,)), dma((2,)),
-            dma((6,)), dma((6,)), dma, dma, dma((FOUR,)), dma((FOUR,)),
+            dma((6,)), dma((6,)), dma((6,)), dma((6,)), dma((FOUR,)), dma((FOUR,)), dma((FOUR,)), dma((FOUR,)),
         ],
         compiler_params=pltpu.CompilerParams(
-            collective_id=0, has_side_effects=True, vmem_limit_bytes=48 * 2**20
+            collective_id=0, has_side_effects=True, vmem_limit_bytes=63 * 2**20
         ),
         name="layer",
     )(

time: 123 us -> 99 us (0.80)
  local copies, waits for them, and re-layouts: 15.3 us -> 1.67 us
  Pallas kernels: 106 us -> 97.1 us
    unnamed x41 -> x1, local copies, waits for them, and re-layouts: 15.3 us -> 1.67 us
    pallas_call x1, Pallas kernels: 106 us -> 97.1 us  [local(): pl.pallas_call(layer_kernel, out_shape=jax.ShapeDtypeStruct((tokens // 2,...]
where the time goes in v5:
time: 99 us; the launch traced here: 98.8 us
  Pallas kernels  97.1 us (98%)
  local copies, waits for them, and re-layouts  1.67 us (2%)
    pallas_call x1, Pallas kernels, local(): pl.pallas_call(layer_kernel, out_shape=jax.ShapeDtypeStruct((tokens // 2,...  97.1 us

profile of v5, /device:TPU:1, one launch (start us, length us, event | category | flops | bytes accessed | tf_op | source)
XLA Modules:
  0.0 98.8 jit_solution(3292641018433893846)
XLA Ops:
  0.0 97.1 %layer.1 = bf16[64,2048]{1,0:T(8,128)(2,1)} custom-call(bf16[128,1024]{1,0:T(8,128)(2,1)} %bitcast.11, f32[1,2048]{1,0:T(1,128)} %bitcast.14, bf16[16,512]{1,0:T(8,128)(2,1)} %wr_ref.1, bf16[16,512]{1,0:T(8,128)(2,1)} %wk_ref.1, bf16[16,512]{1,0:T(8,128)(2,1)} %wv_ref.1, bf16[16,512]{1,0:T(8,128)(2,1)} %wq_ref.1, bf16[16,128]{1,0:T(8,128)(2,1)} %wak_ref.1, ...), custom_call_target="tpu_custom_call" | custom-call | tf_op jit(solution)/shard_map/layer/pallas_call | solution.py:919
  97.1 1.7 %copy.22 = bf16[1,64,2048]{2,1,0:T(8,128)(2,1)} copy(bf16[1,64,2048]{2,1,0:T(8,128)(2,1)} %bitcast.8) | data formatting | bytes 524288

commit v6 on v5

--- a/solution.py
+++ b/solution.py
@@ -17,6 +17,7 @@
 ATT_BLOCK = 128
 SP = ("sp_0", "sp_1")
 FOUR = 4
+ROUND = 2
 SP_FS = ("sp_0", "sp_1", "fs")
 SP_TP = ("sp_0", "sp_1", "tp")
 NORM_EPS = 1e-06
@@ -81,45 +82,54 @@
     return jnp.where(cond, 1.0, 0.0).astype(BF)
 
 
-def ring_of_four(buf, out_sem, in_sem):
+def settle(where, sem):
+    pltpu.make_async_copy(where, where, sem).wait()
+
+
+def ring_of_four(buf, out_sem, in_sem, give_ref=None, core=None):
     me = lax.axis_index("fs")
     right, left, far = (me + 1) % FOUR, (me + 3) % FOUR, (me + 2) % FOUR
     half = buf.shape[1] // 2
+    near_buf = buf if give_ref is None else give_ref[1]
 
     def piece(block, part, target, number):
         where = buf.at[block, part * half : (part + 1) * half]
         return pltpu.make_async_remote_copy(
-            src_ref=where, dst_ref=where, send_sem=out_sem.at[number], recv_sem=in_sem.at[number],
+            src_ref=where, dst_ref=where, send_sem=out_sem.at[0], recv_sem=in_sem.at[number],
             device_id={"fs": target}, device_id_type=MESH,
         )
 
+    def launch(part, target, number):
+        if give_ref is None:
+            piece(me, part, target, number).start()
+            return
+        rows = slice(part * half, (part + 1) * half)
+        pltpu.make_async_remote_copy(
+            src_ref=give_ref[0].at[rows], dst_ref=near_buf.at[me, rows],
+            send_sem=out_sem.at[0], recv_sem=in_sem.at[number],
+            device_id={"fs": target, "tp": core}, device_id_type=MESH,
+        ).start()
+
     def start():
-        piece(me, 0, right, 0).start()
-        piece(me, 1, left, 1).start()
-        piece(me, 1, right, 2).start()
-        piece(me, 0, left, 3).start()
+        launch(0, right, 0)
+        launch(1, left, 1)
+        launch(1, right, 2)
+        launch(0, left, 2)
 
     def relay():
         piece(left, 0, right, 0).wait_recv()
-        piece(left, 0, right, 4).start()
+        piece(left, 0, right, 3).start()
         piece(right, 1, left, 1).wait_recv()
-        piece(right, 1, left, 5).start()
+        piece(right, 1, left, 3).start()
 
     def arrive_near():
-        piece(left, 1, right, 2).wait_recv()
-        piece(right, 0, left, 3).wait_recv()
+        settle(buf.at[0], in_sem.at[2])
 
     def arrive_far():
-        piece(far, 0, right, 4).wait_recv()
-        piece(far, 1, left, 5).wait_recv()
+        settle(buf.at[0], in_sem.at[3])
 
     def finish_sends():
-        piece(me, 0, right, 0).wait_send()
-        piece(me, 1, left, 1).wait_send()
-        piece(me, 1, right, 2).wait_send()
-        piece(me, 0, left, 3).wait_send()
-        piece(left, 0, right, 4).wait_send()
-        piece(right, 1, left, 5).wait_send()
+        settle(buf.at[0:3], out_sem.at[0])
 
     return start, relay, arrive_near, arrive_far, finish_sends
 
@@ -150,13 +160,45 @@
     sin_ref[...] = jnp.sin(angle)
 
 
+def share(ref, give_ref, ring_sems, give_sems, place_of):
+    f, c = place_of[2:]
+    own = ring_of_four(ref.at[c], *ring_sems[0])
+    other = ring_of_four(ref.at[1 - c], *ring_sems[1], (give_ref, ref.at[c]), 1 - c)
+
+    def give(core):
+        return pltpu.make_async_remote_copy(
+            src_ref=give_ref, dst_ref=ref.at[core, f], send_sem=give_sems[0], recv_sem=give_sems[1],
+            device_id={"tp": 1 - c}, device_id_type=MESH,
+        )
+
+    def start():
+        own[0]()
+        other[0]()
+        give(c).start()
+
+    def collect():
+        own[1]()
+        other[1]()
+        give(1 - c).wait_recv()
+        for ring in (own, other):
+            ring[2]()
+            ring[3]()
+
+    def drain():
+        give(c).wait_send()
+        own[4]()
+        other[4]()
+
+    return start, collect, drain
+
+
 def front(refs, place_of):
     (
         x_ref, gain_ref, wr_ref, wk_ref, wv_ref, wq_ref, wak_ref, wav_ref, down_d_ref, down_e_ref,
         up_d_ref, up_e_ref, off_d_ref, off_e_ref, extra_ref, proj_ref, logd_ref, learn_ref,
         both_ref, hid_ref, stage_ref, cols_ref, ext_ref, load_sem,
         x_out, x_in, hid_out, hid_in, stage_out, stage_in, ext_out, ext_in,
-        z_out, z_in, near_out, near_in, far_out, far_in, cos_ref, sin_ref, late,
+        ring_out, z_in, near_in, far_in, cos_ref, sin_ref, late, start_rows,
     ) = refs
     z, x, f, c = place_of
     nz, nx = lax.axis_size("sp_0"), lax.axis_size("sp_1")
@@ -165,12 +207,10 @@
     loads = []
     for g in range(FOUR):
         for k, ref in enumerate((wr_ref, wk_ref, wv_ref, wq_ref)):
-            loads.append((ref.at[:, g * PAIR : (g + 1) * PAIR], stage_ref.at[g, :, k * PAIR : (k + 1) * PAIR]))
-    loads.append((x_ref, both_ref.at[c]))
-    loads.append((extra_ref.at[0], ext_ref.at[f]))
-    loads = [
-        pltpu.make_async_copy(start, end, load_sem.at[number]) for number, (start, end) in enumerate(loads)
-    ]
+            loads.append((ref.at[:, g * PAIR : (g + 1) * PAIR], stage_ref.at[g, :, k * PAIR : (k + 1) * PAIR], 0))
+    loads.append((x_ref, both_ref.at[c], 1))
+    loads.append((extra_ref.at[0], ext_ref.at[f], 2))
+    loads = [pltpu.make_async_copy(start, end, load_sem.at[number]) for start, end, number in loads]
     for load in loads:
         load.start()
     for load in late:
@@ -184,7 +224,8 @@
     for g in range(FOUR):
         stage_ref[g, :, 4 * PAIR :] = shared[g // 2]
     with jax.named_scope("f_load"):
-        for load in loads:
+        settle(stage_ref.at[:, :, : 4 * PAIR], load_sem.at[0])
+        for load in loads[-2:]:
             load.wait()
     my_rows = pl.ds(pl.multiple_of(f * rows, rows), rows)
     cols_ref[mine, my_rows, :] = stage_ref[f]
@@ -201,20 +242,13 @@
         g = (f + k) % FOUR
         return pltpu.make_async_remote_copy(
             src_ref=stage_ref.at[g], dst_ref=cols_ref.at[mine, my_rows, :],
-            send_sem=stage_out.at[k], recv_sem=stage_in.at[k], device_id={"fs": g}, device_id_type=MESH,
-        )
-
-    def stage_arrival(k):
-        g = (f + FOUR - k) % FOUR
-        return pltpu.make_async_remote_copy(
-            src_ref=stage_ref.at[g], dst_ref=cols_ref.at[mine, pl.ds(pl.multiple_of(g * rows, rows), rows), :],
-            send_sem=stage_out.at[k], recv_sem=stage_in.at[k], device_id={"fs": g}, device_id_type=MESH,
+            send_sem=stage_out, recv_sem=stage_in, device_id={"fs": g}, device_id_type=MESH,
         )
 
     def ext_copy(k, source):
         return pltpu.make_async_remote_copy(
             src_ref=ext_ref.at[source], dst_ref=ext_ref.at[source],
-            send_sem=ext_out.at[k], recv_sem=ext_in.at[k], device_id={"fs": (f + k) % FOUR}, device_id_type=MESH,
+            send_sem=ext_out, recv_sem=ext_in, device_id={"fs": (f + k) % FOUR}, device_id_type=MESH,
         )
 
     for k in range(1, FOUR):
@@ -229,38 +263,36 @@
     def z_copy(k_from, side, step):
         where = cols_ref.at[z_block(k_from) * nx + x]
         return pltpu.make_async_remote_copy(
-            src_ref=where, dst_ref=where, send_sem=z_out.at[side, step], recv_sem=z_in.at[side, step],
+            src_ref=where, dst_ref=where, send_sem=ring_out, recv_sem=z_in.at[side, step],
             device_id={"sp_0": (z + (1 if side == 0 else nz - 1)) % nz}, device_id_type=MESH,
         )
 
     def near_copy(k, side, column):
         where = cols_ref.at[z_block(k) * nx + column]
         return pltpu.make_async_remote_copy(
-            src_ref=where, dst_ref=where, send_sem=near_out.at[k, side], recv_sem=near_in.at[k, side],
+            src_ref=where, dst_ref=where, send_sem=ring_out, recv_sem=near_in.at[k],
             device_id={"sp_1": (x + (1 if side == 0 else nx - 1)) % nx}, device_id_type=MESH,
         )
 
     def far_copy(k, column):
         where = cols_ref.at[z_block(k) * nx + column]
         return pltpu.make_async_remote_copy(
-            src_ref=where, dst_ref=where, send_sem=far_out.at[k], recv_sem=far_in.at[k],
+            src_ref=where, dst_ref=where, send_sem=ring_out, recv_sem=far_in,
             device_id={"sp_1": (x + (1 if k % 2 == 0 else nx - 1)) % nx}, device_id_type=MESH,
         )
 
-    left, right, across = (x + nx - 1) % nx, (x + 1) % nx, (x + 2) % nx
+    left, right, _ = (x + nx - 1) % nx, (x + 1) % nx, 0
 
     def spread(k):
         near_copy(k, 0, x).start()
         near_copy(k, 1, x).start()
 
     def pass_on(k):
-        near_copy(k, 0, left).wait_recv()
-        near_copy(k, 1, right).wait_recv()
+        settle(cols_ref.at[0:2], near_in.at[k])
         far_copy(k, left if k % 2 == 0 else right).start()
 
     with jax.named_scope("f_stage_wait"):
-        for k in range(1, FOUR):
-            stage_arrival(k).wait_recv()
+        settle(stage_ref.at[1:FOUR], stage_in)
     z_copy(0, 0, 0).start()
     z_copy(0, 1, 0).start()
     spread(0)
@@ -299,11 +331,11 @@
                 relay()
     with jax.named_scope("f_pass_last"):
         pass_on(nz - 1)
+    start_rows()
     with jax.named_scope("f_hid_wait"):
         arrive_near()
         arrive_far()
-        for k in range(1, FOUR):
-            ext_copy(k, (f + FOUR - k) % FOUR).wait_recv()
+        settle(ext_ref.at[1:FOUR], ext_in)
 
     for load in late:
         load.wait()
@@ -334,8 +366,7 @@
                 learn_ref[d, p] = learn[part]
 
     with jax.named_scope("f_far_wait"):
-        for k in range(nz):
-            far_copy(k, across).wait_recv()
+        settle(cols_ref.at[0:nz], far_in)
     depth = cols_ref.shape[0] * cols_ref.shape[1]
     with jax.named_scope("f_proj"):
         for first_col, last_col in ((0, 256), (256, 512), (512, 640)):
@@ -346,17 +377,9 @@
 
     half_copy.wait_send()
     finish_sends()
-    for k in range(1, FOUR):
-        stage_copy(k).wait_send()
-        ext_copy(k, f).wait_send()
-    for step in range(steps):
-        z_copy(0, 0, step).wait_send()
-        if step < steps - 1:
-            z_copy(0, 1, step).wait_send()
-    for k in range(nz):
-        near_copy(k, 0, x).wait_send()
-        near_copy(k, 1, x).wait_send()
-        far_copy(k, left).wait_send()
+    settle(stage_ref.at[1:FOUR], stage_out)
+    settle(ext_ref.at[1:FOUR], ext_out)
+    settle(cols_ref.at[0 : 4 * nz - 1], ring_out)
 
 
 def stacked(x):
@@ -368,27 +391,69 @@
     return x[:CH] + x[CH:]
 
 
-def local_maps(refs, place_of, send_halo, send_maps):
-    proj_ref, logd_ref, learn_ref, wout_ref, q_ref, o_ref, msg_ref, rows_ref, z_out, z_in, x_out, x_in = refs
-    z, x = place_of[:2]
+def gather_rows(refs, place_of):
+    wout_ref, rows_ref, z_out, z_in, x_out, x_in, c_out, c_in = refs
+    z, x, _, c = place_of
     nz, nx = lax.axis_size("sp_0"), lax.axis_size("sp_1")
-    rows_ref[z, x] = wout_ref[...]
+    half = nz // 2
+    left, right, across = (x + nx - 1) % nx, (x + 1) % nx, (x + 2) % nx
 
     def z_copy(k, source):
         return pltpu.make_async_remote_copy(
-            src_ref=wout_ref, dst_ref=rows_ref.at[source, x], send_sem=z_out.at[k], recv_sem=z_in.at[k],
+            src_ref=wout_ref, dst_ref=rows_ref.at[c, source, x], send_sem=z_out, recv_sem=z_in,
             device_id={"sp_0": (z + k) % nz}, device_id_type=MESH,
         )
 
-    def x_copy(k, column):
-        where = rows_ref.at[:, column]
-        return pltpu.make_async_remote_copy(
-            src_ref=where, dst_ref=where, send_sem=x_out.at[k], recv_sem=x_in.at[k],
-            device_id={"sp_1": (x + k) % nx}, device_id_type=MESH,
-        )
-
-    for k in range(1, nz):
-        z_copy(k, z).start()
+    def x_copy(number, column):
+        part = slice(0, nz) if number < 2 else slice(0, half) if number == 2 else slice(half, nz)
+        where = rows_ref.at[c, part, column]
+        return pltpu.make_async_remote_copy(
+            src_ref=where, dst_ref=where, send_sem=x_out, recv_sem=x_in.at[min(number, 2)],
+            device_id={"sp_1": right if number % 2 == 0 else left}, device_id_type=MESH,
+        )
+
+    def c_copy(number, core, column):
+        where = rows_ref.at[core, :, column]
+        return pltpu.make_async_remote_copy(
+            src_ref=where, dst_ref=where, send_sem=c_out, recv_sem=c_in,
+            device_id={"tp": 1 - c}, device_id_type=MESH,
+        )
+
+    def first():
+        rows_ref[c, z, x] = wout_ref[...]
+        for k in range(1, nz):
+            z_copy(k, z).start()
+
+    def second():
+        settle(rows_ref.at[c, 1:nz, x], z_in)
+        x_copy(0, x).start()
+        x_copy(1, x).start()
+        c_copy(0, c, x).start()
+
+    def third():
+        x_copy(0, left).wait_recv()
+        x_copy(2, left).start()
+        x_copy(1, right).wait_recv()
+        x_copy(3, right).start()
+        c_copy(1, c, left).start()
+        c_copy(2, c, right).start()
+
+    def fourth():
+        settle(rows_ref.at[c, :, across], x_in.at[2])
+        c_copy(3, c, across).start()
+
+    def last():
+        settle(rows_ref.at[1 - c], c_in)
+        settle(rows_ref.at[c], c_out)
+        settle(rows_ref.at[c, 1:nz, x], z_out)
+        settle(rows_ref.at[c, :, 1:nx], x_out)
+
+    return first, second, third, fourth, last
+
+
+def local_maps(refs, send_halo, send_maps, rows_steps):
+    proj_ref, logd_ref, learn_ref, q_ref, o_ref, msg_ref = refs
+    rows_steps[1]()
     row = iota((2 * CH, 2 * CH), 0)
     col = iota((2 * CH, 2 * CH), 1)
     t, s = row % CH, col % CH
@@ -398,51 +463,48 @@
     strict = [t > s, t < s]
     within = [t >= s, t <= s]
 
-    def one_pair(p, carry):
-        @pl.when(p == 1)
+    def one_round(it, carry):
+        @pl.when(it == 1)
         def _():
+            for u in range(ROUND):
+                send_maps(u)
             send_halo()
 
-        @pl.when(p == FOUR // 2)
-        def _():
-            for k in range(1, nz):
-                z_copy(k, (z + nz - k) % nz).wait_recv()
-            for k in range(1, nx):
-                x_copy(k, x).start()
-
-        recept = proj_ref[p, :, :PAIR].astype(F32)
-        keys = proj_ref[p, :, PAIR : 2 * PAIR].astype(F32)
-        values = proj_ref[p, :, 2 * PAIR : 3 * PAIR].astype(F32)
-        squares = mm2(keys * keys, same_head)
-        unit = keys * lax.rsqrt(squares + NORM_EPS)
-        jobs = [(d, c) for d in range(2) for c in range(2)]
+        seqs = [it * ROUND + u for u in range(ROUND)]
+        recept, keys, values, unit = {}, {}, {}, {}
+        for u, p in enumerate(seqs):
+            recept[u] = proj_ref[p, :, :PAIR].astype(F32)
+            keys[u] = proj_ref[p, :, PAIR : 2 * PAIR].astype(F32)
+            values[u] = proj_ref[p, :, 2 * PAIR : 3 * PAIR].astype(F32)
+            unit[u] = keys[u] * lax.rsqrt(mm2(keys[u] * keys[u], same_head) + NORM_EPS)
+        jobs = [(u, d, c) for u in range(ROUND) for d in range(2) for c in range(2)]
         stage = {}
-        for d, c in jobs:
+        for u, d, c in jobs:
             rows = slice(c * CH, (c + 1) * CH)
-            logd = logd_ref[d, p, rows, :]
+            logd = logd_ref[d, seqs[u], rows, :]
             parts = jnp.concatenate(split3(logd), axis=0)
             total = dot(jnp.concatenate([tri[d]] * 3, axis=1), parts)
             middle = total[CH // 2 - 1 : CH // 2] if d == 0 else total[CH // 2 : CH // 2 + 1]
             last = total[CH - 1 : CH] if d == 0 else total[0:1]
             grow = jnp.exp(total - middle)
             shrink = jnp.exp(middle - total)
-            read = recept[rows] * grow
-            mark = unit[rows] * jnp.exp(total - logd - middle)
-            erase = unit[rows] * learn_ref[d, p, rows, :] * shrink
-            key = keys[rows] * shrink
+            read = recept[u][rows] * grow
+            mark = unit[u][rows] * jnp.exp(total - logd - middle)
+            erase = unit[u][rows] * learn_ref[d, seqs[u], rows, :] * shrink
+            key = keys[u][rows] * shrink
             read_s, mark_s, erase_s, key_s = map(stacked, (read, mark, erase, key))
             scores = mm3(
                 jnp.concatenate([mark_s, read_s], axis=0),
                 jnp.concatenate([erase_s, key_s], axis=0),
                 NT,
             )
-            stage[d, c] = (read, mark_s, erase_s, key_s, scores, jnp.exp(middle), jnp.exp(last - middle), jnp.exp(last))
+            stage[u, d, c] = (read, mark_s, erase_s, key_s, scores, jnp.exp(middle), jnp.exp(last - middle), jnp.exp(last))
         inverse = {}
         grams = {}
-        for d, c in jobs:
-            gram = jnp.where(strict[d], stage[d, c][4][: 2 * CH, : 2 * CH], 0.0)
-            grams[d, c] = gram
-            inverse[d, c] = jnp.where(eye, 1.0, 0.0) - jnp.where(t // 2 == s // 2, gram, 0.0)
+        for u, d, c in jobs:
+            gram = jnp.where(strict[d], stage[u, d, c][4][: 2 * CH, : 2 * CH], 0.0)
+            grams[u, d, c] = gram
+            inverse[u, d, c] = jnp.where(eye, 1.0, 0.0) - jnp.where(t // 2 == s // 2, gram, 0.0)
         block = 2
         while block < CH:
             joins = (t // (2 * block) == s // (2 * block)) & (t // block != s // block)
@@ -451,67 +513,56 @@
                 inverse[job] = found - mm3(found, mm3(jnp.where(joins, grams[job], 0.0), found))
             block *= 2
         maps, reads, outs = {}, {}, {}
-        for d, c in jobs:
+        for u, d, c in jobs:
             rows = slice(c * CH, (c + 1) * CH)
-            read, mark_s, erase_s, key_s, scores, to_start, to_end, whole = stage[d, c]
-            val_s = stacked(values[rows]).astype(BF)
+            read, mark_s, erase_s, key_s, scores, to_start, to_end, whole = stage[u, d, c]
+            val_s = stacked(values[u][rows]).astype(BF)
             cross = jnp.where(strict[d], scores[: 2 * CH, 2 * CH :], 0.0)
             read_e = jnp.where(within[d], scores[2 * CH :, : 2 * CH], 0.0)
             read_k = jnp.where(within[d], scores[2 * CH :, 2 * CH :], 0.0)
-            solved = mm3(inverse[d, c], jnp.concatenate([mark_s, mm2(cross, val_s)], axis=1))
+            solved = mm3(inverse[u, d, c], jnp.concatenate([mark_s, mm2(cross, val_s)], axis=1))
             solved = jnp.concatenate([solved[:, :PAIR] * to_start, solved[:, PAIR:]], axis=1)
             taken = mm3(read_e, solved)
-            reads[d, c] = read * to_start - unstacked(taken[:, :PAIR])
-            outs[d, c] = unstacked(mm2(read_k, val_s) - taken[:, PAIR:])
+            reads[u, d, c] = read * to_start - unstacked(taken[:, :PAIR])
+            outs[u, d, c] = unstacked(mm2(read_k, val_s) - taken[:, PAIR:])
             ended = mm3(solved, erase_s * to_end, TN)
             k_hi, k_lo = split2(key_s * to_end)
             added = dot(jnp.concatenate([val_s, val_s], axis=0), jnp.concatenate([k_hi, k_lo], axis=0), TN)
             prod = jnp.where(eye, whole - 1.0, 0.0) - ended[:PAIR]
-            maps[d, c] = (prod, added - ended[PAIR:])
-        out_rows = [outs[0, 0] + outs[1, 0], outs[0, 1] + outs[1, 1]]
-        for d in range(2):
-            first, second = (0, 1) if d == 0 else (1, 0)
-            (prod1, add1), (prod2, add2) = maps[d, first], maps[d, second]
-            both = jnp.concatenate([prod1, add1], axis=0)
-            through = mm3(reads[d, second], both, NT)
-            q_ref[d, p, first * CH : (first + 1) * CH, :] = reads[d, first]
-            q_ref[d, p, second * CH : (second + 1) * CH, :] = reads[d, second] + through[:, :PAIR]
-            out_rows[second] = out_rows[second] + through[:, PAIR:]
-            joined = mm3(both, prod2)
-            prod = prod1 + prod2 + joined[:PAIR]
-            add = add1 + joined[PAIR:] + add2
-            for hh in range(2):
-                for half in range(2):
-                    message = jnp.concatenate(
-                        [
-                            folded(prod, hh, hh * HD, HD // 2),
-                            folded(add, hh, hh * HD + half * (HD // 2), HD // 4),
-                        ],
-                        axis=0,
-                    )
-                    msg_ref[d * 16 + p * 4 + hh * 2 + half] = message.astype(msg_ref.dtype)
-        for c in range(2):
-            o_ref[p, c * CH : (c + 1) * CH, :] = out_rows[c]
-
-        @pl.when(p > 0)
-        def _():
-            send_maps(p - 1)
+            maps[u, d, c] = (prod, added - ended[PAIR:])
+        for u, p in enumerate(seqs):
+            out_rows = [outs[u, 0, 0] + outs[u, 1, 0], outs[u, 0, 1] + outs[u, 1, 1]]
+            for d in range(2):
+                first, second = (0, 1) if d == 0 else (1, 0)
+                (prod1, add1), (prod2, add2) = maps[u, d, first], maps[u, d, second]
+                both = jnp.concatenate([prod1, add1], axis=0)
+                through = mm3(reads[u, d, second], both, NT)
+                q_ref[d, p, first * CH : (first + 1) * CH, :] = reads[u, d, first]
+                q_ref[d, p, second * CH : (second + 1) * CH, :] = reads[u, d, second] + through[:, :PAIR]
+                out_rows[second] = out_rows[second] + through[:, PAIR:]
+                joined = mm3(both, prod2)
+                prod = prod1 + prod2 + joined[:PAIR]
+                add = add1 + joined[PAIR:] + add2
+                for hh in range(2):
+                    for half in range(2):
+                        message = jnp.concatenate(
+                            [
+                                folded(prod, hh, hh * HD, HD // 2),
+                                folded(add, hh, hh * HD + half * (HD // 2), HD // 4),
+                            ],
+                            axis=0,
+                        )
+                        msg_ref[d * 16 + p * 4 + hh * 2 + half] = message.astype(msg_ref.dtype)
+            for c in range(2):
+                o_ref[p, c * CH : (c + 1) * CH, :] = out_rows[c]
 
         return carry
 
     with jax.named_scope("l_loop"):
-        lax.fori_loop(0, FOUR, one_pair, 0)
-    send_maps(FOUR - 1)
-
-    def await_rows():
-        for k in range(1, nx):
-            x_copy(k, (x + nx - k) % nx).wait_recv()
-        for k in range(1, nz):
-            z_copy(k, z).wait_send()
-        for k in range(1, nx):
-            x_copy(k, x).wait_send()
-
-    return await_rows
+        lax.fori_loop(0, FOUR // ROUND, one_round, 0)
+    for u in range(ROUND):
+        send_maps(FOUR - ROUND + u)
+    rows_steps[2]()
 
 
 def folded(x, hh, first, count):
@@ -523,7 +574,7 @@
 
 def exchange(refs, place_of):
     (
-        msg_ref, init_ref, reads_ref, local_ref, gain_ref, proj_ref, cos_ref, sin_ref, sink_ref, lin_ref, att_ref,
+        msg_ref, init_ref, reads_ref, local_ref, gain_ref, proj_ref, cos_ref, sin_ref, sink_ref, lin_ref, att_ref, lin_give, att_give,
         recv_ref, sent_ref, enter_ref, halo_ref, comp_ref,
         out_sem, in_sem, back_out_sem, back_in_sem, halo_out_sem, halo_in_sem,
     ) = refs
@@ -536,8 +587,8 @@
         return pltpu.make_async_remote_copy(
             src_ref=proj_ref.at[:, :, kv_first : kv_first + PAIR],
             dst_ref=halo_ref.at[1 - side],
-            send_sem=halo_out_sem.at[side],
-            recv_sem=halo_in_sem.at[1 - side],
+            send_sem=halo_out_sem,
+            recv_sem=halo_in_sem,
             device_id=peer_id(target),
             device_id_type=MESH,
         )
@@ -546,39 +597,19 @@
         return pltpu.make_async_remote_copy(
             src_ref=msg_ref.at[target],
             dst_ref=recv_ref.at[place],
-            send_sem=out_sem.at[target],
-            recv_sem=in_sem.at[place],
+            send_sem=out_sem,
+            recv_sem=in_sem,
             device_id=peer_id(target),
             device_id_type=MESH,
         )
 
-    def map_arrival(source):
-        return pltpu.make_async_remote_copy(
-            src_ref=msg_ref.at[source],
-            dst_ref=recv_ref.at[source],
-            send_sem=out_sem.at[source],
-            recv_sem=in_sem.at[source],
-            device_id=peer_id(source),
-            device_id_type=MESH,
-        )
-
     def entry_copy(target):
         return pltpu.make_async_remote_copy(
             src_ref=sent_ref.at[target],
             dst_ref=enter_ref.at[place],
-            send_sem=back_out_sem.at[target],
-            recv_sem=back_in_sem.at[place],
+            send_sem=back_out_sem,
+            recv_sem=back_in_sem,
             device_id=peer_id(target),
-            device_id_type=MESH,
-        )
-
-    def entry_arrival(source):
-        return pltpu.make_async_remote_copy(
-            src_ref=sent_ref.at[source],
-            dst_ref=enter_ref.at[source],
-            send_sem=back_out_sem.at[source],
-            recv_sem=back_in_sem.at[source],
-            device_id=peer_id(source),
             device_id_type=MESH,
         )
 
@@ -598,8 +629,8 @@
     def run(after_attend, after_chain):
         tokens = local_ref.shape[1]
         with jax.named_scope("x_halo"):
-            for side in range(2):
-                halo_copy(side).wait()
+            settle(halo_ref, halo_in_sem)
+            settle(halo_ref, halo_out_sem)
         lane = iota((1, PAIR), 1)
         low = lane < HD
         front = lane % 32 < 16
@@ -633,7 +664,7 @@
             raised = jnp.exp(scores - top)
             total = jnp.exp(sink - top) + jnp.sum(raised, axis=-1, keepdims=True)
             mixed = dot((raised / total).astype(BF), value)
-            att_ref[pair, p] = jnp.where(low, mixed[:tokens], mixed[tokens:]).astype(BF)
+            keep(jnp.where(low, mixed[:tokens], mixed[tokens:]).astype(BF), place_of, p, att_ref, att_give)
             return carry
 
         with jax.named_scope("x_attend"):
@@ -642,12 +673,9 @@
         after_attend()
         recv_ref[place] = msg_ref[place]
 
-        def await_map(k, carry):
-            map_arrival((place + k) % count).wait()
-            return carry
-
         with jax.named_scope("x_await_map"):
-            lax.fori_loop(1, count, await_map, 0)
+            settle(recv_ref.at[1:count], in_sem)
+            settle(msg_ref.at[1:count], out_sem)
 
         unit_idx = place // 2
         direction, half = unit_idx // 8, place % 2
@@ -704,19 +732,23 @@
         dispatch(groups - 1)
         after_chain()
 
-        def await_entry(k, carry):
-            entry_arrival((place + k) % count).wait()
-            return carry
-
         with jax.named_scope("x_await_entry"):
-            lax.fori_loop(1, count, await_entry, 0)
+            settle(enter_ref.at[1:count], back_in_sem)
+            settle(sent_ref.at[1:count], back_out_sem)
         with jax.named_scope("x_finish"):
-            finish(reads_ref, local_ref, enter_ref, gain_ref, lin_ref.at[pair])
+            finish(reads_ref, local_ref, enter_ref, gain_ref, lin_ref, lin_give, place_of)
 
     return send_halo, send_maps, run
 
 
-def finish(q_ref, o_ref, enter_ref, gain_ref, mix_ref):
+def keep(value, place_of, p, mine_ref, give_ref):
+    f, c = place_of[2:]
+    half = value.shape[0] // 2
+    mine_ref[c, f, p] = jnp.where(c == 0, value[:half], value[half:])
+    give_ref[p] = jnp.where(c == 0, value[half:], value[:half])
+
+
+def finish(q_ref, o_ref, enter_ref, gain_ref, lin_ref, lin_give, place_of):
     row = iota((PAIR, PAIR), 0)
     col = iota((PAIR, PAIR), 1)
     same_head = ones_where(row // HD == col // HD)
@@ -738,74 +770,38 @@
             out = out + mm2(q_ref[d, p], jnp.concatenate(pieces, axis=0).astype(BF), NT)
         centred = out - mm2(out, same_head) * (1.0 / HD)
         spread = mm2(centred * centred, same_head) * (1.0 / HD)
-        mix_ref[p] = (centred * lax.rsqrt(spread + GROUP_EPS) * gain).astype(BF)
-
-
-def project_out(refs, place_of, weight):
-    (
-        out_ref, lin_ref, total_ref, other_ref, ready_ref, got_ref,
-        lin_out, lin_in, half_out, half_in, back_out, back_in,
-    ) = refs
-    f, c = place_of[2:]
-    tokens, columns = total_ref.shape[1:]
-    start, relay, arrive_near, arrive_far, finish_sends = ring_of_four(lin_ref, lin_out, lin_in)
-    start()
-    with jax.named_scope("o_lin_wait"):
-        relay()
-        arrive_near()
-        arrive_far()
-    half = tokens // 2
-    theirs = pl.ds(pl.multiple_of((1 - c) * half, half), half)
-    ours = pl.ds(pl.multiple_of(c * half, half), half)
-
-    def half_copy(p):
-        return pltpu.make_async_remote_copy(
-            src_ref=total_ref.at[p, theirs, :], dst_ref=other_ref.at[p],
-            send_sem=half_out.at[p], recv_sem=half_in.at[p],
-            device_id={"tp": 1 - c}, device_id_type=MESH,
-        )
-
-    with jax.named_scope("o_lin"):
-        for p in range(FOUR):
-            joined = jnp.concatenate([lin_ref[g, p] for g in range(FOUR)], axis=1)
-            total_ref[p] += dot(joined, weight, NT)
-            half_copy(p).start()
+        mix = (centred * lax.rsqrt(spread + GROUP_EPS) * gain).astype(BF)
+        keep(mix, place_of, p, lin_ref, lin_give)
+
+
+def send_back(refs, place_of):
+    out_ref, ready_ref, got_ref, back_out, back_in = refs
+    f = place_of[2]
+    columns = ready_ref.shape[2]
 
     def back_copy(target, source):
         return pltpu.make_async_remote_copy(
             src_ref=ready_ref.at[target], dst_ref=got_ref.at[source],
-            send_sem=back_out.at[target], recv_sem=back_in.at[source],
+            send_sem=back_out, recv_sem=back_in,
             device_id={"fs": target}, device_id_type=MESH,
         )
 
-    with jax.named_scope("o_half"):
-        for p in range(FOUR):
-            half_copy(p).wait_recv()
-            ready_ref[p] = (total_ref[p, ours, :] + other_ref[p]).astype(BF)
-
-            @pl.when(f != p)
-            def _():
-                back_copy(p, f).start()
-
+    for k in range(1, FOUR):
+        back_copy((f + k) % FOUR, f).start()
     got_ref[f] = ready_ref[f]
-    finish_sends()
     wide = FOUR * PAIR
     source, target = iota((wide, wide), 0), iota((wide, wide), 1)
     place = source % PAIR // 16 * (FOUR * 16) + source // PAIR * 16 + source % 16
     shuffle = ones_where(place == target)
     with jax.named_scope("o_back"):
-        for k in range(1, FOUR):
-            back_copy((f + k) % FOUR, (f + k) % FOUR).wait_recv()
+        settle(got_ref.at[1:FOUR], back_in)
     with jax.named_scope("o_shuffle"):
         for b in range(columns // PAIR):
             lanes = slice(b * PAIR, (b + 1) * PAIR)
             joined = jnp.concatenate([got_ref[g, :, lanes] for g in range(FOUR)], axis=1)
             out_ref[:, b * wide : (b + 1) * wide] = dot(joined, shuffle).astype(BF)
     with jax.named_scope("o_drain"):
-        for p in range(FOUR):
-            half_copy(p).wait_send()
-        for k in range(1, FOUR):
-            back_copy((f + k) % FOUR, f).wait_send()
+        settle(ready_ref.at[1:FOUR], back_out)
 
 
 def layer_kernel(
@@ -816,13 +812,13 @@
     both_ref, hid_ref, stage_ref, cols_ref, ext_ref, down_d_ref, down_e_ref, up_d_ref, up_e_ref, init_ref,
     proj_ref, logd_ref, learn_ref, cos_ref, sin_ref, wout_ref,
     reads_ref, local_ref, msg_ref, rows_ref,
-    recv_ref, sent_ref, enter_ref, halo_ref, comp_ref,
-    lin_ref, att_ref, total_ref, other_ref, ready_ref, got_ref,
+    recv_ref, sent_ref, enter_ref, halo_ref, comp_ref, total_ref,
+    lin_ref, att_ref, lin_give, att_give, ready_ref, got_ref,
     load_sem, late_sem, x_out, x_in, hid_out, hid_in, stage_out, stage_in, ext_out, ext_in,
-    z_out, z_in, near_out, near_in, far_out, far_in,
-    wz_out, wz_in, wx_out, wx_in,
+    ring_out, z_in, near_in, far_in,
+    wz_out, wz_in, wx_out, wx_in, wc_out, wc_in,
     out_sem, in_sem, back_out_sem, back_in_sem, halo_out_sem, halo_in_sem,
-    lin_out, lin_in, att_out, att_in, half_out, half_in, back_out, back_in,
+    lin_out, lin_in, lin_out2, lin_in2, att_out, att_in, att_out2, att_in2, give_sem, back_out, back_in,
 ):
     place_of = tuple(lax.axis_index(a) for a in ("sp_0", "sp_1", "fs", "tp"))
     for peer in neighbours(place_of):
@@ -837,62 +833,72 @@
     width = lin_out_ref.shape[1]
     wout_ref[:, :width] = lin_out_ref[...]
     wout_ref[:, width:] = att_out_ref[...]
+    rows_steps = gather_rows(
+        (wout_ref, rows_ref, wz_out, wz_in, wx_out, wx_in, wc_out, wc_in), place_of
+    )
     front(
         (
             x_ref, gain_ref, wr_ref, wk_ref, wv_ref, wq_ref, wak_ref, wav_ref, down_d_ref, down_e_ref,
             up_d_ref, up_e_ref, off_d_ref, off_e_ref, extra_ref, proj_ref, logd_ref, learn_ref,
             both_ref, hid_ref, stage_ref, cols_ref, ext_ref, load_sem,
             x_out, x_in, hid_out, hid_in, stage_out, stage_in, ext_out, ext_in,
-            z_out, z_in, near_out, near_in, far_out, far_in, cos_ref, sin_ref, late,
+            ring_out, z_in, near_in, far_in, cos_ref, sin_ref, late, rows_steps[0],
         ),
         place_of,
     )
     send_halo, send_maps, run = exchange(
         (
             msg_ref, init_ref, reads_ref, local_ref, head_gain_ref, proj_ref, cos_ref, sin_ref, sink_ref,
-            lin_ref, att_ref, recv_ref, sent_ref, enter_ref, halo_ref, comp_ref,
+            lin_ref, att_ref, lin_give, att_give, recv_ref, sent_ref, enter_ref, halo_ref, comp_ref,
             out_sem, in_sem, back_out_sem, back_in_sem, halo_out_sem, halo_in_sem,
         ),
         place_of,
     )
-    await_rows = local_maps(
-        (
-            proj_ref, logd_ref, learn_ref, wout_ref, reads_ref, local_ref, msg_ref, rows_ref,
-            wz_out, wz_in, wx_out, wx_in,
-        ),
-        place_of,
+    local_maps(
+        (proj_ref, logd_ref, learn_ref, reads_ref, local_ref, msg_ref),
         send_halo,
         send_maps,
-    )
-    att_ring = ring_of_four(att_ref, att_out, att_in)
-    width = wout_ref.shape[1] // 2
-    columns = total_ref.shape[2]
-
-    def weights(first):
-        return rows_ref[:, :, :, first : first + width].reshape(columns, width)
+        rows_steps,
+    )
+    att_share = share(
+        att_ref, att_give, ((att_out, att_in), (att_out2, att_in2)), (give_sem.at[0], give_sem.at[1]), place_of
+    )
+    lin_share = share(
+        lin_ref, lin_give, ((lin_out, lin_in), (lin_out2, lin_in2)), (give_sem.at[2], give_sem.at[3]), place_of
+    )
+    columns = ready_ref.shape[2]
+    joined_rows = FOUR * ready_ref.shape[1]
+
+    def product(ref, first):
+        result = None
+        for core in range(2):
+            left = jnp.concatenate([ref[core, g].reshape(joined_rows, PAIR) for g in range(FOUR)], axis=1)
+            weight = rows_ref[core, :, :, :, first : first + width].reshape(columns, width)
+            term = dot(left, weight, NT)
+            result = term if result is None else result + term
+        return result
 
     def after_chain():
-        start, relay, arrive_near, arrive_far, finish_sends = att_ring
         with jax.named_scope("o_att_wait"):
-            relay()
-            await_rows()
-            arrive_near()
-            arrive_far()
+            att_share[1]()
+            rows_steps[4]()
         with jax.named_scope("o_att"):
-            for p in range(FOUR):
-                joined = jnp.concatenate([att_ref[g, p] for g in range(FOUR)], axis=1)
-                total_ref[p] = dot(joined, weights(width), NT)
-
-    run(att_ring[0], after_chain)
-    att_ring[4]()
-    project_out(
-        (
-            out_ref, lin_ref, total_ref, other_ref, ready_ref, got_ref,
-            lin_out, lin_in, half_out, half_in, back_out, back_in,
-        ),
-        place_of,
-        weights(0),
-    )
+            total_ref[...] = product(att_ref, width)
+
+    def after_attend():
+        att_share[0]()
+        rows_steps[3]()
+
+    run(after_attend, after_chain)
+    lin_share[0]()
+    att_share[2]()
+    with jax.named_scope("o_lin_wait"):
+        lin_share[1]()
+    with jax.named_scope("o_lin"):
+        result = (total_ref[...] + product(lin_ref, 0)).astype(BF)
+        ready_ref[...] = result.reshape(ready_ref.shape)
+    send_back((out_ref, ready_ref, got_ref, back_out, back_in), place_of)
+    lin_share[2]()
 
 
 def local(
@@ -941,24 +947,25 @@
             space(F32, 2, FOUR, tokens, PAIR),
             space(F32, FOUR, tokens, PAIR),
             space(BF, places, 48, PAIR),
-            space(BF, nz, nx, out_rows, 2 * FOUR * PAIR),
+            space(BF, 2, nz, nx, out_rows, 2 * FOUR * PAIR),
             space(BF, places, 48, PAIR),
             space(BF, places, 16, PAIR),
             space(BF, places, 16, PAIR),
             space(BF, 2, FOUR, tokens, PAIR),
             space(F32, 4, places // 4, 3 * HD // 2, HD),
-            space(BF, FOUR, FOUR, tokens, PAIR),
-            space(BF, FOUR, FOUR, tokens, PAIR),
-            space(F32, FOUR, tokens, columns),
-            space(F32, FOUR, tokens // 2, columns),
+            space(F32, FOUR * tokens // 2, columns),
+            space(BF, 2, FOUR, FOUR, tokens // 2, PAIR),
+            space(BF, 2, FOUR, FOUR, tokens // 2, PAIR),
+            space(BF, FOUR, tokens // 2, PAIR),
+            space(BF, FOUR, tokens // 2, PAIR),
             space(BF, FOUR, tokens // 2, columns),
             space(BF, FOUR, tokens // 2, columns),
-            dma((18,)), dma((5,)),
-            dma, dma, dma((6,)), dma((6,)), dma((FOUR,)), dma((FOUR,)), dma((FOUR,)), dma((FOUR,)),
-            dma((2, nz // 2)), dma((2, nz // 2)), dma((nz, 2)), dma((nz, 2)), dma((nz,)), dma((nz,)),
-            dma((nz,)), dma((nz,)), dma((nx,)), dma((nx,)),
-            dma((places,)), dma((places,)), dma((places,)), dma((places,)), dma((2,)), dma((2,)),
-            dma((6,)), dma((6,)), dma((6,)), dma((6,)), dma((FOUR,)), dma((FOUR,)), dma((FOUR,)), dma((FOUR,)),
+            dma((3,)), dma((5,)),
+            dma, dma, dma((1,)), dma((4,)), dma, dma, dma, dma,
+            dma, dma((2, nz // 2)), dma((nz,)), dma,
+            dma, dma, dma, dma((3,)), dma, dma,
+            dma, dma, dma, dma, dma, dma,
+            *[dma((1,)), dma((4,))] * 4, dma((FOUR,)), dma, dma,
         ],
         compiler_params=pltpu.CompilerParams(
             collective_id=0, has_side_effects=True, vmem_limit_bytes=63 * 2**20

time: 99 us -> 89.9 us (0.908)
  Pallas kernels: 97.1 us -> 88 us
    pallas_call x1, Pallas kernels: 97.1 us -> 88 us  [local(): pl.pallas_call(layer_kernel, out_shape=jax.ShapeDtypeStruct((tokens // 2,...]
where the time goes in v6:
time: 89.9 us; the launch traced here: 89.7 us
  Pallas kernels  88 us (98%)
  local copies, waits for them, and re-layouts  1.67 us (2%)
    pallas_call x1, Pallas kernels, local(): pl.pallas_call(layer_kernel, out_shape=jax.ShapeDtypeStruct((tokens // 2,...  88 us

profile of v6, /device:TPU:1, one launch (start us, length us, event | category | flops | bytes accessed | tf_op | source)
XLA Modules:
  0.0 89.7 jit_solution(1416395248505366121)
XLA Ops:
  0.0 88.0 %layer.1 = bf16[64,2048]{1,0:T(8,128)(2,1)} custom-call(bf16[128,1024]{1,0:T(8,128)(2,1)} %bitcast.11, f32[1,2048]{1,0:T(1,128)} %bitcast.14, bf16[16,512]{1,0:T(8,128)(2,1)} %wr_ref.1, bf16[16,512]{1,0:T(8,128)(2,1)} %wk_ref.1, bf16[16,512]{1,0:T(8,128)(2,1)} %wv_ref.1, bf16[16,512]{1,0:T(8,128)(2,1)} %wq_ref.1, bf16[16,128]{1,0:T(8,128)(2,1)} %wak_ref.1, ...), custom_call_target="tpu_custom_call" | custom-call | tf_op jit(solution)/shard_map/layer/pallas_call | solution.py:925
  88.0 1.7 %copy.22 = bf16[1,64,2048]{2,1,0:T(8,128)(2,1)} copy(bf16[1,64,2048]{2,1,0:T(8,128)(2,1)} %bitcast.8) | data formatting | bytes 524288

commit v7 on v6

--- a/solution.py
+++ b/solution.py
@@ -144,7 +144,7 @@
     nz, nx = lax.axis_size("sp_0"), lax.axis_size("sp_1")
     peers = [{"fs": (f + k) % FOUR} for k in range(1, FOUR)] + [{"tp": 1 - c}]
     peers += [{"sp_0": (z + k) % nz} for k in (1, nz - 1)]
-    return peers + [{"sp_1": (x + k) % nx} for k in (1, nx - 1)]
+    return peers + [{"sp_1": (x + k) % nx} for k in range(1, nx)]
 
 
 def rope_tables(place, cos_ref, sin_ref):
@@ -198,7 +198,7 @@
         up_d_ref, up_e_ref, off_d_ref, off_e_ref, extra_ref, proj_ref, logd_ref, learn_ref,
         both_ref, hid_ref, stage_ref, cols_ref, ext_ref, load_sem,
         x_out, x_in, hid_out, hid_in, stage_out, stage_in, ext_out, ext_in,
-        ring_out, z_in, near_in, far_in, cos_ref, sin_ref, late, start_rows,
+        ring_out, z_in, near_in, far_in, rest_x_out, rest_x_in, rest_z_out, rest_z_in, cos_ref, sin_ref, late,
     ) = refs
     z, x, f, c = place_of
     nz, nx = lax.axis_size("sp_0"), lax.axis_size("sp_1")
@@ -260,22 +260,51 @@
         step = (k - 1) // 2
         return (z + nz - 1 - step) % nz if k % 2 else (z + 1 + step) % nz
 
+    main = 3 * PAIR
+
+    def rest_x_copy(k):
+        where = cols_ref.at[mine, :, main:]
+        return pltpu.make_async_remote_copy(
+            src_ref=where, dst_ref=where, send_sem=rest_x_out, recv_sem=rest_x_in,
+            device_id={"sp_1": (x + k) % nx}, device_id_type=MESH,
+        )
+
+    def rest_z_copy(block, side, step):
+        where = cols_ref.at[pl.ds(block * nx, nx), :, main:]
+        return pltpu.make_async_remote_copy(
+            src_ref=where, dst_ref=where, send_sem=rest_z_out, recv_sem=rest_z_in.at[side, step],
+            device_id={"sp_0": (z + (1 if side == 0 else nz - 1)) % nz}, device_id_type=MESH,
+        )
+
+    def rest_begin():
+        settle(cols_ref.at[0 : nx - 1, :, main:], rest_x_in)
+        rest_z_copy(z, 0, 0).start()
+        rest_z_copy(z, 1, 0).start()
+
+    def rest_pass(step):
+        for side, last in ((0, nz // 2 - 1), (1, nz // 2 - 2)):
+            if step <= last:
+                block = z_block(2 * step + 1 + side)
+                rest_z_copy(block, side, step).wait_recv()
+                if step < last:
+                    rest_z_copy(block, side, step + 1).start()
+
     def z_copy(k_from, side, step):
-        where = cols_ref.at[z_block(k_from) * nx + x]
+        where = cols_ref.at[z_block(k_from) * nx + x, :, :main]
         return pltpu.make_async_remote_copy(
             src_ref=where, dst_ref=where, send_sem=ring_out, recv_sem=z_in.at[side, step],
             device_id={"sp_0": (z + (1 if side == 0 else nz - 1)) % nz}, device_id_type=MESH,
         )
 
     def near_copy(k, side, column):
-        where = cols_ref.at[z_block(k) * nx + column]
+        where = cols_ref.at[z_block(k) * nx + column, :, :main]
         return pltpu.make_async_remote_copy(
             src_ref=where, dst_ref=where, send_sem=ring_out, recv_sem=near_in.at[k],
             device_id={"sp_1": (x + (1 if side == 0 else nx - 1)) % nx}, device_id_type=MESH,
         )
 
     def far_copy(k, column):
-        where = cols_ref.at[z_block(k) * nx + column]
+        where = cols_ref.at[z_block(k) * nx + column, :, :main]
         return pltpu.make_async_remote_copy(
             src_ref=where, dst_ref=where, send_sem=ring_out, recv_sem=far_in,
             device_id={"sp_1": (x + (1 if k % 2 == 0 else nx - 1)) % nx}, device_id_type=MESH,
@@ -288,7 +317,7 @@
         near_copy(k, 1, x).start()
 
     def pass_on(k):
-        settle(cols_ref.at[0:2], near_in.at[k])
+        settle(cols_ref.at[0:2, :, :main], near_in.at[k])
         far_copy(k, left if k % 2 == 0 else right).start()
 
     with jax.named_scope("f_stage_wait"):
@@ -296,6 +325,8 @@
     z_copy(0, 0, 0).start()
     z_copy(0, 1, 0).start()
     spread(0)
+    for k in range(1, nx):
+        rest_x_copy(k).start()
 
     with jax.named_scope("f_norm"):
         half_copy.wait_recv()
@@ -327,11 +358,14 @@
             else:
                 pass_on(k - 2)
                 pass_on(k - 1)
+            if step == 0:
+                rest_begin()
+            elif step > 1:
+                rest_pass(step - 2)
             if step == 1:
                 relay()
     with jax.named_scope("f_pass_last"):
         pass_on(nz - 1)
-    start_rows()
     with jax.named_scope("f_hid_wait"):
         arrive_near()
         arrive_far()
@@ -366,20 +400,32 @@
                 learn_ref[d, p] = learn[part]
 
     with jax.named_scope("f_far_wait"):
-        settle(cols_ref.at[0:nz], far_in)
+        settle(cols_ref.at[0:nz, :, :main], far_in)
     depth = cols_ref.shape[0] * cols_ref.shape[1]
     with jax.named_scope("f_proj"):
-        for first_col, last_col in ((0, 256), (256, 512), (512, 640)):
+        for first_col, last_col in ((0, 256), (256, 384)):
             weight = cols_ref[:, :, first_col:last_col].reshape(depth, last_col - first_col)
             result = dot(hidden, weight).astype(BF)
             for p in range(FOUR):
                 proj_ref[p, :, first_col:last_col] = result[p * tokens : (p + 1) * tokens]
 
+    rest_pass(nz // 2 - 2)
     half_copy.wait_send()
     finish_sends()
     settle(stage_ref.at[1:FOUR], stage_out)
     settle(ext_ref.at[1:FOUR], ext_out)
-    settle(cols_ref.at[0 : 4 * nz - 1], ring_out)
+    settle(cols_ref.at[0 : 4 * nz - 1, :, :main], ring_out)
+
+    def project_rest():
+        rest_pass(nz // 2 - 1)
+        weight = cols_ref[:, :, main:].reshape(depth, cols_ref.shape[2] - main)
+        result = dot(hid_ref[...].reshape(FOUR * tokens, hid_ref.shape[2]), weight).astype(BF)
+        for p in range(FOUR):
+            proj_ref[p, :, main:] = result[p * tokens : (p + 1) * tokens]
+        settle(cols_ref.at[0 : nx - 1, :, main:], rest_x_out)
+        settle(cols_ref.at[0 : nx * (nz - 1), :, main:], rest_z_out)
+
+    return project_rest
 
 
 def stacked(x):
@@ -451,9 +497,9 @@
     return first, second, third, fourth, last
 
 
-def local_maps(refs, send_halo, send_maps, rows_steps):
+def local_maps(refs, project_rest, send_halo, send_maps, rows_steps):
     proj_ref, logd_ref, learn_ref, q_ref, o_ref, msg_ref = refs
-    rows_steps[1]()
+    rows_steps[0]()
     row = iota((2 * CH, 2 * CH), 0)
     col = iota((2 * CH, 2 * CH), 1)
     t, s = row % CH, col % CH
@@ -466,6 +512,7 @@
     def one_round(it, carry):
         @pl.when(it == 1)
         def _():
+            project_rest()
             for u in range(ROUND):
                 send_maps(u)
             send_halo()
@@ -562,7 +609,7 @@
         lax.fori_loop(0, FOUR // ROUND, one_round, 0)
     for u in range(ROUND):
         send_maps(FOUR - ROUND + u)
-    rows_steps[2]()
+    rows_steps[1]()
 
 
 def folded(x, hh, first, count):
@@ -815,7 +862,7 @@
     recv_ref, sent_ref, enter_ref, halo_ref, comp_ref, total_ref,
     lin_ref, att_ref, lin_give, att_give, ready_ref, got_ref,
     load_sem, late_sem, x_out, x_in, hid_out, hid_in, stage_out, stage_in, ext_out, ext_in,
-    ring_out, z_in, near_in, far_in,
+    ring_out, z_in, near_in, far_in, rest_x_out, rest_x_in, rest_z_out, rest_z_in,
     wz_out, wz_in, wx_out, wx_in, wc_out, wc_in,
     out_sem, in_sem, back_out_sem, back_in_sem, halo_out_sem, halo_in_sem,
     lin_out, lin_in, lin_out2, lin_in2, att_out, att_in, att_out2, att_in2, give_sem, back_out, back_in,
@@ -836,13 +883,13 @@
     rows_steps = gather_rows(
         (wout_ref, rows_ref, wz_out, wz_in, wx_out, wx_in, wc_out, wc_in), place_of
     )
-    front(
+    project_rest = front(
         (
             x_ref, gain_ref, wr_ref, wk_ref, wv_ref, wq_ref, wak_ref, wav_ref, down_d_ref, down_e_ref,
             up_d_ref, up_e_ref, off_d_ref, off_e_ref, extra_ref, proj_ref, logd_ref, learn_ref,
             both_ref, hid_ref, stage_ref, cols_ref, ext_ref, load_sem,
             x_out, x_in, hid_out, hid_in, stage_out, stage_in, ext_out, ext_in,
-            ring_out, z_in, near_in, far_in, cos_ref, sin_ref, late, rows_steps[0],
+            ring_out, z_in, near_in, far_in, rest_x_out, rest_x_in, rest_z_out, rest_z_in, cos_ref, sin_ref, late,
         ),
         place_of,
     )
@@ -856,6 +903,7 @@
     )
     local_maps(
         (proj_ref, logd_ref, learn_ref, reads_ref, local_ref, msg_ref),
+        project_rest,
         send_halo,
         send_maps,
         rows_steps,
@@ -878,19 +926,17 @@
             result = term if result is None else result + term
         return result
 
-    def after_chain():
-        with jax.named_scope("o_att_wait"):
-            att_share[1]()
-            rows_steps[4]()
-        with jax.named_scope("o_att"):
-            total_ref[...] = product(att_ref, width)
-
     def after_attend():
         att_share[0]()
-        rows_steps[3]()
-
-    run(after_attend, after_chain)
+
+    run(after_attend, rows_steps[2])
     lin_share[0]()
+    rows_steps[3]()
+    with jax.named_scope("o_att_wait"):
+        att_share[1]()
+        rows_steps[4]()
+    with jax.named_scope("o_att"):
+        total_ref[...] = product(att_ref, width)
     att_share[2]()
     with jax.named_scope("o_lin_wait"):
         lin_share[1]()
@@ -962,7 +1008,7 @@
             space(BF, FOUR, tokens // 2, columns),
             dma((3,)), dma((5,)),
             dma, dma, dma((1,)), dma((4,)), dma, dma, dma, dma,
-            dma, dma((2, nz // 2)), dma((nz,)), dma,
+            dma, dma((2, nz // 2)), dma((nz,)), dma, dma, dma, dma, dma((2, nz // 2)),
             dma, dma, dma, dma((3,)), dma, dma,
             dma, dma, dma, dma, dma, dma,
             *[dma((1,)), dma((4,))] * 4, dma((FOUR,)), dma, dma,

time: 89.9 us -> 88 us (0.979)
  the two profiles are of different devices: /device:TPU:1 before, /device:TPU:2 now
where the time goes in v7:
time: 88 us; the launch traced here: 87.8 us
  Pallas kernels  86.1 us (98%)
  local copies, waits for them, and re-layouts  1.67 us (2%)
    pallas_call x1, Pallas kernels, local(): pl.pallas_call(layer_kernel, out_shape=jax.ShapeDtypeStruct((tokens // 2,...  86.1 us

profile of v7, /device:TPU:2, one launch (start us, length us, event | category | flops | bytes accessed | tf_op | source)
XLA Modules:
  0.0 87.8 jit_solution(9484062441654149672)
XLA Ops:
  0.0 86.1 %layer.1 = bf16[64,2048]{1,0:T(8,128)(2,1)} custom-call(bf16[128,1024]{1,0:T(8,128)(2,1)} %bitcast.11, f32[1,2048]{1,0:T(1,128)} %bitcast.14, bf16[16,512]{1,0:T(8,128)(2,1)} %wr_ref.1, bf16[16,512]{1,0:T(8,128)(2,1)} %wk_ref.1, bf16[16,512]{1,0:T(8,128)(2,1)} %wv_ref.1, bf16[16,512]{1,0:T(8,128)(2,1)} %wq_ref.1, bf16[16,128]{1,0:T(8,128)(2,1)} %wak_ref.1, ...), custom_call_target="tpu_custom_call" | custom-call | tf_op jit(solution)/shard_map/layer/pallas_call | solution.py:971
  86.1 1.7 %copy.22 = bf16[1,64,2048]{2,1,0:T(8,128)(2,1)} copy(bf16[1,64,2048]{2,1,0:T(8,128)(2,1)} %bitcast.8) | data formatting | bytes 524288

commit v8 on v7

--- a/solution.py
+++ b/solution.py
@@ -198,7 +198,7 @@
         up_d_ref, up_e_ref, off_d_ref, off_e_ref, extra_ref, proj_ref, logd_ref, learn_ref,
         both_ref, hid_ref, stage_ref, cols_ref, ext_ref, load_sem,
         x_out, x_in, hid_out, hid_in, stage_out, stage_in, ext_out, ext_in,
-        ring_out, z_in, near_in, far_in, rest_x_out, rest_x_in, rest_z_out, rest_z_in, cos_ref, sin_ref, late,
+        ring_out, z_in, near_in, far_in, rest_x_out, rest_x_in, rest_z_out, rest_z_in, cos_ref, sin_ref, late, early,
     ) = refs
     z, x, f, c = place_of
     nz, nx = lax.axis_size("sp_0"), lax.axis_size("sp_1")
@@ -211,10 +211,10 @@
     loads.append((x_ref, both_ref.at[c], 1))
     loads.append((extra_ref.at[0], ext_ref.at[f], 2))
     loads = [pltpu.make_async_copy(start, end, load_sem.at[number]) for start, end, number in loads]
-    for load in loads:
+    for load in early + loads + late:
         load.start()
-    for load in late:
-        load.start()
+    for load in early:
+        load.wait()
     low = iota((rows, PAIR), 1) < HD
     keys, values = wak_ref[...].astype(F32), wav_ref[...].astype(F32)
     shared = [
@@ -744,7 +744,7 @@
             for g in range(groups):
                 step = message(g * length + s)
                 comp_ref[g, s] = maps[g]
-                longer.append(maps[g] + mm3(maps[g], step[:HD]) + step)
+                longer.append(maps[g] + mm2(maps[g], step[:HD].astype(BF)) + step)
             return tuple(longer)
 
         nothing = jnp.zeros((3 * rows, HD), F32)
@@ -852,10 +852,11 @@
 
 
 def layer_kernel(
-    x_ref, gain_ref, wr_ref, wk_ref, wv_ref, wq_ref, wak_ref, wav_ref, down_d_hbm, down_e_hbm,
-    up_d_hbm, up_e_hbm, off_d_ref, off_e_ref, extra_ref, init_hbm, head_gain_ref, sink_ref,
-    lin_out_ref, att_out_ref,
+    x_ref, gain_hbm, wr_ref, wk_ref, wv_ref, wq_ref, wak_hbm, wav_hbm, down_d_hbm, down_e_hbm,
+    up_d_hbm, up_e_hbm, off_d_hbm, off_e_hbm, extra_ref, init_hbm, head_gain_hbm, sink_hbm,
+    lin_out_hbm, att_out_hbm,
     out_ref,
+    gain_ref, wak_ref, wav_ref, off_d_ref, off_e_ref, head_gain_ref, sink_ref,
     both_ref, hid_ref, stage_ref, cols_ref, ext_ref, down_d_ref, down_e_ref, up_d_ref, up_e_ref, init_ref,
     proj_ref, logd_ref, learn_ref, cos_ref, sin_ref, wout_ref,
     reads_ref, local_ref, msg_ref, rows_ref,
@@ -868,18 +869,21 @@
     lin_out, lin_in, lin_out2, lin_in2, att_out, att_in, att_out2, att_in2, give_sem, back_out, back_in,
 ):
     place_of = tuple(lax.axis_index(a) for a in ("sp_0", "sp_1", "fs", "tp"))
+    width = lin_out_hbm.shape[1]
     for peer in neighbours(place_of):
         pl.semaphore_signal(
             pltpu.get_barrier_semaphore(), inc=1, device_id=peer, device_id_type=MESH
         )
     pairs = (
         (down_d_hbm, down_d_ref), (down_e_hbm, down_e_ref), (up_d_hbm, up_d_ref), (up_e_hbm, up_e_ref),
-        (init_hbm, init_ref),
+        (init_hbm, init_ref), (off_d_hbm, off_d_ref), (off_e_hbm, off_e_ref), (head_gain_hbm, head_gain_ref),
+        (sink_hbm, sink_ref), (lin_out_hbm, wout_ref.at[:, :width]), (att_out_hbm, wout_ref.at[:, width:]),
     )
     late = [pltpu.make_async_copy(a, b, late_sem.at[k]) for k, (a, b) in enumerate(pairs)]
-    width = lin_out_ref.shape[1]
-    wout_ref[:, :width] = lin_out_ref[...]
-    wout_ref[:, width:] = att_out_ref[...]
+    early = [
+        pltpu.make_async_copy(a, b, load_sem.at[3 + k])
+        for k, (a, b) in enumerate(((gain_hbm, gain_ref), (wak_hbm, wak_ref), (wav_hbm, wav_ref)))
+    ]
     rows_steps = gather_rows(
         (wout_ref, rows_ref, wz_out, wz_in, wx_out, wx_in, wc_out, wc_in), place_of
     )
@@ -889,7 +893,7 @@
             up_d_ref, up_e_ref, off_d_ref, off_e_ref, extra_ref, proj_ref, logd_ref, learn_ref,
             both_ref, hid_ref, stage_ref, cols_ref, ext_ref, load_sem,
             x_out, x_in, hid_out, hid_in, stage_out, stage_in, ext_out, ext_in,
-            ring_out, z_in, near_in, far_in, rest_x_out, rest_x_in, rest_z_out, rest_z_in, cos_ref, sin_ref, late,
+            ring_out, z_in, near_in, far_in, rest_x_out, rest_x_in, rest_z_out, rest_z_in, cos_ref, sin_ref, late, early,
         ),
         place_of,
     )
@@ -960,8 +964,7 @@
     out_rows = linear_output_weight.shape[1]
     columns = places * out_rows
     vmem = pl.BlockSpec(memory_space=pltpu.VMEM)
-    hbm = pl.BlockSpec(memory_space=pl.ANY)
-    smem = pl.BlockSpec(memory_space=pltpu.SMEM)
+    hbm = pl.BlockSpec(memory_space=pltpu.HBM)
     dma = pltpu.SemaphoreType.DMA
     down_d, down_e = decay_down_weight.T, erasure_down_weight.T
 
@@ -971,9 +974,16 @@
     out = pl.pallas_call(
         layer_kernel,
         out_shape=jax.ShapeDtypeStruct((tokens // 2, FOUR * columns), BF),
-        in_specs=[hbm, vmem, hbm, hbm, hbm, hbm, vmem, vmem, hbm, hbm, hbm, hbm, vmem, vmem, hbm, hbm, vmem, smem, vmem, vmem],
+        in_specs=[hbm] * 20,
         out_specs=vmem,
         scratch_shapes=[
+            space(F32, 1, model),
+            space(BF, *window_key_weight.shape),
+            space(BF, *window_value_weight.shape),
+            space(F32, *decay_offset.shape),
+            space(F32, *erasure_offset.shape),
+            space(F32, 1, *head_norm_gain.shape),
+            pltpu.SMEM(query_sink_logit.shape, F32),
             space(BF, 2, tokens, model // 2),
             space(BF, FOUR, tokens, model),
             space(BF, FOUR, rows, 5 * PAIR),
@@ -1006,7 +1016,7 @@
             space(BF, FOUR, tokens // 2, PAIR),
             space(BF, FOUR, tokens // 2, columns),
             space(BF, FOUR, tokens // 2, columns),
-            dma((3,)), dma((5,)),
+            dma((6,)), dma((11,)),
             dma, dma, dma((1,)), dma((4,)), dma, dma, dma, dma,
             dma, dma((2, nz // 2)), dma((nz,)), dma, dma, dma, dma, dma((2, nz // 2)),
             dma, dma, dma, dma((3,)), dma, dma,

time: 88 us -> 86.4 us (0.982)
  Pallas kernels: 86.1 us -> 84.6 us
    pallas_call x1, Pallas kernels: 86.1 us -> 84.6 us  [local(): pl.pallas_call(layer_kernel, out_shape=jax.ShapeDtypeStruct((tokens // 2,...]
where the time goes in v8:
time: 86.4 us; the launch traced here: 86.3 us
  Pallas kernels  84.6 us (98%)
  local copies, waits for them, and re-layouts  1.67 us (2%)
    pallas_call x1, Pallas kernels, local(): pl.pallas_call(layer_kernel, out_shape=jax.ShapeDtypeStruct((tokens // 2,...  84.6 us

profile of v8, /device:TPU:2, one launch (start us, length us, event | category | flops | bytes accessed | tf_op | source)
XLA Modules:
  0.0 86.3 jit_solution(2233073044056466907)
XLA Ops:
  0.0 84.6 %layer.1 = bf16[64,2048]{1,0:T(8,128)(2,1)} custom-call(bf16[128,1024]{1,0:T(8,128)(2,1)} %bitcast.11, f32[1,2048]{1,0:T(1,128)} %bitcast.14, bf16[16,512]{1,0:T(8,128)(2,1)} %wr_ref.1, bf16[16,512]{1,0:T(8,128)(2,1)} %wk_ref.1, bf16[16,512]{1,0:T(8,128)(2,1)} %wv_ref.1, bf16[16,512]{1,0:T(8,128)(2,1)} %wq_ref.1, bf16[16,128]{1,0:T(8,128)(2,1)} %wak_hbm.1, ...), custom_call_target="tpu_custom_call" | custom-call | tf_op jit(solution)/shard_map/layer/pallas_call | solution.py:974
  84.6 1.7 %copy.22 = bf16[1,64,2048]{2,1,0:T(8,128)(2,1)} copy(bf16[1,64,2048]{2,1,0:T(8,128)(2,1)} %bitcast.8) | data formatting | bytes 524288

commit v9 on v8

--- a/solution.py
+++ b/solution.py
@@ -366,38 +366,40 @@
                 relay()
     with jax.named_scope("f_pass_last"):
         pass_on(nz - 1)
-    with jax.named_scope("f_hid_wait"):
-        arrive_near()
-        arrive_far()
-        settle(ext_ref.at[1:FOUR], ext_in)
-
     for load in late:
         load.wait()
+    settle(ext_ref.at[1:FOUR], ext_in)
     tokens = hid_ref.shape[1]
-    hidden = hid_ref[...].reshape(FOUR * tokens, hid_ref.shape[2])
-    with jax.named_scope("f_rates"):
-        decay_low = dot(hidden, down_d_ref[...], NT).astype(BF)
-        learn_low = dot(hidden, down_e_ref[...], NT).astype(BF)
+    heads = ext_ref.shape[1]
+    chosen = pl.ds(pl.multiple_of(c * heads * HD + f * PAIR, PAIR), PAIR)
+    select = ones_where(iota((heads, PAIR), 0) == 2 * f + iota((heads, PAIR), 1) // HD).astype(F32)
+
+    def rates(p):
+        rows_in = hid_ref[p]
+        decay_low = dot(rows_in, down_d_ref[...], NT).astype(BF)
+        learn_low = dot(rows_in, down_e_ref[...], NT).astype(BF)
         decay_act = jnp.tanh(decay_low.astype(F32)).astype(BF)
-        heads = ext_ref.shape[1]
-        first = c * heads * HD + f * PAIR
-        chosen = pl.ds(pl.multiple_of(first, PAIR), PAIR)
-        select = ones_where(iota((heads, PAIR), 0) == 2 * f + iota((heads, PAIR), 1) // HD).astype(F32)
-        spikes = [
-            lax.dot_general(
-                ext_ref[p], select, TN, precision=lax.Precision.HIGHEST, preferred_element_type=F32
-            )
-            for p in range(FOUR)
-        ]
+        spikes = lax.dot_general(
+            ext_ref[p], select, TN, precision=lax.Precision.HIGHEST, preferred_element_type=F32
+        )
         for d in range(2):
             pre = off_d_ref[d : d + 1, chosen] + dot(decay_act, up_d_ref[d, :, chosen])
             softplus = jnp.maximum(-pre, 0.0) + jnp.log1p(jnp.exp(-jnp.abs(pre)))
-            rate = jnp.exp(-softplus - 0.5)
-            learn = jax.nn.sigmoid(off_e_ref[d : d + 1, chosen] + dot(learn_low, up_e_ref[d, :, chosen]))
-            for p in range(FOUR):
-                part = slice(p * tokens, (p + 1) * tokens)
-                logd_ref[d, p] = spikes[p] - rate[part]
-                learn_ref[d, p] = learn[part]
+            logd_ref[d, p] = spikes - jnp.exp(-softplus - 0.5)
+            learn_ref[d, p] = jax.nn.sigmoid(
+                off_e_ref[d : d + 1, chosen] + dot(learn_low, up_e_ref[d, :, chosen])
+            )
+
+    with jax.named_scope("f_rates"):
+        rates(f)
+        arrive_near()
+        rates((f + 1) % FOUR)
+        rates((f + 3) % FOUR)
+    with jax.named_scope("f_hid_wait"):
+        arrive_far()
+    with jax.named_scope("f_rates_far"):
+        rates((f + 2) % FOUR)
+    hidden = hid_ref[...].reshape(FOUR * tokens, hid_ref.shape[2])
 
     with jax.named_scope("f_far_wait"):
         settle(cols_ref.at[0:nz, :, :main], far_in)

time: 86.4 us -> 86.8 us (level)
  the two profiles are of different devices: /device:TPU:2 before, /device:TPU:32 now
where the time goes in v9:
time: 86.8 us; the launch traced here: 86.7 us
  Pallas kernels  85 us (98%)
  local copies, waits for them, and re-layouts  1.67 us (2%)
    pallas_call x1, Pallas kernels, local(): pl.pallas_call(layer_kernel, out_shape=jax.ShapeDtypeStruct((tokens // 2,...  85 us

profile of v9, /device:TPU:32, one launch (start us, length us, event | category | flops | bytes accessed | tf_op | source)
XLA Modules:
  0.0 86.7 jit_solution(646288606813048877)
XLA Ops:
  0.0 85.0 %layer.1 = bf16[64,2048]{1,0:T(8,128)(2,1)} custom-call(bf16[128,1024]{1,0:T(8,128)(2,1)} %bitcast.11, f32[1,2048]{1,0:T(1,128)} %bitcast.14, bf16[16,512]{1,0:T(8,128)(2,1)} %wr_ref.1, bf16[16,512]{1,0:T(8,128)(2,1)} %wk_ref.1, bf16[16,512]{1,0:T(8,128)(2,1)} %wv_ref.1, bf16[16,512]{1,0:T(8,128)(2,1)} %wq_ref.1, bf16[16,128]{1,0:T(8,128)(2,1)} %wak_hbm.1, ...), custom_call_target="tpu_custom_call" | custom-call | tf_op jit(solution)/shard_map/layer/pallas_call | solution.py:976
  85.0 1.7 %copy.22 = bf16[1,64,2048]{2,1,0:T(8,128)(2,1)} copy(bf16[1,64,2048]{2,1,0:T(8,128)(2,1)} %bitcast.8) | data formatting | bytes 524288
